TPU v7x, 32 devices: a whole 2x2x4 slice. The times are simulated.
32 devices in a mesh: grp: 2 (over x), tp: 4 (over z), dp: 4 (over y, core).
Axes of the slice: x: 2, y: 2, z: 4, core: 2. Of those that a mesh axis runs over, the one named last changes fastest.
Arguments:
- tokens: bfloat16 [8, 4, 4096], P(('grp', 'tp'), None, 'dp'), parts along dimension 0, may hold values from -6 to 6
- lengths: int32 [8], P('grp'), parts along dimension 0, may hold values from 1 to 4, 8 in all
- norm_gain: float32 [2, 4096], P(None, 'dp'), may hold values from 0.1 to 1.9
- input_weight: bfloat16 [2, 4096, 8192], P(None, 'dp', 'tp'), may hold values from -0.09375 to 0.09375
- gate_weight: bfloat16 [2, 4096, 8192], P(None, 'dp', 'tp'), may hold values from -0.09375 to 0.09375
- decay_rate: float32 [2, 512, 64], P(None, 'tp'), may hold values from 0.05 to 2
- frequency: float32 [2, 512, 64], P(None, 'tp'), may hold values from 0 to 4
- log_step: float32 [2, 512], P(None, 'tp'), may hold values from -2.3 to 0
- input_map: bfloat16 [2, 512, 16, 128], P(None, 'tp'), may hold values from -1 to 1
- readout_map: bfloat16 [2, 512, 16, 128], P(None, 'tp'), may hold values from -0.5 to 0.5
- skip_weight: bfloat16 [2, 8192], P(None, 'tp'), may hold values from -4 to 4
- out_weight: bfloat16 [2, 8192, 4096], P(None, 'tp', 'dp'), may hold values from -0.0625 to 0.0625
- state: float32 [2, 8, 512, 128], P(None, ('grp', 'dp'), 'tp'), parts along dimension 1, may hold values from -5 to 5
Outputs:
- mixed: bfloat16 [8, 4, 4096], P(('grp', 'tp'), None, 'dp'), parts along dimension 0
- new_state: float32 [2, 8, 512, 128], P(None, ('grp', 'dp'), 'tp'), parts along dimension 1
There are 2 independent parts, one for each index of `grp`. A program takes and returns all parts, laid end to end along the dimension named above; an argument that names none is the same for every part. Nothing has to cross between parts.
Inputs may be any that keep to these rules, and one draw needn't show every extreme that they name: `lengths`: the number of live new positions of each sequence; positions beyond it take no part.
All inputs are finite; a program needn't handle non-finite values.
Results may differ from a plain program's by a relative error of at most 0.023.
Values may be sent and summed in bfloat16 or wider, within the bound.
No kernel may reach another device: no remote copies, remote signals or barrier semaphores. Data moves between devices by JAX's collectives and lax.ppermute only.
A program may use at most 64 MiB of HBM per device.

v0:
```python
import jax
import jax.numpy as jnp
from jax import lax
from jax.sharding import PartitionSpec as P

D = 4096
S5_IN = 16
LAYERS = 2


epsilon = 1e-06


def advance_state(
    drive_value,
    gate_value,
    carried,
    alive_mask,
    decay_rate,
    frequency,
    log_step,
    input_map,
    readout_map,
    skip_row,
):
    seq_count, new_count, inner_width = drive_value.shape
    group_count = inner_width // S5_IN
    state_half = carried.shape[-1] // 2
    step_size = jnp.exp(log_step)[:, None]
    magnitude = jnp.exp(-decay_rate * step_size)
    turn_angle = frequency * step_size
    decay_real = magnitude * jnp.cos(turn_angle)
    decay_imag = magnitude * jnp.sin(turn_angle)
    denominator = decay_rate * decay_rate + frequency * frequency
    coeff_real = (-(decay_real - 1.0) * decay_rate + decay_imag * frequency) / denominator
    coeff_imag = (-decay_imag * decay_rate - (decay_real - 1.0) * frequency) / denominator
    map_real = input_map[..., :state_half].astype(jnp.float32)
    map_imag = input_map[..., state_half:].astype(jnp.float32)
    coupled = jnp.concatenate(
        [
            coeff_real[:, None, :] * map_real - coeff_imag[:, None, :] * map_imag,
            coeff_real[:, None, :] * map_imag + coeff_imag[:, None, :] * map_real,
        ],
        axis=-1,
    )
    inputs = drive_value.astype(jnp.float32).reshape(seq_count, new_count, group_count, S5_IN)
    pushed = jnp.einsum("stgi,giq->stgq", inputs, coupled, precision=lax.Precision.HIGHEST)
    real_state = carried[..., :state_half]
    imag_state = carried[..., state_half:]
    history = []
    for position in range(new_count):
        keep = alive_mask[:, position][:, None, None] > 0.5
        next_real = (
            decay_real * real_state - decay_imag * imag_state + pushed[:, position, :, :state_half]
        )
        next_imag = (
            decay_real * imag_state + decay_imag * real_state + pushed[:, position, :, state_half:]
        )
        real_state = jnp.where(keep, next_real, real_state)
        imag_state = jnp.where(keep, next_imag, imag_state)
        history.append(jnp.concatenate([real_state, -imag_state], axis=-1))
    stacked = jnp.stack(history, axis=1)
    readout = jnp.einsum(
        "stgq,giq->stgi", stacked, readout_map.astype(jnp.float32), precision=lax.Precision.HIGHEST
    )
    readout = readout.reshape(seq_count, new_count, inner_width)
    response = readout + skip_row.astype(jnp.float32) * inputs.reshape(
        seq_count, new_count, inner_width
    )
    branch = (
        jax.nn.gelu(response) * jax.nn.silu(gate_value.astype(jnp.float32)) * alive_mask[:, :, None]
    )
    return (jnp.concatenate([real_state, imag_state], axis=-1), branch.astype(jnp.bfloat16))


def body(
    tokens,
    lengths,
    norm_gain,
    input_weight,
    gate_weight,
    decay_rate,
    frequency,
    log_step,
    input_map,
    readout_map,
    skip_weight,
    out_weight,
    state,
):
    own_seqs = state.shape[1]
    block_seqs, new_count, feature_count = tokens.shape
    all_seqs = lengths.shape[0]
    inner_width = input_weight.shape[2]
    dp_index = lax.axis_index("dp")
    tp_index = lax.axis_index("tp")
    positions = lax.broadcasted_iota(jnp.int32, (all_seqs, new_count), 1)
    alive_all = (positions < lengths[:, None]).astype(jnp.float32)
    alive_own = lax.dynamic_slice_in_dim(alive_all, dp_index * own_seqs, own_seqs, 0)
    own_rows = own_seqs * new_count
    block_count = block_seqs * new_count
    own_block = tokens
    states = []
    for layer_index in range(LAYERS):
        gathered = lax.all_gather(own_block, "tp", axis=0, tiled=True)
        flattened = gathered.reshape(all_seqs * new_count, feature_count).astype(jnp.float32)
        scaled = (flattened * norm_gain[layer_index][None, :]).astype(jnp.bfloat16)
        partial_squares = jnp.sum(flattened * flattened, axis=1)
        part_drive = jnp.dot(scaled, input_weight[layer_index], preferred_element_type=jnp.float32)
        part_gate = jnp.dot(scaled, gate_weight[layer_index], preferred_element_type=jnp.float32)
        total_squares = lax.psum(partial_squares, "dp")
        summed_drive, summed_gate = (
            lax.psum_scatter(
                part_drive.astype(jnp.bfloat16), "dp", scatter_dimension=0, tiled=True
            ).astype(jnp.float32),
            lax.psum_scatter(
                part_gate.astype(jnp.bfloat16), "dp", scatter_dimension=0, tiled=True
            ).astype(jnp.float32),
        )
        own_squares = lax.dynamic_slice_in_dim(total_squares, dp_index * own_rows, own_rows, 0)
        inverse = lax.rsqrt(own_squares / D + epsilon)[:, None]
        drive_value = (
            (inverse * summed_drive).astype(jnp.bfloat16).reshape(own_seqs, new_count, inner_width)
        )
        gate_value = (
            (inverse * summed_gate).astype(jnp.bfloat16).reshape(own_seqs, new_count, inner_width)
        )
        next_state, branch = advance_state(
            drive_value,
            gate_value,
            state[layer_index],
            alive_own,
            decay_rate[layer_index],
            frequency[layer_index],
            log_step[layer_index],
            input_map[layer_index],
            readout_map[layer_index],
            skip_weight[layer_index],
        )
        states.append(next_state)
        weight_now = out_weight[layer_index]
        projected = jnp.dot(
            lax.all_gather(branch.reshape(own_rows, inner_width), "dp", axis=0, tiled=True),
            weight_now,
            preferred_element_type=jnp.float32,
        )
        branch_sum = lax.psum_scatter(
            projected.astype(jnp.bfloat16), "tp", scatter_dimension=0, tiled=True
        ).astype(jnp.float32)
        own_base = lax.dynamic_slice_in_dim(flattened, tp_index * block_count, block_count, 0)
        own_block = (own_base + branch_sum).astype(jnp.bfloat16).reshape(tokens.shape)
    return (own_block, jnp.stack(states))


def solution(mesh):
    return jax.shard_map(
        body,
        mesh=mesh,
        in_specs=(
            P(("grp", "tp"), None, "dp"),
            P("grp"),
            P(None, "dp"),
            P(None, "dp", "tp"),
            P(None, "dp", "tp"),
            P(None, "tp", None),
            P(None, "tp", None),
            P(None, "tp"),
            P(None, "tp", None, None),
            P(None, "tp", None, None),
            P(None, "tp"),
            P(None, "tp", "dp"),
            P(None, ("grp", "dp"), "tp", None),
        ),
        out_specs=(P(("grp", "tp"), None, "dp"), P(None, ("grp", "dp"), "tp", None)),
        check_vma=False,
    )
```

profile of v0, /device:TPU:0, one launch (start us, length us, event | category | flops | bytes accessed | tf_op | source)
XLA Modules:
  0.0 198.8 jit_solution(4493405564464504982)
XLA Ops:
  7.3 15.2 %all_gather.12 = bf16[4,4,1024]{2,1,0:T(4,128)(2,1)S(1)} all-gather(bf16[1,4,1024]{2,1,0:T(4,128)(2,1)} %param.13), channel_id=1, replica_groups=mesh['grp'=2,'tp'=4,'dp'=4] {'tp'}, dimensions={0}, use_global_device_ids=true | all-gather | bytes 40960 | tf_op jit(solution)/shard_map/all_gather | solution.py:105
  22.5 0.8 fusion.153
  23.4 3.5 %fusion.21 = bf16[16,2048]{1,0:T(8,128)(2,1)} fusion(bf16[16,1024]{1,0:T(8,128)(2,1)S(1)} %convert_element_type.158, bf16[2,1024,2048]{2,1,0:T(8,128)(2,1)} %param.17), kind=kOutput, calls=%fused_computation.19 | convolution fusion | flops 67141632 | bytes 4292608 | tf_op jit(solution)/shard_map/dot_general | solution.py:110
  26.9 3.5 %fusion.18 = bf16[16,2048]{1,0:T(8,128)(2,1)} fusion(bf16[16,1024]{1,0:T(8,128)(2,1)S(1)} %convert_element_type.158, bf16[2,1024,2048]{2,1,0:T(8,128)(2,1)} %param.16), kind=kOutput, calls=%fused_computation.18 | convolution fusion | flops 67141632 | bytes 4292608 | tf_op jit(solution)/shard_map/dot_general | solution.py:109
  30.4 0.6 reshape.446
  31.2 5.6 %psum.14 = f32[16]{0:T(128)S(1)} all-reduce(f32[16]{0:T(128)S(1)} %reduce_sum.23), channel_id=1, replica_groups=mesh['grp'=2,'tp'=4,'dp'=4] {'dp'}, use_global_device_ids=true, to_apply=%region_1.0 | all-reduce | flops 16 | bytes 128 | tf_op jit(solution)/shard_map/psum | solution.py:111
  36.9 0.3 fusion.111
  37.4 0.2 slice_bitcast_fusion
  37.7 0.6 fusion.154
  40.9 0.6 dynamic-slice.1
  41.5 0.6 dynamic-slice.5
  43.7 1.7 fusion.36
  45.4 0.4 fusion.38
  45.9 17.5 %all-reduce.13.cloned.1.call-done = (bf16[16,2048]{1,0:T(8,128)(2,1)}, bf16[16,2048]{1,0:T(8,128)(2,1)}) async-done(((bf16[16,2048]{1,0:T(8,128)(2,1)}, bf16[16,2048]{1,0:T(8,128)(2,1)}), (bf16[16,2048]{1,0:T(8,128)(2,1)}, bf16[16,2048]{1,0:T(8,128)(2,1)})) %all-reduce.13.cloned.1.call-update) | async-done | bytes 131088
  63.4 0.8 multiply_convert_fusion.7
  64.2 0.1 reshape.438
  64.3 2.4 %fusion.40 = f32[128,128,4]{1,2,0:T(4,128)S(1)} fusion(f32[128,16,64]{2,1,0:T(8,128)} %get-tuple-element.37, f32[128,16,64]{2,1,0:T(8,128)} %get-tuple-element.36, bf16[4,128,16]{2,1,0:T(8,128)(2,1)S(1)} %reshape.438), kind=kOutput, calls=%fused_computation.38 | convolution fusion | flops 12845056 | bytes 1327104 | tf_op jit(solution)/shard_map/stgi,giq->stgq/dot_general | solution.py:47
  66.7 0.1 copy.73
  66.9 0.2 fusion.143
  67.2 0.6 fusion.57
  67.8 0.1 copy.74
  68.0 2.0 convolution_bitcast_fusion.1
  70.0 0.2 reshape.440
  70.1 0.9 fusion.127
  71.0 5.2 %all-gather.1 = bf16[4,4,2048]{2,1,0:T(4,128)(2,1)S(1)} all-gather(bf16[1,4,2048]{2,1,0:T(4,128)(2,1)S(1)} %fusion.127), channel_id=1, replica_groups=mesh['grp'=2,'tp'=4,'dp'=4] {'dp'}, dimensions={0}, use_global_device_ids=true | all-gather | bytes 81920 | tf_op jit(solution)/shard_map/all_gather | solution.py:143
  76.3 2.8 %fusion.30 = bf16[16,1024]{1,0:T(8,128)(2,1)S(1)} fusion(bf16[16,2048]{1,0:T(8,128)(2,1)S(1)} %reshape.456, bf16[2,2048,1024]{2,1,0:T(8,128)(2,1)} %param.24), kind=kOutput, calls=%fused_computation.32 | convolution fusion | flops 67125248 | bytes 4292608 | tf_op jit(solution)/shard_map/dot_general | solution.py:142
  79.1 19.1 %all-reduce.2 = bf16[16,1024]{1,0:T(8,128)(2,1)S(1)} all-reduce(bf16[16,1024]{1,0:T(8,128)(2,1)S(1)} %fusion.30), channel_id=5, replica_groups=mesh['grp'=2,'tp'=4,'dp'=4] {'tp'}, use_global_device_ids=true, to_apply=%region_4.5.clone | all-reduce | flops 16384 | bytes 65536
  98.3 0.8 fusion.129
  99.0 13.1 %all-gather.2 = bf16[4,4,1024]{2,1,0:T(4,128)(2,1)S(1)} all-gather(bf16[1,4,1024]{2,1,0:T(4,128)(2,1)S(1)} %fusion.129), channel_id=2, replica_groups=mesh['grp'=2,'tp'=4,'dp'=4] {'tp'}, dimensions={0}, use_global_device_ids=true | all-gather | bytes 40960 | tf_op jit(solution)/shard_map/all_gather | solution.py:105
  112.2 0.6 reshape.461
  112.9 3.5 %fusion.27 = bf16[16,2048]{1,0:T(8,128)(2,1)} fusion(bf16[16,1024]{1,0:T(8,128)(2,1)S(1)} %convert_element_type.179, bf16[2,1024,2048]{2,1,0:T(8,128)(2,1)} %param.17), kind=kOutput, calls=%fused_computation.21 | convolution fusion | flops 67141632 | bytes 4292608 | tf_op jit(solution)/shard_map/dot_general | solution.py:110
  116.4 3.5 %fusion.24 = bf16[16,2048]{1,0:T(8,128)(2,1)} fusion(bf16[16,1024]{1,0:T(8,128)(2,1)S(1)} %convert_element_type.179, bf16[2,1024,2048]{2,1,0:T(8,128)(2,1)} %param.16), kind=kOutput, calls=%fused_computation.20 | convolution fusion | flops 67141632 | bytes 4292608 | tf_op jit(solution)/shard_map/dot_general | solution.py:109
  120.0 5.9 %psum.15 = f32[16]{0:T(128)S(1)} all-reduce(f32[16]{0:T(128)S(1)} %reduce_sum.25), channel_id=1, replica_groups=mesh['grp'=2,'tp'=4,'dp'=4] {'dp'}, use_global_device_ids=true, to_apply=%region_6.7 | all-reduce | flops 16 | bytes 128 | tf_op jit(solution)/shard_map/psum | solution.py:111
  125.9 29.1 %all-reduce.11.cloned.1.call-done = (bf16[16,2048]{1,0:T(8,128)(2,1)}, bf16[16,2048]{1,0:T(8,128)(2,1)}) async-done(((bf16[16,2048]{1,0:T(8,128)(2,1)}, bf16[16,2048]{1,0:T(8,128)(2,1)}), (bf16[16,2048]{1,0:T(8,128)(2,1)}, bf16[16,2048]{1,0:T(8,128)(2,1)})) %all-reduce.11.cloned.1.call-update) | async-done | bytes 131088
  155.1 0.8 multiply_convert_fusion.4
  155.9 0.8 reshape.442
  156.7 1.7 fusion.44
  158.6 0.9 fusion.134
  159.7 0.1 copy.81
  159.9 0.9 convolution_bitcast_fusion
  160.8 0.2 reshape.444
  161.0 0.9 fusion.128
  161.9 5.2 %all-gather.3 = bf16[4,4,2048]{2,1,0:T(4,128)(2,1)S(1)} all-gather(bf16[1,4,2048]{2,1,0:T(4,128)(2,1)S(1)} %fusion.128), channel_id=1, replica_groups=mesh['grp'=2,'tp'=4,'dp'=4] {'dp'}, dimensions={0}, use_global_device_ids=true | all-gather | bytes 81920 | tf_op jit(solution)/shard_map/all_gather | solution.py:143
  167.2 2.8 %fusion.33 = bf16[16,1024]{1,0:T(8,128)(2,1)S(1)} fusion(bf16[16,2048]{1,0:T(8,128)(2,1)S(1)} %reshape.460, bf16[2,2048,1024]{2,1,0:T(8,128)(2,1)} %param.24), kind=kOutput, calls=%fused_computation.33 | convolution fusion | flops 67125248 | bytes 4292608 | tf_op jit(solution)/shard_map/dot_general | solution.py:142
  170.0 19.0 %all-reduce.5 = bf16[16,1024]{1,0:T(8,128)(2,1)S(1)} all-reduce(bf16[16,1024]{1,0:T(8,128)(2,1)S(1)} %fusion.33), channel_id=8, replica_groups=mesh['grp'=2,'tp'=4,'dp'=4] {'tp'}, use_global_device_ids=true, to_apply=%region_9.10.clone | all-reduce | flops 16384 | bytes 65536
  189.0 0.9 pad_maximum_fusion
  189.9 0.8 copy.83
  190.6 1.4 fusion.130
  (70 shorter events, 1.9 us)
Async XLA Ops:
  7.2 33.8 %copy-start.12 = (u32[32]{0:T(128)S(1)}, u32[32]{0:T(128)}, u32[]{:S(2)}) copy-start(u32[32]{0:T(128)} %constant.47) | copy-start | bytes 388
  7.2 34.3 %copy-start.11 = (u32[32]{0:T(128)S(1)}, u32[32]{0:T(128)}, u32[]{:S(2)}) copy-start(u32[32]{0:T(128)} %constant.55) | copy-start | bytes 388
  7.2 23.9 %copy-start.10 = (s32[4]{0:T(128)S(1)}, s32[4]{0:T(128)}, u32[]{:S(2)}) copy-start(s32[4]{0:T(128)} %param.14) | copy-start | bytes 52
  7.2 29.7 %copy-start.9 = (f32[2,128]{1,0:T(2,128)S(1)}, f32[2,128]{1,0:T(2,128)}, u32[]{:S(2)}) copy-start(f32[2,128]{1,0:T(2,128)} %param.20) | copy-start | bytes 3076
  7.2 29.7 %copy-start.2 = (f32[2,128,64]{1,2,0:T(8,128)S(1)}, f32[2,128,64]{1,2,0:T(8,128)}, u32[]{:S(2)}) copy-start(f32[2,128,64]{1,2,0:T(8,128)} %param.18) | copy-start | bytes 196612
  7.2 29.7 %copy-start.3 = (f32[2,128,64]{1,2,0:T(8,128)S(1)}, f32[2,128,64]{1,2,0:T(8,128)}, u32[]{:S(2)}) copy-start(f32[2,128,64]{1,2,0:T(8,128)} %param.19) | copy-start | bytes 196612
  7.2 30.2 %copy-start = (bf16[2,128,16,128]{3,2,1,0:T(8,128)(2,1)S(1)}, bf16[2,128,16,128]{3,2,1,0:T(8,128)(2,1)}, u32[]{:S(2)}) copy-start(bf16[2,128,16,128]{3,2,1,0:T(8,128)(2,1)} %param.21) | copy-start | bytes 3145732
  7.2 30.4 %copy-start.4 = (f32[2,1,128,128]{3,2,1,0:T(8,128)S(1)}, f32[2,1,128,128]{3,2,1,0:T(8,128)}, u32[]{:S(2)}) copy-start(f32[2,1,128,128]{3,2,1,0:T(8,128)} %param.25) | copy-start | bytes 393220
  7.3 33.6 %copy-start.5 = (bf16[2,2048]{1,0:T(2,128)(2,1)S(1)}, bf16[2,2048]{1,0:T(2,128)(2,1)}, u32[]{:S(2)}) copy-start(bf16[2,2048]{1,0:T(2,128)(2,1)} %param.23) | copy-start | bytes 24580
  7.3 56.1 %all-reduce.13.cloned.1.call-start = ((), (), s32[]{:S(2)}) async-start(), calls=%async_computation.1 | async-start | bytes 262144
  30.4 124.7 %all-reduce.11.cloned.1.call-start = ((), (), s32[]{:S(2)}) async-start(), calls=%async_computation | async-start | bytes 262144
  31.1 39.0 %copy-start.6 = (f32[4]{0:T(128)}, f32[4]{0:T(128)S(1)}, u32[]{:S(2)}) copy-start(f32[4]{0:T(128)S(1)} %fusion.163) | copy-start | bytes 52
  79.1 80.7 %copy-start.1 = (bf16[2,128,16,128]{3,2,1,0:T(8,128)(2,1)S(1)}, bf16[2,128,16,128]{3,2,1,0:T(8,128)(2,1)}, u32[]{:S(2)}) copy-start(bf16[2,128,16,128]{3,2,1,0:T(8,128)(2,1)} %param.22) | copy-start | bytes 3145732
  112.9 48.1 %copy-start.7 = (f32[4]{0:T(128)S(1)}, f32[4]{0:T(128)}, u32[]{:S(2)}) copy-start(f32[4]{0:T(128)} %copy-done.6) | copy-start | bytes 52
  125.9 30.8 %copy-start.8 = (f32[4]{0:T(128)}, f32[4]{0:T(128)S(1)}, u32[]{:S(2)}) copy-start(f32[4]{0:T(128)S(1)} %add_rsqrt_fusion) | copy-start | bytes 52
Sparse Core Ops, SparseCore 0:
  30.5 32.8 all-reduce.12
  126.0 29.0 all-reduce.10
where the time goes:
time: 200 us; the launch traced here: 199 us
  blocking collectives  88.4 us (44%)
  waiting for transfers between devices  46.7 us (23%)
  matrix products  26.6 us (13%)
  between operations  18.3 us (9%)
  other arithmetic  11.3 us (6%)
  local copies, waits for them, and re-layouts  7.52 us (4%)
    unnamed x4, waiting for transfers between devices  46.7 us
    unnamed x2, blocking collectives  38.1 us
    all_gather x2, blocking collectives, body(): gathered = lax.all_gather(own_block, 'tp', axis=0, tiled=True)  28.3 us
    psum x2, blocking collectives, body(): total_squares = lax.psum(partial_squares, 'dp')  11.5 us
    all_gather x2, blocking collectives, body(): lax.all_gather(branch.reshape(own_rows, inner_width), 'dp', axis=0, tiled...  10.5 us
    dot_general x2, matrix products, body(): jnp.dot(scaled, gate_weight[layer_index], preferred_element_type=jnp.floa...  6.96 us
    dot_general x2, matrix products, body(): jnp.dot(scaled, input_weight[layer_index], preferred_element_type=jnp.flo...  6.92 us
    dot_general x2, matrix products, body(): jnp.dot(lax.all_gather(branch.reshape(own_rows, inner_width), 'dp', axis=...  5.69 us
  transfers between devices with their start and end apart: 2, of which 2 were waited for; matrix products, arithmetic and copies ran while one was open for 3% of the time, Pallas kernels for 0%

commit v1 on v0

--- a/solution.py
+++ b/solution.py
@@ -73,6 +73,65 @@
     return (jnp.concatenate([real_state, imag_state], axis=-1), branch.astype(jnp.bfloat16))
 
 
+def direct(size):
+    return 1 < size <= 8 and size & (size - 1) == 0
+
+
+def swap(value, axis, distance, size):
+    return lax.ppermute(value, axis, [(i, i ^ distance) for i in range(size)])
+
+
+def gather_rows(block, axis, size):
+    if not direct(size):
+        return lax.all_gather(block, axis, axis=0, tiled=True)
+    index = lax.axis_index(axis)
+    slots = jnp.stack([block] + [swap(block, axis, k, size) for k in range(1, size)])
+    ordered = [lax.dynamic_index_in_dim(slots, index ^ s, 0, keepdims=False) for s in range(size)]
+    return jnp.concatenate(ordered, axis=0)
+
+
+def exchange_rows(value, axis, size):
+    index = lax.axis_index(axis)
+    rows = value.shape[0] // size
+    blocks = [
+        lax.dynamic_slice_in_dim(value, (index ^ k) * rows, rows, 0) for k in range(size)
+    ]
+    return [blocks[0]] + [swap(blocks[k], axis, k, size) for k in range(1, size)]
+
+
+def split_three(value):
+    pieces = []
+    for _ in range(3):
+        piece = lax.reduce_precision(value, 8, 7)
+        pieces.append(piece.astype(jnp.bfloat16))
+        value = value - piece
+    return pieces
+
+
+def scatter_projections(part_drive, part_gate, squares, axis, size):
+    index = lax.axis_index(axis)
+    width = part_drive.shape[1]
+    rows = part_drive.shape[0] // size
+    if not direct(size):
+        total = lax.psum(squares, axis)
+        own = lax.dynamic_slice_in_dim(total, index * rows, rows, 0)
+        drive, gate = (
+            lax.psum_scatter(
+                part.astype(jnp.bfloat16), axis, scatter_dimension=0, tiled=True
+            ).astype(jnp.float32)
+            for part in (part_drive, part_gate)
+        )
+        return drive, gate, own
+    extra = jnp.stack(split_three(squares), axis=1)
+    extra = jnp.pad(extra, ((0, 0), (0, 128 - extra.shape[1])))
+    message = jnp.concatenate(
+        [part_drive.astype(jnp.bfloat16), part_gate.astype(jnp.bfloat16), extra], axis=1
+    )
+    total = sum(part.astype(jnp.float32) for part in exchange_rows(message, axis, size))
+    own = jnp.sum(total[:, 2 * width :], axis=1)
+    return total[:, :width], total[:, width : 2 * width], own
+
+
 def body(
     tokens,
     lengths,
@@ -94,30 +153,24 @@
     inner_width = input_weight.shape[2]
     dp_index = lax.axis_index("dp")
     tp_index = lax.axis_index("tp")
+    dp_size = lax.axis_size("dp")
+    tp_size = lax.axis_size("tp")
     positions = lax.broadcasted_iota(jnp.int32, (all_seqs, new_count), 1)
     alive_all = (positions < lengths[:, None]).astype(jnp.float32)
     alive_own = lax.dynamic_slice_in_dim(alive_all, dp_index * own_seqs, own_seqs, 0)
     own_rows = own_seqs * new_count
     block_count = block_seqs * new_count
-    own_block = tokens
     states = []
+    gathered = gather_rows(tokens.reshape(block_count, feature_count), "tp", tp_size)
     for layer_index in range(LAYERS):
-        gathered = lax.all_gather(own_block, "tp", axis=0, tiled=True)
-        flattened = gathered.reshape(all_seqs * new_count, feature_count).astype(jnp.float32)
+        flattened = gathered.astype(jnp.float32)
         scaled = (flattened * norm_gain[layer_index][None, :]).astype(jnp.bfloat16)
         partial_squares = jnp.sum(flattened * flattened, axis=1)
         part_drive = jnp.dot(scaled, input_weight[layer_index], preferred_element_type=jnp.float32)
         part_gate = jnp.dot(scaled, gate_weight[layer_index], preferred_element_type=jnp.float32)
-        total_squares = lax.psum(partial_squares, "dp")
-        summed_drive, summed_gate = (
-            lax.psum_scatter(
-                part_drive.astype(jnp.bfloat16), "dp", scatter_dimension=0, tiled=True
-            ).astype(jnp.float32),
-            lax.psum_scatter(
-                part_gate.astype(jnp.bfloat16), "dp", scatter_dimension=0, tiled=True
-            ).astype(jnp.float32),
-        )
-        own_squares = lax.dynamic_slice_in_dim(total_squares, dp_index * own_rows, own_rows, 0)
+        summed_drive, summed_gate, own_squares = scatter_projections(
+            part_drive, part_gate, partial_squares, "dp", dp_size
+        )
         inverse = lax.rsqrt(own_squares / D + epsilon)[:, None]
         drive_value = (
             (inverse * summed_drive).astype(jnp.bfloat16).reshape(own_seqs, new_count, inner_width)
@@ -140,15 +193,28 @@
         states.append(next_state)
         weight_now = out_weight[layer_index]
         projected = jnp.dot(
-            lax.all_gather(branch.reshape(own_rows, inner_width), "dp", axis=0, tiled=True),
+            gather_rows(branch.reshape(own_rows, inner_width), "dp", dp_size),
             weight_now,
             preferred_element_type=jnp.float32,
-        )
-        branch_sum = lax.psum_scatter(
-            projected.astype(jnp.bfloat16), "tp", scatter_dimension=0, tiled=True
-        ).astype(jnp.float32)
+        ).astype(jnp.bfloat16)
+        last = layer_index == LAYERS - 1
+        if direct(tp_size) and not last:
+            parts = [projected] + [swap(projected, "tp", k, tp_size) for k in range(1, tp_size)]
+            total = sum(part.astype(jnp.float32) for part in parts)
+            gathered = (flattened + total).astype(jnp.bfloat16)
+            continue
+        if direct(tp_size):
+            parts = exchange_rows(projected, "tp", tp_size)
+            branch_sum = sum(part.astype(jnp.float32) for part in parts)
+        else:
+            branch_sum = lax.psum_scatter(
+                projected, "tp", scatter_dimension=0, tiled=True
+            ).astype(jnp.float32)
         own_base = lax.dynamic_slice_in_dim(flattened, tp_index * block_count, block_count, 0)
-        own_block = (own_base + branch_sum).astype(jnp.bfloat16).reshape(tokens.shape)
+        own_block = (own_base + branch_sum).astype(jnp.bfloat16)
+        if not last:
+            gathered = lax.all_gather(own_block, "tp", axis=0, tiled=True)
+    own_block = own_block.reshape(tokens.shape)
     return (own_block, jnp.stack(states))
 
 

time: 200 us -> 80.2 us (0.40)
  blocking collectives: 88.4 us -> 0 us
  waiting for transfers between devices: 46.7 us -> 14.1 us
  starting transfers between devices: 0.08 us -> 22.3 us
  between operations: 18.3 us -> 3.73 us
  matrix products: 26.6 us -> 22.8 us
  other arithmetic: 11.3 us -> 7.85 us
    unnamed x4 -> x0, waiting for transfers between devices: 46.7 us -> none
    all_gather x4 -> x0, blocking collectives: 38.8 us -> none  [the longest x2 28.3 us: body(): gathered = lax.all_gather(own_block, 'tp', axis=0, tiled=True)]
    unnamed x2 -> x0, blocking collectives: 38.1 us -> none
    ppermute x0 -> x21, starting transfers between devices: none -> 22.3 us  [swap(): return lax.ppermute(value, axis, [(i, i ^ distance) for i in range(size)])]
    ppermute x0 -> x21, waiting for transfers between devices: none -> 14.1 us  [swap(): return lax.ppermute(value, axis, [(i, i ^ distance) for i in range(size)])]
    psum x2 -> x0, blocking collectives: 11.5 us -> none  [body(): total_squares = lax.psum(partial_squares, 'dp')]
    unnamed x3 -> x0, other arithmetic: 2.6 us -> none
    dot_general x2, matrix products: 4.09 us -> 1.7 us  [advance_state(): jnp.einsum('stgi,giq->stgq', inputs, coupled, precision=lax.Precision.HIG...]
  transfers between devices with their start and end apart: 2 -> 21, of which waited for: 2 -> 9; matrix products, arithmetic and copies ran while one was open for 3% -> 15% of each run, Pallas kernels for 0% -> 0%
where the time goes in v1:
time: 80.2 us; the launch traced here: 79.4 us
  matrix products  22.8 us (28%)
  starting transfers between devices  22.3 us (28%)
  waiting for transfers between devices  14.1 us (18%)
  local copies, waits for them, and re-layouts  8.72 us (11%)
  other arithmetic  7.85 us (10%)
  between operations  3.73 us (5%)
    ppermute x21, starting transfers between devices, swap(): return lax.ppermute(value, axis, [(i, i ^ distance) for i in range(size)])  22.3 us
    ppermute x21, waiting for transfers between devices, swap(): return lax.ppermute(value, axis, [(i, i ^ distance) for i in range(size)])  14.1 us
    dot_general x2, matrix products, body(): jnp.dot(scaled, gate_weight[layer_index], preferred_element_type=jnp.floa...  5.71 us
    dot_general x2, matrix products, body(): jnp.dot(scaled, input_weight[layer_index], preferred_element_type=jnp.flo...  5.71 us
    dot_general x2, matrix products, body(): jnp.dot(gather_rows(branch.reshape(own_rows, inner_width), 'dp', dp_size)...  5.69 us
    dot_general x2, matrix products, advance_state(): jnp.einsum('stgq,giq->stgi', stacked, readout_map.astype(jnp.float32), pr...  3.94 us
    div x1, other arithmetic, advance_state(): (-(decay_real - 1.0) * decay_rate + decay_imag * frequency) / denominator  1.72 us
    dot_general x2, matrix products, advance_state(): jnp.einsum('stgi,giq->stgq', inputs, coupled, precision=lax.Precision.HIG...  1.7 us
  transfers between devices with their start and end apart: 21, of which 9 were waited for; matrix products, arithmetic and copies ran while one was open for 15% of the time, Pallas kernels for 0%

profile of v1, /device:TPU:0, one launch (start us, length us, event | category | flops | bytes accessed | tf_op | source)
XLA Modules:
  0.0 79.4 jit_solution(4355566715863542931)
XLA Ops:
  0.6 3.1 %collective-permute-start = (bf16[4,1024]{1,0:T(4,128)(2,1)}, bf16[4,1024]{1,0:T(4,128)(2,1)}, u32[]{:S(2)}, u32[]{:S(2)}) collective-permute-start(bf16[4,1024]{1,0:T(4,128)(2,1)} %bitcast.424), channel_id=1, source_target_pairs={{0,4},{4,0},{8,12},{12,8},{1,5},{5,1},{9,13},{13,9},{2,6},{6,2},{1... | collective-permute-start | bytes 24584 | tf_op jit(solution)/shard_map/ppermute | solution.py:81
  3.7 2.6 %collective-permute-start.1 = (bf16[4,1024]{1,0:T(4,128)(2,1)}, bf16[4,1024]{1,0:T(4,128)(2,1)}, u32[]{:S(2)}, u32[]{:S(2)}) collective-permute-start(bf16[4,1024]{1,0:T(4,128)(2,1)} %bitcast.425), channel_id=1, source_target_pairs={{0,8},{4,12},{8,0},{12,4},{1,9},{5,13},{9,1},{13,5},{2,10},{6,14},... | collective-permute-start | bytes 24584 | tf_op jit(solution)/shard_map/ppermute | solution.py:81
  6.3 1.4 %fusion.184 = (f32[1,1024]{1,0:T(1,128)S(1)}, f32[1,1024]{1,0:T(1,128)}) fusion(f32[2,1024]{1,0:T(2,128)} %param.15), kind=kLoop, calls=%fused_computation.290 | loop fusion | bytes 16384 | tf_op jit(solution)/shard_map/slice | solution.py:167
  7.7 0.8 exponential_bitcast_fusion.1
  8.5 1.7 %fusion.144 = (f32[128,64]{0,1:T(8,128)S(1)}, f32[128,64]{0,1:T(8,128)S(1)}, f32[128,64]{0,1:T(8,128)}, f32[128,64]{0,1:T(8,128)}) fusion(f32[2,128,64]{1,2,0:T(8,128)} %param.18, f32[2,128,64]{1,2,0:T(8,128)} %param.19, f32[128]{0:T(128)S(1)} %get-tuple-element.73, f32[128]{0:T(128)S(1)} %get-tuple-element.74), kind=kLoop, calls=%fused_computation.207 | loop fusion | flops 311296 | bytes 263168 | tf_op jit(solution)/shard_map/div | solution.py:35
  10.4 1.4 %slice_bitcast_fusion.1 = (bf16[128,16,128]{2,1,0:T(8,128)(2,1)S(1)}, bf16[128,16,128]{2,1,0:T(8,128)(2,1)S(1)}) fusion(bf16[2,128,16,128]{3,2,1,0:T(8,128)(2,1)} %param.21), kind=kLoop, calls=%fused_computation.51 | loop fusion | bytes 2097152 | tf_op jit(solution)/shard_map/squeeze | solution.py:189
  11.8 0.8 fusion.155
  12.6 0.9 %fusion.183 = (f32[1,1,128,128]{3,2,1,0:T(8,128)S(1)}, f32[1,1,128,128]{3,2,1,0:T(8,128)S(1)}) fusion(f32[2,1,128,128]{3,2,1,0:T(8,128)} %param.25), kind=kLoop, calls=%fused_computation.289 | loop fusion | bytes 262144 | tf_op jit(solution)/shard_map/slice | solution.py:184
  13.4 1.4 %slice_convert_fusion = (f32[1,2048]{1,0:T(1,128)S(1)}, f32[1,2048]{1,0:T(1,128)}) fusion(bf16[2,2048]{1,0:T(2,128)(2,1)} %param.23), kind=kLoop, calls=%fused_computation.240 | loop fusion | flops 4096 | bytes 24576 | tf_op jit(solution)/shard_map/convert_element_type | solution.py:67
  14.8 0.4 fusion.36
  15.2 0.7 fusion.185
  15.9 0.8 pad_maximum_fusion.7
  17.0 2.9 %fusion.18 = bf16[16,2048]{1,0:T(8,128)(2,1)S(1)} fusion(bf16[2,1024,2048]{2,1,0:T(8,128)(2,1)} %param.16, f32[1024]{0:T(1024)} %bitcast.427, bf16[4,1024]{1,0:T(4,128)(2,1)S(1)} %get-tuple-element.66, bf16[4,1024]{1,0:T(4,128)(2,1)S(1)} %get-tuple-element.67, bf16[4,1024]{1,0:T(4,128)(2,1)S(1)} %get-tuple-element.68, bf16[4,1024]{1,0:T(4,128)(2,1)S(1)} %get-tuple-element.65), kind=kOutput, calls=%fused_computation.18 | convolution fusion | flops 67305472 | bytes 4296704 | tf_op jit(solution)/shard_map/dot_general | solution.py:169
  19.9 2.9 %fusion.21 = bf16[16,2048]{1,0:T(8,128)(2,1)S(1)} fusion(bf16[2,1024,2048]{2,1,0:T(8,128)(2,1)} %param.17, f32[1024]{0:T(1024)} %bitcast.428, bf16[4,1024]{1,0:T(4,128)(2,1)S(1)} %get-tuple-element.66, bf16[4,1024]{1,0:T(4,128)(2,1)S(1)} %get-tuple-element.67, bf16[4,1024]{1,0:T(4,128)(2,1)S(1)} %get-tuple-element.68, bf16[4,1024]{1,0:T(4,128)(2,1)S(1)} %get-tuple-element.65), kind=kOutput, calls=%fused_computation.19 | convolution fusion | flops 67305472 | bytes 4296704 | tf_op jit(solution)/shard_map/dot_general | solution.py:170
  22.9 1.8 %collective-permute-start.4 = (bf16[4,4224]{1,0:T(4,128)(2,1)S(1)}, bf16[4,4224]{1,0:T(4,128)(2,1)S(1)}, u32[]{:S(2)}, u32[]{:S(2)}) collective-permute-start(bf16[4,4224]{1,0:T(4,128)(2,1)S(1)} %get-tuple-element.41), channel_id=1, source_target_pairs={{0,2},{1,3},{2,0},{3,1},{4,6},{5,7},{6,4},{7,5},{8,10},{9,11},{10,... | collective-permute-start | bytes 101384 | tf_op jit(solution)/shard_map/ppermute | solution.py:81
  24.7 0.7 fusion.188
  28.6 0.8 %fusion.40 = f32[128,128,4]{1,2,0:T(4,128)S(1)} fusion(f32[128,16,64]{2,1,0:T(8,128)S(1)} %get-tuple-element.33, f32[128,16,64]{2,1,0:T(8,128)S(1)} %get-tuple-element.32, bf16[4,128,16]{2,1,0:T(8,128)(2,1)S(1)} %reshape.487), kind=kOutput, calls=%fused_computation.38 | convolution fusion | flops 12845056 | bytes 1327104 | tf_op jit(solution)/shard_map/stgi,giq->stgq/dot_general | solution.py:47
  30.1 2.0 %convolution_bitcast_fusion.1 = f32[1,4,128,16]{3,1,2,0:T(4,128)S(1)} fusion(f32[4,128,128]{2,0,1:T(4,128)S(1)} %copy.85, bf16[2,128,16,128]{3,2,1,0:T(8,128)(2,1)} %param.22), kind=kOutput, calls=%fused_computation.31 | convolution fusion | flops 12582912 | bytes 819200 | tf_op jit(solution)/shard_map/stgq,giq->stgi/dot_general | solution.py:63
  32.4 0.4 collective-permute-start.6
  32.8 1.7 %collective-permute-start.7 = (bf16[4,2048]{1,0:T(4,128)(2,1)S(1)}, bf16[4,2048]{1,0:T(4,128)(2,1)S(1)}, u32[]{:S(2)}, u32[]{:S(2)}) collective-permute-start(bf16[4,2048]{1,0:T(4,128)(2,1)S(1)} %multiply_convert_fusion.2), channel_id=1, source_target_pairs={{0,2},{1,3},{2,0},{3,1},{4,6},{5,7},{6,4},{7,5},{8,10},{9,11},{10,... | collective-permute-start | bytes 49160 | tf_op jit(solution)/shard_map/ppermute | solution.py:81
  34.5 2.0 %collective-permute-done.7 = bf16[4,2048]{1,0:T(4,128)(2,1)S(1)} collective-permute-done((bf16[4,2048]{1,0:T(4,128)(2,1)S(1)}, bf16[4,2048]{1,0:T(4,128)(2,1)S(1)}, u32[]{:S(2)}, u32[]{:S(2)}) %collective-permute-start.7) | collective-permute-done | bytes 16416 | tf_op jit(solution)/shard_map/ppermute | solution.py:81
  36.5 1.3 %collective-permute-done.8 = bf16[4,2048]{1,0:T(4,128)(2,1)S(1)} collective-permute-done((bf16[4,2048]{1,0:T(4,128)(2,1)S(1)}, bf16[4,2048]{1,0:T(4,128)(2,1)S(1)}, u32[]{:S(2)}, u32[]{:S(2)}) %collective-permute-start.8) | collective-permute-done | bytes 16416 | tf_op jit(solution)/shard_map/ppermute | solution.py:81
  37.9 2.8 %fusion.30 = bf16[16,1024]{1,0:T(8,128)(2,1)S(1)} fusion(bf16[2,2048,1024]{2,1,0:T(8,128)(2,1)} %param.24, bf16[4,2048]{1,0:T(4,128)(2,1)S(1)} %get-tuple-element.55, bf16[4,2048]{1,0:T(4,128)(2,1)S(1)} %get-tuple-element.56, bf16[4,2048]{1,0:T(4,128)(2,1)S(1)} %get-tuple-element.57, bf16[4,2048]{1,0:T(4,128)(2,1)S(1)} %get-tuple-element.54), kind=kOutput, calls=%fused_computation.32 | convolution fusion | flops 67387392 | bytes 4292608 | tf_op jit(solution)/shard_map/dot_general | solution.py:195
  40.8 1.7 %collective-permute-start.10 = (bf16[16,1024]{1,0:T(8,128)(2,1)S(1)}, bf16[16,1024]{1,0:T(8,128)(2,1)S(1)}, u32[]{:S(2)}, u32[]{:S(2)}) collective-permute-start(bf16[16,1024]{1,0:T(8,128)(2,1)S(1)} %fusion.30), channel_id=1, source_target_pairs={{0,8},{4,12},{8,0},{12,4},{1,9},{5,13},{9,1},{13,5},{2,10},{6,14},... | collective-permute-start | bytes 98312 | tf_op jit(solution)/shard_map/ppermute | solution.py:81
  42.5 2.0 %collective-permute-start.11 = (bf16[16,1024]{1,0:T(8,128)(2,1)S(1)}, bf16[16,1024]{1,0:T(8,128)(2,1)S(1)}, u32[]{:S(2)}, u32[]{:S(2)}) collective-permute-start(bf16[16,1024]{1,0:T(8,128)(2,1)S(1)} %fusion.30), channel_id=1, source_target_pairs={{0,12},{4,8},{8,4},{12,0},{1,13},{5,9},{9,5},{13,1},{2,14},{6,10},... | collective-permute-start | bytes 98312 | tf_op jit(solution)/shard_map/ppermute | solution.py:81
  44.4 0.5 collective-permute-start.9
  45.2 1.1 %collective-permute-done.10 = bf16[16,1024]{1,0:T(8,128)(2,1)S(1)} collective-permute-done((bf16[16,1024]{1,0:T(8,128)(2,1)S(1)}, bf16[16,1024]{1,0:T(8,128)(2,1)S(1)}, u32[]{:S(2)}, u32[]{:S(2)}) %collective-permute-start.10) | collective-permute-done | bytes 32800 | tf_op jit(solution)/shard_map/ppermute | solution.py:81
  46.3 2.1 %collective-permute-done.11 = bf16[16,1024]{1,0:T(8,128)(2,1)S(1)} collective-permute-done((bf16[16,1024]{1,0:T(8,128)(2,1)S(1)}, bf16[16,1024]{1,0:T(8,128)(2,1)S(1)}, u32[]{:S(2)}, u32[]{:S(2)}) %collective-permute-start.11) | collective-permute-done | bytes 32800 | tf_op jit(solution)/shard_map/ppermute | solution.py:81
  48.7 2.8 %fusion.24 = bf16[16,2048]{1,0:T(8,128)(2,1)S(1)} fusion(bf16[2,1024,2048]{2,1,0:T(8,128)(2,1)} %param.16, f32[16,1024]{1,0:T(8,128)S(1)} %get-tuple-element.17, f32[1024]{0:T(1024)S(1)} %bitcast.414), kind=kOutput, calls=%fused_computation.20 | convolution fusion | flops 67174400 | bytes 4329472 | tf_op jit(solution)/shard_map/dot_general | solution.py:169
  51.5 2.9 %fusion.27 = bf16[16,2048]{1,0:T(8,128)(2,1)S(1)} fusion(bf16[2,1024,2048]{2,1,0:T(8,128)(2,1)} %param.17, f32[16,1024]{1,0:T(8,128)S(1)} %get-tuple-element.17, f32[1024]{0:T(1024)S(1)} %bitcast.415), kind=kOutput, calls=%fused_computation.21 | convolution fusion | flops 67174400 | bytes 4329472 | tf_op jit(solution)/shard_map/dot_general | solution.py:170
  54.7 0.6 collective-permute-start.13
  55.3 1.2 %collective-permute-start.14 = (bf16[4,4224]{1,0:T(4,128)(2,1)S(1)}, bf16[4,4224]{1,0:T(4,128)(2,1)S(1)}, u32[]{:S(2)}, u32[]{:S(2)}) collective-permute-start(bf16[4,4224]{1,0:T(4,128)(2,1)S(1)} %get-tuple-element.37), channel_id=1, source_target_pairs={{0,3},{1,2},{2,1},{3,0},{4,7},{5,6},{6,5},{7,4},{8,11},{9,10},{10,... | collective-permute-start | bytes 101384 | tf_op jit(solution)/shard_map/ppermute | solution.py:81
  56.5 0.4 fusion.38
  57.0 2.0 %collective-permute-done.13 = bf16[4,4224]{1,0:T(4,128)(2,1)S(1)} collective-permute-done((bf16[4,4224]{1,0:T(4,128)(2,1)S(1)}, bf16[4,4224]{1,0:T(4,128)(2,1)S(1)}, u32[]{:S(2)}, u32[]{:S(2)}) %collective-permute-start.13) | collective-permute-done | bytes 33824 | tf_op jit(solution)/shard_map/ppermute | solution.py:81
  59.5 0.8 %fusion.44 = f32[128,128,4]{1,2,0:T(4,128)S(1)} fusion(f32[128,16,64]{2,1,0:T(8,128)S(1)} %get-tuple-element.35, f32[128,16,64]{2,1,0:T(8,128)S(1)} %get-tuple-element.34, bf16[4,128,16]{2,1,0:T(8,128)(2,1)S(1)} %reshape.490), kind=kOutput, calls=%fused_computation.42 | convolution fusion | flops 12845056 | bytes 1327104 | tf_op jit(solution)/shard_map/stgi,giq->stgq/dot_general | solution.py:47
  61.0 2.0 %convolution_bitcast_fusion = f32[1,4,128,16]{3,1,2,0:T(4,128)S(1)} fusion(f32[4,128,128]{2,0,1:T(4,128)S(1)} %copy.93, bf16[2,128,16,128]{3,2,1,0:T(8,128)(2,1)} %param.22), kind=kOutput, calls=%fused_computation.30 | convolution fusion | flops 12582912 | bytes 819200 | tf_op jit(solution)/shard_map/stgq,giq->stgi/dot_general | solution.py:63
  63.3 0.2 collective-permute-start.15
  63.5 1.1 %collective-permute-start.16 = (bf16[4,2048]{1,0:T(4,128)(2,1)S(1)}, bf16[4,2048]{1,0:T(4,128)(2,1)S(1)}, u32[]{:S(2)}, u32[]{:S(2)}) collective-permute-start(bf16[4,2048]{1,0:T(4,128)(2,1)S(1)} %multiply_convert_fusion.1), channel_id=1, source_target_pairs={{0,2},{1,3},{2,0},{3,1},{4,6},{5,7},{6,4},{7,5},{8,10},{9,11},{10,... | collective-permute-start | bytes 49160 | tf_op jit(solution)/shard_map/ppermute | solution.py:81
  64.6 0.6 collective-permute-start.17
  65.2 2.1 %collective-permute-done.16 = bf16[4,2048]{1,0:T(4,128)(2,1)S(1)} collective-permute-done((bf16[4,2048]{1,0:T(4,128)(2,1)S(1)}, bf16[4,2048]{1,0:T(4,128)(2,1)S(1)}, u32[]{:S(2)}, u32[]{:S(2)}) %collective-permute-start.16) | collective-permute-done | bytes 16416 | tf_op jit(solution)/shard_map/ppermute | solution.py:81
  67.2 0.5 collective-permute-done.17
  67.9 2.8 %fusion.33 = bf16[16,1024]{1,0:T(8,128)(2,1)S(1)} fusion(bf16[2,2048,1024]{2,1,0:T(8,128)(2,1)} %param.24, bf16[4,2048]{1,0:T(4,128)(2,1)S(1)} %get-tuple-element.51, bf16[4,2048]{1,0:T(4,128)(2,1)S(1)} %get-tuple-element.52, bf16[4,2048]{1,0:T(4,128)(2,1)S(1)} %get-tuple-element.53, bf16[4,2048]{1,0:T(4,128)(2,1)S(1)} %get-tuple-element.50), kind=kOutput, calls=%fused_computation.33 | convolution fusion | flops 67387392 | bytes 4292608 | tf_op jit(solution)/shard_map/dot_general | solution.py:195
  70.7 0.6 collective-permute-start.18
  71.4 2.0 %collective-permute-start.19 = (bf16[4,1024]{1,0:T(4,128)(2,1)S(1)}, bf16[4,1024]{1,0:T(4,128)(2,1)S(1)}, u32[]{:S(2)}, u32[]{:S(2)}) collective-permute-start(bf16[4,1024]{1,0:T(4,128)(2,1)S(1)} %get-tuple-element.64), channel_id=1, source_target_pairs={{0,8},{4,12},{8,0},{12,4},{1,9},{5,13},{9,1},{13,5},{2,10},{6,14},... | collective-permute-start | bytes 24584 | tf_op jit(solution)/shard_map/ppermute | solution.py:81
  73.3 1.9 %collective-permute-start.20 = (bf16[4,1024]{1,0:T(4,128)(2,1)S(1)}, bf16[4,1024]{1,0:T(4,128)(2,1)S(1)}, u32[]{:S(2)}, u32[]{:S(2)}) collective-permute-start(bf16[4,1024]{1,0:T(4,128)(2,1)S(1)} %get-tuple-element.63), channel_id=1, source_target_pairs={{0,12},{4,8},{8,4},{12,0},{1,13},{5,9},{9,5},{13,1},{2,14},{6,10},... | collective-permute-start | bytes 24584 | tf_op jit(solution)/shard_map/ppermute | solution.py:81
  75.2 0.8 copy.95
  76.0 2.8 %collective-permute-done.20 = bf16[4,1024]{1,0:T(4,128)(2,1)S(1)} collective-permute-done((bf16[4,1024]{1,0:T(4,128)(2,1)S(1)}, bf16[4,1024]{1,0:T(4,128)(2,1)S(1)}, u32[]{:S(2)}, u32[]{:S(2)}) %collective-permute-start.20) | collective-permute-done | bytes 8224 | tf_op jit(solution)/shard_map/ppermute | solution.py:81
  78.8 0.6 fusion.154
  (98 shorter events, 4.5 us)
Async XLA Ops:
  0.6 15.3 %collective-permute-start = (bf16[4,1024]{1,0:T(4,128)(2,1)}, bf16[4,1024]{1,0:T(4,128)(2,1)}, u32[]{:S(2)}, u32[]{:S(2)}) collective-permute-start(bf16[4,1024]{1,0:T(4,128)(2,1)} %bitcast.424), channel_id=1, source_target_pairs={{0,4},{4,0},{8,12},{12,8},{1,5},{5,1},{9,13},{13,9},{2,6},{6,2},{1... | collective-permute-start | bytes 24584 | tf_op jit(solution)/shard_map/ppermute | solution.py:81
  3.7 12.2 %collective-permute-start.1 = (bf16[4,1024]{1,0:T(4,128)(2,1)}, bf16[4,1024]{1,0:T(4,128)(2,1)}, u32[]{:S(2)}, u32[]{:S(2)}) collective-permute-start(bf16[4,1024]{1,0:T(4,128)(2,1)} %bitcast.425), channel_id=1, source_target_pairs={{0,8},{4,12},{8,0},{12,4},{1,9},{5,13},{9,1},{13,5},{2,10},{6,14},... | collective-permute-start | bytes 24584 | tf_op jit(solution)/shard_map/ppermute | solution.py:81
  6.3 9.6 %collective-permute-start.2 = (bf16[4,1024]{1,0:T(4,128)(2,1)}, bf16[4,1024]{1,0:T(4,128)(2,1)}, u32[]{:S(2)}, u32[]{:S(2)}) collective-permute-start(bf16[4,1024]{1,0:T(4,128)(2,1)} %bitcast.426), channel_id=1, source_target_pairs={{0,12},{4,8},{8,4},{12,0},{1,13},{5,9},{9,5},{13,1},{2,14},{6,10},... | collective-permute-start | bytes 24584 | tf_op jit(solution)/shard_map/ppermute | solution.py:81
  8.5 4.1 %copy-start.5 = (f32[128]{0:T(128)}, f32[128]{0:T(128)S(1)}, u32[]{:S(2)}) copy-start(f32[128]{0:T(128)S(1)} %get-tuple-element.73) | copy-start | bytes 1540
  11.8 17.8 %copy-start = (f32[2,128,64]{1,2,0:T(8,128)S(1)}, f32[2,128,64]{1,2,0:T(8,128)}, u32[]{:S(2)}) copy-start(f32[2,128,64]{1,2,0:T(8,128)} %param.18) | copy-start | bytes 196612
  11.8 17.8 %copy-start.1 = (f32[2,128,64]{1,2,0:T(8,128)S(1)}, f32[2,128,64]{1,2,0:T(8,128)}, u32[]{:S(2)}) copy-start(f32[2,128,64]{1,2,0:T(8,128)} %param.19) | copy-start | bytes 196612
  12.6 2.3 %copy-start.7 = (f32[4,4]{1,0:T(4,128)}, f32[4,4]{1,0:T(4,128)S(1)}, u32[]{:S(2)}) copy-start(f32[4,4]{1,0:T(4,128)S(1)} %fusion.155) | copy-start | bytes 196
  15.2 14.3 %copy-start.6 = (f32[128]{0:T(128)S(1)}, f32[128]{0:T(128)}, u32[]{:S(2)}) copy-start(f32[128]{0:T(128)} %copy-done.5) | copy-start | bytes 1540
  17.0 15.3 %copy-start.4 = (f32[1,2048]{1,0:T(1,128)S(1)}, f32[1,2048]{1,0:T(1,128)}, u32[]{:S(2)}) copy-start(f32[1,2048]{1,0:T(1,128)} %get-tuple-element.70) | copy-start | bytes 24580
  19.9 25.1 %copy-start.3 = (f32[128,64]{0,1:T(8,128)S(1)}, f32[128,64]{0,1:T(8,128)}, u32[]{:S(2)}) copy-start(f32[128,64]{0,1:T(8,128)} %get-tuple-element.49) | copy-start | bytes 98308
  19.9 25.2 %copy-start.2 = (f32[128,64]{0,1:T(8,128)S(1)}, f32[128,64]{0,1:T(8,128)}, u32[]{:S(2)}) copy-start(f32[128,64]{0,1:T(8,128)} %get-tuple-element.48) | copy-start | bytes 98308
  22.8 5.3 %collective-permute-start.3 = (bf16[4,4224]{1,0:T(4,128)(2,1)S(1)}, bf16[4,4224]{1,0:T(4,128)(2,1)S(1)}, u32[]{:S(2)}, u32[]{:S(2)}) collective-permute-start(bf16[4,4224]{1,0:T(4,128)(2,1)S(1)} %get-tuple-element.39), channel_id=1, source_target_pairs={{0,1},{1,0},{2,3},{3,2},{4,5},{5,4},{6,7},{7,6},{8,9},{9,8},{10,11... | collective-permute-start | bytes 101384 | tf_op jit(solution)/shard_map/ppermute | solution.py:81
  22.9 5.2 %collective-permute-start.4 = (bf16[4,4224]{1,0:T(4,128)(2,1)S(1)}, bf16[4,4224]{1,0:T(4,128)(2,1)S(1)}, u32[]{:S(2)}, u32[]{:S(2)}) collective-permute-start(bf16[4,4224]{1,0:T(4,128)(2,1)S(1)} %get-tuple-element.41), channel_id=1, source_target_pairs={{0,2},{1,3},{2,0},{3,1},{4,6},{5,7},{6,4},{7,5},{8,10},{9,11},{10,... | collective-permute-start | bytes 101384 | tf_op jit(solution)/shard_map/ppermute | solution.py:81
  24.7 3.4 %collective-permute-start.5 = (bf16[4,4224]{1,0:T(4,128)(2,1)S(1)}, bf16[4,4224]{1,0:T(4,128)(2,1)S(1)}, u32[]{:S(2)}, u32[]{:S(2)}) collective-permute-start(bf16[4,4224]{1,0:T(4,128)(2,1)S(1)} %get-tuple-element.40), channel_id=1, source_target_pairs={{0,3},{1,2},{2,1},{3,0},{4,7},{5,6},{6,5},{7,4},{8,11},{9,10},{10,... | collective-permute-start | bytes 101384 | tf_op jit(solution)/shard_map/ppermute | solution.py:81
  32.4 2.2 %collective-permute-start.6 = (bf16[4,2048]{1,0:T(4,128)(2,1)S(1)}, bf16[4,2048]{1,0:T(4,128)(2,1)S(1)}, u32[]{:S(2)}, u32[]{:S(2)}) collective-permute-start(bf16[4,2048]{1,0:T(4,128)(2,1)S(1)} %multiply_convert_fusion.2), channel_id=1, source_target_pairs={{0,1},{1,0},{2,3},{3,2},{4,5},{5,4},{6,7},{7,6},{8,9},{9,8},{10,11... | collective-permute-start | bytes 49160 | tf_op jit(solution)/shard_map/ppermute | solution.py:81
  32.8 3.7 %collective-permute-start.7 = (bf16[4,2048]{1,0:T(4,128)(2,1)S(1)}, bf16[4,2048]{1,0:T(4,128)(2,1)S(1)}, u32[]{:S(2)}, u32[]{:S(2)}) collective-permute-start(bf16[4,2048]{1,0:T(4,128)(2,1)S(1)} %multiply_convert_fusion.2), channel_id=1, source_target_pairs={{0,2},{1,3},{2,0},{3,1},{4,6},{5,7},{6,4},{7,5},{8,10},{9,11},{10,... | collective-permute-start | bytes 49160 | tf_op jit(solution)/shard_map/ppermute | solution.py:81
  34.5 3.3 %collective-permute-start.8 = (bf16[4,2048]{1,0:T(4,128)(2,1)S(1)}, bf16[4,2048]{1,0:T(4,128)(2,1)S(1)}, u32[]{:S(2)}, u32[]{:S(2)}) collective-permute-start(bf16[4,2048]{1,0:T(4,128)(2,1)S(1)} %multiply_convert_fusion.2), channel_id=1, source_target_pairs={{0,3},{1,2},{2,1},{3,0},{4,7},{5,6},{6,5},{7,4},{8,11},{9,10},{10,... | collective-permute-start | bytes 49160 | tf_op jit(solution)/shard_map/ppermute | solution.py:81
  40.8 5.5 %collective-permute-start.10 = (bf16[16,1024]{1,0:T(8,128)(2,1)S(1)}, bf16[16,1024]{1,0:T(8,128)(2,1)S(1)}, u32[]{:S(2)}, u32[]{:S(2)}) collective-permute-start(bf16[16,1024]{1,0:T(8,128)(2,1)S(1)} %fusion.30), channel_id=1, source_target_pairs={{0,8},{4,12},{8,0},{12,4},{1,9},{5,13},{9,1},{13,5},{2,10},{6,14},... | collective-permute-start | bytes 98312 | tf_op jit(solution)/shard_map/ppermute | solution.py:81
  42.5 5.9 %collective-permute-start.11 = (bf16[16,1024]{1,0:T(8,128)(2,1)S(1)}, bf16[16,1024]{1,0:T(8,128)(2,1)S(1)}, u32[]{:S(2)}, u32[]{:S(2)}) collective-permute-start(bf16[16,1024]{1,0:T(8,128)(2,1)S(1)} %fusion.30), channel_id=1, source_target_pairs={{0,12},{4,8},{8,4},{12,0},{1,13},{5,9},{9,5},{13,1},{2,14},{6,10},... | collective-permute-start | bytes 98312 | tf_op jit(solution)/shard_map/ppermute | solution.py:81
  44.4 4.1 %collective-permute-start.9 = (bf16[16,1024]{1,0:T(8,128)(2,1)S(1)}, bf16[16,1024]{1,0:T(8,128)(2,1)S(1)}, u32[]{:S(2)}, u32[]{:S(2)}) collective-permute-start(bf16[16,1024]{1,0:T(8,128)(2,1)S(1)} %fusion.30), channel_id=1, source_target_pairs={{0,4},{4,0},{8,12},{12,8},{1,5},{5,1},{9,13},{13,9},{2,6},{6,2},{1... | collective-permute-start | bytes 98312 | tf_op jit(solution)/shard_map/ppermute | solution.py:81
  54.6 2.4 %collective-permute-start.12 = (bf16[4,4224]{1,0:T(4,128)(2,1)S(1)}, bf16[4,4224]{1,0:T(4,128)(2,1)S(1)}, u32[]{:S(2)}, u32[]{:S(2)}) collective-permute-start(bf16[4,4224]{1,0:T(4,128)(2,1)S(1)} %get-tuple-element.36), channel_id=1, source_target_pairs={{0,1},{1,0},{2,3},{3,2},{4,5},{5,4},{6,7},{7,6},{8,9},{9,8},{10,11... | collective-permute-start | bytes 101384 | tf_op jit(solution)/shard_map/ppermute | solution.py:81
  54.7 4.3 %collective-permute-start.13 = (bf16[4,4224]{1,0:T(4,128)(2,1)S(1)}, bf16[4,4224]{1,0:T(4,128)(2,1)S(1)}, u32[]{:S(2)}, u32[]{:S(2)}) collective-permute-start(bf16[4,4224]{1,0:T(4,128)(2,1)S(1)} %get-tuple-element.38), channel_id=1, source_target_pairs={{0,2},{1,3},{2,0},{3,1},{4,6},{5,7},{6,4},{7,5},{8,10},{9,11},{10,... | collective-permute-start | bytes 101384 | tf_op jit(solution)/shard_map/ppermute | solution.py:81
  55.3 3.7 %collective-permute-start.14 = (bf16[4,4224]{1,0:T(4,128)(2,1)S(1)}, bf16[4,4224]{1,0:T(4,128)(2,1)S(1)}, u32[]{:S(2)}, u32[]{:S(2)}) collective-permute-start(bf16[4,4224]{1,0:T(4,128)(2,1)S(1)} %get-tuple-element.37), channel_id=1, source_target_pairs={{0,3},{1,2},{2,1},{3,0},{4,7},{5,6},{6,5},{7,4},{8,11},{9,10},{10,... | collective-permute-start | bytes 101384 | tf_op jit(solution)/shard_map/ppermute | solution.py:81
  63.3 1.9 %collective-permute-start.15 = (bf16[4,2048]{1,0:T(4,128)(2,1)S(1)}, bf16[4,2048]{1,0:T(4,128)(2,1)S(1)}, u32[]{:S(2)}, u32[]{:S(2)}) collective-permute-start(bf16[4,2048]{1,0:T(4,128)(2,1)S(1)} %multiply_convert_fusion.1), channel_id=1, source_target_pairs={{0,1},{1,0},{2,3},{3,2},{4,5},{5,4},{6,7},{7,6},{8,9},{9,8},{10,11... | collective-permute-start | bytes 49160 | tf_op jit(solution)/shard_map/ppermute | solution.py:81
  63.5 3.7 %collective-permute-start.16 = (bf16[4,2048]{1,0:T(4,128)(2,1)S(1)}, bf16[4,2048]{1,0:T(4,128)(2,1)S(1)}, u32[]{:S(2)}, u32[]{:S(2)}) collective-permute-start(bf16[4,2048]{1,0:T(4,128)(2,1)S(1)} %multiply_convert_fusion.1), channel_id=1, source_target_pairs={{0,2},{1,3},{2,0},{3,1},{4,6},{5,7},{6,4},{7,5},{8,10},{9,11},{10,... | collective-permute-start | bytes 49160 | tf_op jit(solution)/shard_map/ppermute | solution.py:81
  64.6 3.2 %collective-permute-start.17 = (bf16[4,2048]{1,0:T(4,128)(2,1)S(1)}, bf16[4,2048]{1,0:T(4,128)(2,1)S(1)}, u32[]{:S(2)}, u32[]{:S(2)}) collective-permute-start(bf16[4,2048]{1,0:T(4,128)(2,1)S(1)} %multiply_convert_fusion.1), channel_id=1, source_target_pairs={{0,3},{1,2},{2,1},{3,0},{4,7},{5,6},{6,5},{7,4},{8,11},{9,10},{10,... | collective-permute-start | bytes 49160 | tf_op jit(solution)/shard_map/ppermute | solution.py:81
  70.7 5.2 %collective-permute-start.18 = (bf16[4,1024]{1,0:T(4,128)(2,1)S(1)}, bf16[4,1024]{1,0:T(4,128)(2,1)S(1)}, u32[]{:S(2)}, u32[]{:S(2)}) collective-permute-start(bf16[4,1024]{1,0:T(4,128)(2,1)S(1)} %get-tuple-element.62), channel_id=1, source_target_pairs={{0,4},{4,0},{8,12},{12,8},{1,5},{5,1},{9,13},{13,9},{2,6},{6,2},{1... | collective-permute-start | bytes 24584 | tf_op jit(solution)/shard_map/ppermute | solution.py:81
  71.4 4.6 %collective-permute-start.19 = (bf16[4,1024]{1,0:T(4,128)(2,1)S(1)}, bf16[4,1024]{1,0:T(4,128)(2,1)S(1)}, u32[]{:S(2)}, u32[]{:S(2)}) collective-permute-start(bf16[4,1024]{1,0:T(4,128)(2,1)S(1)} %get-tuple-element.64), channel_id=1, source_target_pairs={{0,8},{4,12},{8,0},{12,4},{1,9},{5,13},{9,1},{13,5},{2,10},{6,14},... | collective-permute-start | bytes 24584 | tf_op jit(solution)/shard_map/ppermute | solution.py:81
  73.3 5.4 %collective-permute-start.20 = (bf16[4,1024]{1,0:T(4,128)(2,1)S(1)}, bf16[4,1024]{1,0:T(4,128)(2,1)S(1)}, u32[]{:S(2)}, u32[]{:S(2)}) collective-permute-start(bf16[4,1024]{1,0:T(4,128)(2,1)S(1)} %get-tuple-element.63), channel_id=1, source_target_pairs={{0,12},{4,8},{8,4},{12,0},{1,13},{5,9},{9,5},{13,1},{2,14},{6,10},... | collective-permute-start | bytes 24584 | tf_op jit(solution)/shard_map/ppermute | solution.py:81

commit v2 on v1

--- a/solution.py
+++ b/solution.py
@@ -1,6 +1,10 @@
+import functools
+
 import jax
 import jax.numpy as jnp
 from jax import lax
+from jax.experimental import pallas as pl
+from jax.experimental.pallas import tpu as pltpu
 from jax.sharding import PartitionSpec as P
 
 D = 4096
@@ -132,7 +136,7 @@
     return total[:, :width], total[:, width : 2 * width], own
 
 
-def body(
+def general_body(
     tokens,
     lengths,
     norm_gain,
@@ -218,6 +222,454 @@
     return (own_block, jnp.stack(states))
 
 
+LANES = 128
+COST = 4000000
+SUBLANES = 8
+VMEM = pl.BlockSpec(memory_space=pltpu.VMEM)
+HBM = pl.BlockSpec(memory_space=pltpu.MemorySpace.HBM)
+
+
+def vmem_call(kernel, outs, *operands, in_specs=None, scratch=(), limit=8 << 20, cost=0):
+    outs = [jax.ShapeDtypeStruct(shape, dtype) for shape, dtype in outs]
+    in_specs = in_specs or [VMEM] * len(operands)
+    operands = [
+        pltpu.with_memory_space_constraint(operand, pltpu.MemorySpace.HBM) if spec is HBM else operand
+        for spec, operand in zip(in_specs, operands)
+    ]
+    return pl.pallas_call(
+        kernel,
+        out_shape=outs,
+        in_specs=in_specs,
+        out_specs=[VMEM] * len(outs),
+        scratch_shapes=list(scratch),
+        compiler_params=pltpu.CompilerParams(vmem_limit_bytes=limit),
+        cost_estimate=pl.CostEstimate(flops=cost, bytes_accessed=0, transcendentals=0) if cost else None,
+    )(*operands)
+
+
+def twice(value):
+    return jnp.concatenate([value, value], axis=-1)
+
+
+def halves(value):
+    high = value.astype(jnp.bfloat16)
+    low = (value - high.astype(jnp.float32)).astype(jnp.bfloat16)
+    return high, low
+
+
+def group_mask(dtype=jnp.float32):
+    lane = lax.broadcasted_iota(jnp.int32, (SUBLANES, LANES), 1)
+    row = lax.broadcasted_iota(jnp.int32, (SUBLANES, LANES), 0)
+    return lane // S5_IN == row
+
+
+def start_copies(sources, targets, semaphores):
+    copies = [
+        pltpu.make_async_copy(source, target, semaphores.at[i])
+        for i, (source, target) in enumerate(zip(sources, targets))
+    ]
+    for copy in copies:
+        copy.start()
+    return copies
+
+
+def wait_copies(copies):
+    for copy in copies:
+        copy.wait()
+
+
+def parameter_step(decay, frequency, log_step, map_ref, real_ref, imag_ref, coupled_ref):
+    half, groups = decay.shape
+    step = jnp.exp(log_step)
+    magnitude = jnp.exp(-decay * step)
+    angle = frequency * step
+    real = magnitude * jnp.cos(angle)
+    imag = magnitude * jnp.sin(angle)
+    denominator = decay * decay + frequency * frequency
+    coeff_real = (imag * frequency - (real - 1.0) * decay) / denominator
+    coeff_imag = (-imag * decay - (real - 1.0) * frequency) / denominator
+
+    def across(first, second):
+        return jnp.transpose(jnp.concatenate([first, second], axis=0))
+
+    real_ref[...] = across(real, real)
+    imag_ref[...] = across(-imag, imag)
+    scale_real = across(coeff_real, coeff_real)
+    scale_imag = across(-coeff_imag, coeff_imag)
+    for chunk in range(groups // SUBLANES):
+        rows = slice(chunk * SUBLANES, (chunk + 1) * SUBLANES)
+        values = map_ref[rows].astype(jnp.float32).reshape(LANES, LANES)
+        spread = [
+            jnp.broadcast_to(s[rows][:, None, :], (SUBLANES, S5_IN, LANES)).reshape(LANES, LANES)
+            for s in (scale_real, scale_imag)
+        ]
+        coupled = spread[0] * values + spread[1] * pltpu.roll(values, half, 1)
+        high, low = halves(coupled)
+        coupled_ref[chunk, :LANES] = high
+        coupled_ref[chunk, LANES:] = low
+
+
+def prepare_kernel(layer, decay_hbm, frequency_hbm, log_step_hbm, map_hbm, *refs):
+    count = (len(refs) - 8) // 2
+    sources, targets = refs[:count], refs[count : 2 * count]
+    real_ref, imag_ref, coupled_ref = refs[2 * count : 2 * count + 3]
+    decay, frequency, log_step, maps, semaphores = refs[2 * count + 3 :]
+    small = start_copies(
+        [decay_hbm.at[layer], frequency_hbm.at[layer], log_step_hbm, map_hbm.at[layer]],
+        [decay, frequency, log_step, maps],
+        semaphores.at[pl.ds(0, 4)],
+    )
+    large = start_copies(
+        [source.at[layer] for source in sources], targets, semaphores.at[pl.ds(4, count)]
+    )
+    wait_copies(small)
+    parameter_step(
+        decay[...], frequency[...], log_step[layer : layer + 1], maps, real_ref, imag_ref, coupled_ref
+    )
+    wait_copies(large)
+
+
+def prepare(layer, decay, frequency, log_step, input_map, projections, after=()):
+    _, half, groups = decay.shape
+    f32, bf16 = jnp.float32, jnp.bfloat16
+    after = list(after)
+
+    def kernel(*refs):
+        prepare_kernel(layer, *refs[len(after) :])
+
+    return vmem_call(
+        kernel,
+        [(p.shape[1:], bf16) for p in projections]
+        + [((groups, LANES), f32)] * 2
+        + [((groups // SUBLANES, 2 * LANES, LANES), bf16)],
+        *after, decay, frequency, log_step, input_map, *projections,
+        in_specs=[VMEM] * len(after) + [HBM] * (4 + len(projections)),
+        scratch=[
+            pltpu.VMEM((half, groups), f32),
+            pltpu.VMEM((half, groups), f32),
+            pltpu.VMEM(log_step.shape, f32),
+            pltpu.VMEM(input_map.shape[1:], bf16),
+            pltpu.SemaphoreType.DMA((4 + len(projections),)),
+        ],
+        cost=COST,
+    )
+
+
+def small_kernel(steps, lengths_hbm, *refs):
+    count = (len(refs) - 3) // 2
+    sources, targets = refs[:count], refs[count : 2 * count]
+    live_ref, lengths, semaphores = refs[2 * count :]
+    copies = start_copies(
+        [lengths_hbm, *sources], [lengths, *targets], semaphores
+    )
+    copies[0].wait()
+    length = lengths[lax.axis_index("dp")]
+    place = lax.broadcasted_iota(jnp.int32, (steps * SUBLANES, LANES), 0) // SUBLANES
+    live_ref[...] = (place < length).astype(jnp.float32)
+    wait_copies(copies[1:])
+
+
+def bring_small(steps, lengths, *arrays):
+    return vmem_call(
+        functools.partial(small_kernel, steps),
+        [(a.shape, a.dtype) for a in arrays] + [((steps * SUBLANES, LANES), jnp.float32)],
+        lengths, *arrays,
+        in_specs=[HBM] * (1 + len(arrays)),
+        scratch=[
+            pltpu.SMEM(lengths.shape, jnp.int32),
+            pltpu.SemaphoreType.DMA((1 + len(arrays),)),
+        ],
+        cost=COST,
+    )
+
+
+def bring_all_kernel(count, after, *refs):
+    wait_copies(start_copies(refs[:count], refs[count : 2 * count], refs[-1]))
+
+
+def bring_both(arrays, after):
+    return vmem_call(
+        functools.partial(bring_all_kernel, len(arrays)),
+        [(a.shape, a.dtype) for a in arrays],
+        after, *arrays,
+        in_specs=[VMEM] + [HBM] * len(arrays),
+        scratch=[pltpu.SemaphoreType.DMA((len(arrays),))],
+        cost=COST,
+    )
+
+
+def swaps(values, axis, size):
+    received = {}
+    for k in reversed(range(1, size)):
+        with jax.named_scope(f"k{k}"):
+            value = values[k] if isinstance(values, (list, tuple)) else values
+            received[k] = swap(value, axis, k, size)
+    return [received[k] for k in range(1, size)]
+
+
+def bring_kernel(layer, source, after, target, semaphores):
+    wait_copies(start_copies([source.at[layer]], [target], semaphores))
+
+
+def bring(layer, source, after):
+    return vmem_call(
+        functools.partial(bring_kernel, layer),
+        [(source.shape[1:], source.dtype)],
+        source, after,
+        in_specs=[HBM, VMEM],
+        scratch=[pltpu.SemaphoreType.DMA((1,))],
+        cost=COST,
+    )[0]
+
+
+def project(layer, rows, gain_ref, drive_weight_ref, gate_weight_ref, message_refs):
+    count = rows.shape[0] // len(message_refs)
+    width = drive_weight_ref.shape[1]
+    scaled = (rows * gain_ref[layer : layer + 1]).astype(jnp.bfloat16)
+    squares = jnp.sum(rows * rows, axis=1, keepdims=True)
+    lane = lax.broadcasted_iota(jnp.int32, (rows.shape[0], LANES), 1)
+    extra = jnp.zeros((rows.shape[0], LANES), jnp.float32)
+    for place in range(3):
+        piece = squares.astype(jnp.bfloat16).astype(jnp.float32)
+        extra = jnp.where(lane == place, piece, extra)
+        squares = squares - piece
+    step = min(width, 512)
+    parts = [(2 * width, LANES, extra)]
+    for base, weight_ref in ((0, drive_weight_ref), (width, gate_weight_ref)):
+        for at in range(0, width, step):
+            value = jnp.dot(
+                scaled, weight_ref[:, at : at + step], preferred_element_type=jnp.float32
+            )
+            parts.append((base + at, step, value))
+    for at, size, value in parts:
+        for k, message_ref in enumerate(message_refs):
+            block = value[k * count : (k + 1) * count]
+            message_ref[:, at : at + size] = block.astype(jnp.bfloat16)
+
+
+def pick(blocks, offset):
+    bit = 1
+    while bit < len(blocks):
+        on = (offset & bit) != 0
+        blocks = [jnp.where(on, blocks[k ^ bit], blocks[k]) for k in range(len(blocks))]
+        bit *= 2
+    return blocks
+
+
+def own_offset():
+    return lax.axis_index("dp") ^ lax.axis_index("tp")
+
+
+def first_kernel(size, *refs):
+    block_refs, (gain_ref, drive_ref, gate_ref) = refs[:size], refs[size : size + 3]
+    message_refs, rows_ref = refs[size + 3 : -1], refs[-1]
+    blocks = [ref[...].astype(jnp.float32).reshape(ref.shape[-2:]) for ref in block_refs]
+    rows = jnp.concatenate(pick(blocks, own_offset()), axis=0)
+    rows_ref[...] = rows
+    project(0, rows, gain_ref, drive_ref, gate_ref, message_refs)
+
+
+def next_kernel(size, layer, base_ref, *refs):
+    part_refs, (gain_ref, drive_ref, gate_ref) = refs[:size], refs[size : size + 3]
+    message_refs, rows_ref = refs[size + 3 : -1], refs[-1]
+    rows = base_ref[...]
+    rows = rows + sum(ref[...].astype(jnp.float32) for ref in part_refs)
+    rows = rows.astype(jnp.bfloat16).astype(jnp.float32)
+    rows_ref[...] = rows
+    project(layer, rows, gain_ref, drive_ref, gate_ref, message_refs)
+
+
+def state_kernel(size, layer, features, *refs):
+    message_refs = refs[:size]
+    live_ref, real_ref, imag_ref, coupled_ref, readout_ref, skip_ref, state_ref = refs[size:-2]
+    branch_ref, next_ref = refs[-2:]
+    steps = message_refs[0].shape[0]
+    width = branch_ref.shape[1]
+    half = LANES // 2
+    total = sum(ref[...].astype(jnp.float32) for ref in message_refs)
+    squares = jnp.sum(total[:, 2 * width :], axis=1, keepdims=True)
+    inverse = lax.rsqrt(squares / features + epsilon)
+    drive = (inverse * total[:, :width]).astype(jnp.bfloat16).astype(jnp.float32)
+    gate = (inverse * total[:, width : 2 * width]).astype(jnp.bfloat16).astype(jnp.float32)
+    live = live_ref[...]
+    lane = lax.broadcasted_iota(jnp.int32, (SUBLANES, LANES), 1)
+    row = lax.broadcasted_iota(jnp.int32, (SUBLANES, LANES), 0)
+    own_group = group_mask()
+    keeps = [live[t * SUBLANES : (t + 1) * SUBLANES] > 0.5 for t in range(steps)]
+    live_rows = jnp.concatenate(
+        [live[t * SUBLANES : t * SUBLANES + 1] for t in range(steps)], axis=0
+    )
+    sign = jnp.where(lane < half, 1.0, -1.0)
+    for chunk in range(width // LANES):
+        at = slice(chunk * LANES, (chunk + 1) * LANES)
+        groups = slice(chunk * SUBLANES, (chunk + 1) * SUBLANES)
+        fed = jnp.concatenate(
+            [
+                jnp.where(own_group, jnp.broadcast_to(drive[t : t + 1, at], (SUBLANES, LANES)), 0.0)
+                for t in range(steps)
+            ],
+            axis=0,
+        ).astype(jnp.bfloat16)
+        pushed = jnp.dot(twice(fed), coupled_ref[chunk], preferred_element_type=jnp.float32)
+        turned = pltpu.roll(pushed, half, 1)
+        real, imag = real_ref[groups], imag_ref[groups]
+        value = state_ref[layer, 0, groups]
+        other = pltpu.roll(value, half, 1)
+        history = []
+        for t in range(steps):
+            now = slice(t * SUBLANES, (t + 1) * SUBLANES)
+            new_value = real * value + imag * other + pushed[now]
+            new_other = real * other - imag * value + turned[now]
+            value = jnp.where(keeps[t], new_value, value)
+            other = jnp.where(keeps[t], new_other, other)
+            history.append(value * sign)
+        next_ref[groups] = value
+        high, low = halves(jnp.concatenate(history, axis=0))
+        seen = lax.dot_general(
+            jnp.concatenate([high, low], axis=0),
+            readout_ref[chunk],
+            (((1,), (1,)), ((), ())),
+            preferred_element_type=jnp.float32,
+        )
+        count = steps * SUBLANES
+        seen = seen[:count] + seen[count:]
+        read = jnp.concatenate(
+            [
+                jnp.sum(
+                    jnp.where(own_group, seen[t * SUBLANES : (t + 1) * SUBLANES], 0.0),
+                    axis=0,
+                    keepdims=True,
+                )
+                for t in range(steps)
+            ],
+            axis=0,
+        )
+        response = read + skip_ref[layer : layer + 1, at].astype(jnp.float32) * drive[:, at]
+        value = jax.nn.gelu(response) * jax.nn.silu(gate[:, at]) * live_rows
+        branch_ref[:, at] = value.astype(jnp.bfloat16)
+
+
+def output_kernel(size, *refs):
+    branch_refs, weight_ref, out_ref = refs[:size], refs[size], refs[size + 1]
+    rows = jnp.concatenate([ref[...].astype(jnp.float32) for ref in branch_refs], axis=0)
+    out_ref[...] = jnp.dot(
+        rows.astype(jnp.bfloat16), weight_ref[...], preferred_element_type=jnp.float32
+    ).astype(jnp.bfloat16)
+
+
+def last_output_kernel(size, *refs):
+    branch_refs, weight_ref, base_ref = refs[:size], refs[size], refs[size + 1]
+    out_refs = refs[size + 2 :]
+    rows = jnp.concatenate([ref[...].astype(jnp.float32) for ref in branch_refs], axis=0)
+    value = jnp.dot(rows.astype(jnp.bfloat16), weight_ref[...], preferred_element_type=jnp.float32)
+    count = rows.shape[0] // size
+    blocks = [value[k * count : (k + 1) * count] for k in range(size)]
+    offset = own_offset()
+    blocks = pick(blocks, offset)
+    base = base_ref[...]
+    bases = pick([base[k * count : (k + 1) * count] for k in range(size)], offset)
+    out_refs[0][...] = bases[0] + blocks[0]
+    for out_ref, block in zip(out_refs[1:], blocks[1:]):
+        out_ref[...] = block.astype(jnp.bfloat16)
+
+
+def final_kernel(own_ref, *refs):
+    total = own_ref[...] + sum(ref[...].astype(jnp.float32) for ref in refs[:-1])
+    refs[-1][0] = total.astype(jnp.bfloat16)
+
+
+def fits(tokens, lengths, state, map_rows, dp_size, tp_size):
+    whole_groups = state.shape[2] % LANES == 0 and state.shape[3] == LANES
+    one_each = tokens.shape[0] == 1 and state.shape[1] == 1
+    equal = dp_size == tp_size == lengths.shape[0]
+    return direct(dp_size) and equal and one_each and whole_groups and map_rows == S5_IN
+
+
+def direct_body(
+    tokens,
+    lengths,
+    norm_gain,
+    input_weight,
+    gate_weight,
+    decay_rate,
+    frequency,
+    log_step,
+    input_map,
+    readout_map,
+    skip_weight,
+    out_weight,
+    state,
+):
+    size = lax.axis_size("dp")
+    _, steps, features = tokens.shape
+    inner = input_weight.shape[2]
+    groups = state.shape[2]
+    chunks = groups // SUBLANES
+    count = size * steps
+    bf16, f32 = jnp.bfloat16, jnp.float32
+    message = [((steps, 2 * inner + LANES), bf16)] * size
+    rows_shape = ((count, features), f32)
+    projections = (input_weight, gate_weight)
+    decay, frequency = (jnp.swapaxes(value, 1, 2) for value in (decay_rate, frequency))
+    raw = (decay, frequency, log_step, input_map, projections)
+    own = tokens.reshape(steps, features)
+    with jax.named_scope("a"):
+        pieces = swaps(own, "tp", size)
+        own, gain, live = bring_small(steps, lengths, own, norm_gain)
+        pieces = [own] + pieces
+        *weights, real, imag, coupled = prepare(0, *raw)
+    states = []
+    for layer in range(LAYERS):
+        if layer == 0:
+            kernel, base = functools.partial(first_kernel, size), []
+        else:
+            kernel, base = functools.partial(next_kernel, size, layer), [rows]
+        results = vmem_call(kernel, message + [rows_shape], *base, *pieces, gain, *weights)
+        messages, rows = results[:size], results[size]
+        with jax.named_scope(f"b{layer}"):
+            arrived = [messages[0]] + swaps(messages, "dp", size)
+            out_now = bring(layer, out_weight, messages[0])
+            readout = bring(layer, readout_map, messages[0])
+            if layer == 0:
+                state_now, skip = bring_both((state, skip_weight), messages[0])
+        branch, next_state = vmem_call(
+            functools.partial(state_kernel, size, layer, D),
+            [((steps, inner), bf16), ((groups, LANES), f32)],
+            *arrived, live, real, imag, coupled,
+            readout.reshape(chunks, LANES, LANES), skip, state_now,
+        )
+        states.append(next_state)
+        with jax.named_scope(f"c{layer}"):
+            branches = [branch] + swaps(branch, "dp", size)
+        if layer < LAYERS - 1:
+            (part,) = vmem_call(
+                functools.partial(output_kernel, size),
+                [((count, features), bf16)],
+                *branches, out_now,
+            )
+            with jax.named_scope(f"d{layer}"):
+                pieces = [part] + swaps(part, "tp", size)
+                *weights, real, imag, coupled = prepare(layer + 1, *raw, after=[part])
+            continue
+        parts = vmem_call(
+            functools.partial(last_output_kernel, size),
+            [((steps, features), f32)] + [((steps, features), bf16)] * (size - 1),
+            *branches, out_now, rows,
+        )
+        with jax.named_scope(f"d{layer}"):
+            arrived = swaps(parts, "tp", size)
+        (mixed,) = vmem_call(final_kernel, [((1, steps, features), bf16)], parts[0], *arrived)
+    return mixed, jnp.stack(states)[:, None]
+
+
+def body(*arguments):
+    tokens, lengths, input_map, state = (arguments[i] for i in (0, 1, 8, 12))
+    sizes = lax.axis_size("dp"), lax.axis_size("tp")
+    if fits(tokens, lengths, state, input_map.shape[2], *sizes):
+        return direct_body(*arguments)
+    return general_body(*arguments)
+
+
 def solution(mesh):
     return jax.shard_map(
         body,

time: 80.2 us -> 56.1 us (0.70)
  Pallas kernels: 0 us -> 23.9 us
  matrix products: 22.8 us -> 0 us
  local copies, waits for them, and re-layouts: 8.72 us -> 0 us
  other arithmetic: 7.85 us -> 0.66 us
  waiting for transfers between devices: 14.1 us -> 8.16 us
  between operations: 3.73 us -> 0.79 us
    pallas_call x0 -> x15, Pallas kernels: none -> 23.9 us  [vmem_call(): pl.pallas_call(kernel, out_shape=outs, in_specs=in_specs, out_specs=[VMEM...]
    dot_general x10 -> x0, matrix products: 22.8 us -> none  [the longest x2 5.71 us: body(): jnp.dot(scaled, gate_weight[layer_index], preferred_element_type=jnp.floa...]
    ppermute x21, waiting for transfers between devices: 14.1 us -> 8.16 us  [swap(): return lax.ppermute(value, axis, [(i, i ^ distance) for i in range(size)])]
    slice x3 -> x0, local copies, waits for them, and re-layouts: 2.9 us -> none  [the longest x1 1.36 us: body(): scaled = (flattened * norm_gain[layer_index][None, :]).astype(jnp.bfloat16)]
    convert_element_type x8 -> x0, other arithmetic: 2.57 us -> none  [the longest x1 1.39 us: advance_state(): skip_row.astype(jnp.float32)]
    div x1 -> x0, other arithmetic: 1.72 us -> none  [advance_state(): (-(decay_real - 1.0) * decay_rate + decay_imag * frequency) / denominator]
    squeeze x4 -> x0, local copies, waits for them, and re-layouts: 1.48 us -> none  [the longest x1 1.39 us: body(): input_map[layer_index]]
    another operation x14 -> x0, other arithmetic: 1.02 us -> none  [the longest x3 0.89 us: gather_rows(): jnp.stack([block] + [swap(block, axis, k, size) for k in range(1, size)])]
  transfers between devices with their start and end apart: 21 -> 21, of which waited for: 9 -> 9; matrix products, arithmetic and copies ran while one was open for 15% -> 1% of each run, Pallas kernels for 0% -> 28%
where the time goes in v2:
time: 56.1 us; the launch traced here: 55.8 us
  Pallas kernels  23.9 us (43%)
  starting transfers between devices  22.2 us (40%)
  waiting for transfers between devices  8.16 us (15%)
  between operations  0.79 us (1%)
  other arithmetic  0.66 us (1%)
    pallas_call x15, Pallas kernels, vmem_call(): pl.pallas_call(kernel, out_shape=outs, in_specs=in_specs, out_specs=[VMEM...  23.9 us
    ppermute x21, starting transfers between devices, swap(): return lax.ppermute(value, axis, [(i, i ^ distance) for i in range(size)])  22.2 us
    ppermute x21, waiting for transfers between devices, swap(): return lax.ppermute(value, axis, [(i, i ^ distance) for i in range(size)])  8.16 us
  transfers between devices with their start and end apart: 21, of which 9 were waited for; matrix products, arithmetic and copies ran while one was open for 1% of the time, Pallas kernels for 28%

profile of v2, /device:TPU:0, one launch (start us, length us, event | category | flops | bytes accessed | tf_op | source)
XLA Modules:
  0.0 55.8 jit_solution(14872238672996736281)
XLA Ops:
  0.6 5.1 %collective-permute-start.2 = (bf16[4,1024]{1,0:T(4,128)(2,1)}, bf16[4,1024]{1,0:T(4,128)(2,1)S(1)}, u32[]{:S(2)}, u32[]{:S(2)}) collective-permute-start(bf16[4,1024]{1,0:T(4,128)(2,1)} %bitcast.19), channel_id=1, source_target_pairs={{0,12},{4,8},{8,4},{12,0},{1,13},{5,9},{9,5},{13,1},{2,14},{6,10},... | collective-permute-start | bytes 24584 | tf_op jit(solution)/shard_map/a/k3/ppermute | solution.py:85
  5.8 0.6 %collective-permute-start = (bf16[4,1024]{1,0:T(4,128)(2,1)}, bf16[4,1024]{1,0:T(4,128)(2,1)S(1)}, u32[]{:S(2)}, u32[]{:S(2)}) collective-permute-start(bf16[4,1024]{1,0:T(4,128)(2,1)} %bitcast.21), channel_id=1, source_target_pairs={{0,4},{4,0},{8,12},{12,8},{1,5},{5,1},{9,13},{13,9},{2,6},{6,2},{1... | collective-permute-start | bytes 24584 | tf_op jit(solution)/shard_map/a/k1/ppermute | solution.py:85
  6.4 0.8 %a.2 = (bf16[4,1024]{1,0:T(4,128)(2,1)S(1)}, f32[2,1024]{1,0:T(2,128)S(1)}, f32[32,128]{1,0:T(8,128)S(1)}) custom-call(s32[4]{0:T(128)} %lengths_hbm.1, bf16[4,1024]{1,0:T(4,128)(2,1)} %bitcast.22, f32[2,1024]{1,0:T(2,128)} %refs_1_.2), custom_call_target="tpu_custom_call" | custom-call | flops 4000000 | tf_op jit(solution)/shard_map/a/pallas_call | solution.py:239
  7.2 3.7 %a.3 = (bf16[1024,2048]{1,0:T(8,128)(2,1)S(1)}, bf16[1024,2048]{1,0:T(8,128)(2,1)S(1)}, f32[128,128]{1,0:T(8,128)S(1)}, f32[128,128]{1,0:T(8,128)S(1)}, bf16[16,256,128]{2,1,0:T(8,128)(2,1)S(1)}) custom-call(f32[2,64,128]{2,1,0:T(8,128)} %bitcast.15, f32[2,64,128]{2,1,0:T(8,128)} %bitcast.17, f32[2,128]{1,0:T(2,128)} %refs_3_.3, ...), custom_call_target="tpu_custom_call" | custom-call | flops 4000000 | tf_op jit(solution)/shard_map/a/pallas_call | solution.py:239
  10.9 0.0 collective-permute-done.1.refs_2_
  10.9 0.0 collective-permute-done.refs_1_
  11.0 1.2 %shard_map.140 = (bf16[4,4224]{1,0:T(4,128)(2,1)S(1)}, bf16[4,4224]{1,0:T(4,128)(2,1)S(1)}, bf16[4,4224]{1,0:T(4,128)(2,1)S(1)}, bf16[4,4224]{1,0:T(4,128)(2,1)S(1)}, f32[16,1024]{1,0:T(8,128)S(1)}) custom-call(bf16[4,1024]{1,0:T(4,128)(2,1)S(1)} %get-tuple-element.35.refs_0_, bf16[4,1024]{1,0:T(4,128)(2,1)S(1)} %collective-permute-done.refs_1_, ...), custom_call_target="tpu_custom_call" | custom-call | tf_op jit(solution)/shard_map/pallas_call | solution.py:239
  12.2 0.0 collective-permute-start.3
  12.2 1.7 %collective-permute-start.4 = (bf16[4,4224]{1,0:T(4,128)(2,1)S(1)}, bf16[4,4224]{1,0:T(4,128)(2,1)S(1)}, u32[]{:S(2)}, u32[]{:S(2)}) collective-permute-start(bf16[4,4224]{1,0:T(4,128)(2,1)S(1)} %get-tuple-element.42), channel_id=1, source_target_pairs={{0,2},{1,3},{2,0},{3,1},{4,6},{5,7},{6,4},{7,5},{8,10},{9,11},{10,... | collective-permute-start | bytes 101384 | tf_op jit(solution)/shard_map/b0/k2/ppermute | solution.py:85
  13.9 0.1 collective-permute-start.5
  14.0 1.0 %b0.3 = bf16[128,16,128]{2,1,0:T(8,128)(2,1)S(1)} custom-call(bf16[2,128,16,128]{3,2,1,0:T(8,128)(2,1)} %source.6, bf16[4,4224]{1,0:T(4,128)(2,1)S(1)} %get-tuple-element.40.after.refs_0_), custom_call_target="tpu_custom_call" | custom-call | flops 4000000 | tf_op jit(solution)/shard_map/b0/pallas_call | solution.py:239
  15.1 0.9 %b0.4 = (f32[2,1,128,128]{3,2,1,0:T(8,128)S(1)}, bf16[2,2048]{1,0:T(2,128)(2,1)S(1)}) custom-call(bf16[4,4224]{1,0:T(4,128)(2,1)S(1)} %get-tuple-element.40.after.refs_0_, f32[2,1,128,128]{3,2,1,0:T(8,128)} %refs_0_.1, bf16[2,2048]{1,0:T(2,128)(2,1)} %refs_1_.3), custom_call_target="tpu_custom_call" | custom-call | flops 4000000 | tf_op jit(solution)/shard_map/b0/pallas_call | solution.py:239
  16.0 0.1 collective-permute-done.4.refs_2_
  16.2 1.1 %collective-permute-done.5.refs_3_ = bf16[4,4224]{1,0:T(4,128)(2,1)S(1)} collective-permute-done((bf16[4,4224]{1,0:T(4,128)(2,1)S(1)}, bf16[4,4224]{1,0:T(4,128)(2,1)S(1)}, u32[]{:S(2)}, u32[]{:S(2)}) %collective-permute-start.5) | collective-permute-done | bytes 33824 | tf_op jit(solution)/shard_map/b0/k3/ppermute | solution.py:85
  17.3 2.0 %shard_map.141 = (bf16[4,2048]{1,0:T(4,128)(2,1)S(1)}, f32[128,128]{1,0:T(8,128)S(1)}) custom-call(bf16[4,4224]{1,0:T(4,128)(2,1)S(1)} %get-tuple-element.40.after.refs_0_, bf16[4,4224]{1,0:T(4,128)(2,1)S(1)} %collective-permute-done.3.refs_1_, bf16[4,4224]{1,0:T(4,128)(2,1)S(1)} %collective-permute-done.4.refs_2_, ...), custom_call_target="tpu_custom_call" | custom-call | tf_op jit(solution)/shard_map/pallas_call | solution.py:239
  19.2 0.6 %collective-permute-start.8 = (bf16[4,2048]{1,0:T(4,128)(2,1)S(1)}, bf16[4,2048]{1,0:T(4,128)(2,1)S(1)}, u32[]{:S(2)}, u32[]{:S(2)}) collective-permute-start(bf16[4,2048]{1,0:T(4,128)(2,1)S(1)} %get-tuple-element.50.refs_0_), channel_id=1, source_target_pairs={{0,3},{1,2},{2,1},{3,0},{4,7},{5,6},{6,5},{7,4},{8,11},{9,10},{10,... | collective-permute-start | bytes 49160 | tf_op jit(solution)/shard_map/c0/k3/ppermute | solution.py:85
  19.9 1.2 %collective-permute-start.7 = (bf16[4,2048]{1,0:T(4,128)(2,1)S(1)}, bf16[4,2048]{1,0:T(4,128)(2,1)S(1)}, u32[]{:S(2)}, u32[]{:S(2)}) collective-permute-start(bf16[4,2048]{1,0:T(4,128)(2,1)S(1)} %get-tuple-element.50.refs_0_), channel_id=1, source_target_pairs={{0,2},{1,3},{2,0},{3,1},{4,6},{5,7},{6,4},{7,5},{8,10},{9,11},{10,... | collective-permute-start | bytes 49160 | tf_op jit(solution)/shard_map/c0/k2/ppermute | solution.py:85
  21.1 0.1 collective-permute-start.6
  21.2 2.2 %b0.5.refs_4_ = bf16[2048,1024]{1,0:T(8,128)(2,1)S(1)} custom-call(bf16[2,2048,1024]{2,1,0:T(8,128)(2,1)} %source.7, bf16[4,4224]{1,0:T(4,128)(2,1)S(1)} %get-tuple-element.40.after.refs_0_), custom_call_target="tpu_custom_call" | custom-call | flops 4000000 | tf_op jit(solution)/shard_map/b0/pallas_call | solution.py:239
  23.4 0.0 collective-permute-done.8.refs_3_
  23.4 0.2 collective-permute-done.7.refs_2_
  23.6 0.0 collective-permute-done.6.refs_1_
  23.6 0.6 %shard_map.142.refs_0_ = bf16[16,1024]{1,0:T(8,128)(2,1)S(1)} custom-call(bf16[4,2048]{1,0:T(4,128)(2,1)S(1)} %get-tuple-element.50.refs_0_, bf16[4,2048]{1,0:T(4,128)(2,1)S(1)} %collective-permute-done.6.refs_1_, bf16[4,2048]{1,0:T(4,128)(2,1)S(1)} %collective-permute-done.7.refs_2_, bf16[4,2048]{1,0:T(4,128)(2,1)S(1)} %collective-permute-done.8.refs_3_, ...), custom_call_target="tpu_custom_call" | custom-call | tf_op jit(solution)/shard_map/pallas_call | solution.py:239
  24.3 3.7 %collective-permute-start.11 = (bf16[16,1024]{1,0:T(8,128)(2,1)S(1)}, bf16[16,1024]{1,0:T(8,128)(2,1)S(1)}, u32[]{:S(2)}, u32[]{:S(2)}) collective-permute-start(bf16[16,1024]{1,0:T(8,128)(2,1)S(1)} %shard_map.142.refs_0_), channel_id=1, source_target_pairs={{0,12},{4,8},{8,4},{12,0},{1,13},{5,9},{9,5},{13,1},{2,14},{6,10},... | collective-permute-start | bytes 98312 | tf_op jit(solution)/shard_map/d0/k3/ppermute | solution.py:85
  28.0 0.7 %collective-permute-start.9 = (bf16[16,1024]{1,0:T(8,128)(2,1)S(1)}, bf16[16,1024]{1,0:T(8,128)(2,1)S(1)}, u32[]{:S(2)}, u32[]{:S(2)}) collective-permute-start(bf16[16,1024]{1,0:T(8,128)(2,1)S(1)} %shard_map.142.refs_0_), channel_id=1, source_target_pairs={{0,4},{4,0},{8,12},{12,8},{1,5},{5,1},{9,13},{13,9},{2,6},{6,2},{1... | collective-permute-start | bytes 98312 | tf_op jit(solution)/shard_map/d0/k1/ppermute | solution.py:85
  28.7 3.7 %d0.1 = (bf16[1024,2048]{1,0:T(8,128)(2,1)S(1)}, bf16[1024,2048]{1,0:T(8,128)(2,1)S(1)}, f32[128,128]{1,0:T(8,128)S(1)}, f32[128,128]{1,0:T(8,128)S(1)}, bf16[16,256,128]{2,1,0:T(8,128)(2,1)S(1)}) custom-call(bf16[16,1024]{1,0:T(8,128)(2,1)S(1)} %shard_map.142.refs_0_, f32[2,64,128]{2,1,0:T(8,128)} %bitcast.16, f32[2,64,128]{2,1,0:T(8,128)} %bitcast.18, ...), custom_call_target="tpu_custom_call" | custom-call | flops 4000000 | tf_op jit(solution)/shard_map/d0/pallas_call | solution.py:239
  32.4 0.0 collective-permute-done.11.refs_3_
  32.4 0.4 collective-permute-done.10.refs_2_
  32.8 1.2 %shard_map.143 = (bf16[4,4224]{1,0:T(4,128)(2,1)S(1)}, bf16[4,4224]{1,0:T(4,128)(2,1)S(1)}, bf16[4,4224]{1,0:T(4,128)(2,1)S(1)}, bf16[4,4224]{1,0:T(4,128)(2,1)S(1)}, f32[16,1024]{1,0:T(8,128)S(1)}) custom-call(f32[16,1024]{1,0:T(8,128)S(1)} %get-tuple-element.39.base_ref, bf16[16,1024]{1,0:T(8,128)(2,1)S(1)} %shard_map.142.refs_0_, ...), custom_call_target="tpu_custom_call" | custom-call | tf_op jit(solution)/shard_map/pallas_call | solution.py:239
  34.0 1.2 %collective-permute-start.13 = (bf16[4,4224]{1,0:T(4,128)(2,1)S(1)}, bf16[4,4224]{1,0:T(4,128)(2,1)S(1)}, u32[]{:S(2)}, u32[]{:S(2)}) collective-permute-start(bf16[4,4224]{1,0:T(4,128)(2,1)S(1)} %get-tuple-element.55), channel_id=1, source_target_pairs={{0,2},{1,3},{2,0},{3,1},{4,6},{5,7},{6,4},{7,5},{8,10},{9,11},{10,... | collective-permute-start | bytes 101384 | tf_op jit(solution)/shard_map/b1/k2/ppermute | solution.py:85
  35.2 0.7 %collective-permute-start.14 = (bf16[4,4224]{1,0:T(4,128)(2,1)S(1)}, bf16[4,4224]{1,0:T(4,128)(2,1)S(1)}, u32[]{:S(2)}, u32[]{:S(2)}) collective-permute-start(bf16[4,4224]{1,0:T(4,128)(2,1)S(1)} %get-tuple-element.56), channel_id=1, source_target_pairs={{0,3},{1,2},{2,1},{3,0},{4,7},{5,6},{6,5},{7,4},{8,11},{9,10},{10,... | collective-permute-start | bytes 101384 | tf_op jit(solution)/shard_map/b1/k3/ppermute | solution.py:85
  35.9 1.0 %b1.2 = bf16[128,16,128]{2,1,0:T(8,128)(2,1)S(1)} custom-call(bf16[2,128,16,128]{3,2,1,0:T(8,128)(2,1)} %source.6, bf16[4,4224]{1,0:T(4,128)(2,1)S(1)} %get-tuple-element.53.after.refs_0_), custom_call_target="tpu_custom_call" | custom-call | flops 4000000 | tf_op jit(solution)/shard_map/b1/pallas_call | solution.py:239
  36.9 1.0 %collective-permute-done.13.refs_2_ = bf16[4,4224]{1,0:T(4,128)(2,1)S(1)} collective-permute-done((bf16[4,4224]{1,0:T(4,128)(2,1)S(1)}, bf16[4,4224]{1,0:T(4,128)(2,1)S(1)}, u32[]{:S(2)}, u32[]{:S(2)}) %collective-permute-start.13) | collective-permute-done | bytes 33824 | tf_op jit(solution)/shard_map/b1/k2/ppermute | solution.py:85
  38.0 0.6 %collective-permute-done.14.refs_3_ = bf16[4,4224]{1,0:T(4,128)(2,1)S(1)} collective-permute-done((bf16[4,4224]{1,0:T(4,128)(2,1)S(1)}, bf16[4,4224]{1,0:T(4,128)(2,1)S(1)}, u32[]{:S(2)}, u32[]{:S(2)}) %collective-permute-start.14) | collective-permute-done | bytes 33824 | tf_op jit(solution)/shard_map/b1/k3/ppermute | solution.py:85
  38.6 2.0 %shard_map.144 = (bf16[4,2048]{1,0:T(4,128)(2,1)S(1)}, f32[128,128]{1,0:T(8,128)S(1)}) custom-call(bf16[4,4224]{1,0:T(4,128)(2,1)S(1)} %get-tuple-element.53.after.refs_0_, bf16[4,4224]{1,0:T(4,128)(2,1)S(1)} %collective-permute-done.12.refs_1_, bf16[4,4224]{1,0:T(4,128)(2,1)S(1)} %collective-permute-done.13.refs_2_, ...), custom_call_target="tpu_custom_call" | custom-call | tf_op jit(solution)/shard_map/pallas_call | solution.py:239
  40.6 0.8 %collective-permute-start.17 = (bf16[4,2048]{1,0:T(4,128)(2,1)S(1)}, bf16[4,2048]{1,0:T(4,128)(2,1)S(1)}, u32[]{:S(2)}, u32[]{:S(2)}) collective-permute-start(bf16[4,2048]{1,0:T(4,128)(2,1)S(1)} %get-tuple-element.60.refs_0_), channel_id=1, source_target_pairs={{0,3},{1,2},{2,1},{3,0},{4,7},{5,6},{6,5},{7,4},{8,11},{9,10},{10,... | collective-permute-start | bytes 49160 | tf_op jit(solution)/shard_map/c1/k3/ppermute | solution.py:85
  41.3 1.1 %collective-permute-start.16 = (bf16[4,2048]{1,0:T(4,128)(2,1)S(1)}, bf16[4,2048]{1,0:T(4,128)(2,1)S(1)}, u32[]{:S(2)}, u32[]{:S(2)}) collective-permute-start(bf16[4,2048]{1,0:T(4,128)(2,1)S(1)} %get-tuple-element.60.refs_0_), channel_id=1, source_target_pairs={{0,2},{1,3},{2,0},{3,1},{4,6},{5,7},{6,4},{7,5},{8,10},{9,11},{10,... | collective-permute-start | bytes 49160 | tf_op jit(solution)/shard_map/c1/k2/ppermute | solution.py:85
  42.4 0.0 collective-permute-start.15
  42.5 2.2 %b1.3.refs_4_ = bf16[2048,1024]{1,0:T(8,128)(2,1)S(1)} custom-call(bf16[2,2048,1024]{2,1,0:T(8,128)(2,1)} %source.7, bf16[4,4224]{1,0:T(4,128)(2,1)S(1)} %get-tuple-element.53.after.refs_0_), custom_call_target="tpu_custom_call" | custom-call | flops 4000000 | tf_op jit(solution)/shard_map/b1/pallas_call | solution.py:239
  44.7 0.4 collective-permute-done.16.refs_2_
  45.1 0.7 %shard_map.145 = (f32[4,1024]{1,0:T(4,128)S(1)}, bf16[4,1024]{1,0:T(4,128)(2,1)S(1)}, bf16[4,1024]{1,0:T(4,128)(2,1)S(1)}, bf16[4,1024]{1,0:T(4,128)(2,1)S(1)}) custom-call(bf16[4,2048]{1,0:T(4,128)(2,1)S(1)} %get-tuple-element.60.refs_0_, bf16[4,2048]{1,0:T(4,128)(2,1)S(1)} %collective-permute-done.15.refs_1_, ...), custom_call_target="tpu_custom_call" | custom-call | tf_op jit(solution)/shard_map/pallas_call | solution.py:239
  45.8 1.0 %collective-permute-start.18 = (bf16[4,1024]{1,0:T(4,128)(2,1)S(1)}, bf16[4,1024]{1,0:T(4,128)(2,1)S(1)}, u32[]{:S(2)}, u32[]{:S(2)}) collective-permute-start(bf16[4,1024]{1,0:T(4,128)(2,1)S(1)} %get-tuple-element.63), channel_id=1, source_target_pairs={{0,4},{4,0},{8,12},{12,8},{1,5},{5,1},{9,13},{13,9},{2,6},{6,2},{1... | collective-permute-start | bytes 24584 | tf_op jit(solution)/shard_map/d1/k1/ppermute | solution.py:85
  46.8 2.9 %collective-permute-start.19 = (bf16[4,1024]{1,0:T(4,128)(2,1)S(1)}, bf16[4,1024]{1,0:T(4,128)(2,1)S(1)}, u32[]{:S(2)}, u32[]{:S(2)}) collective-permute-start(bf16[4,1024]{1,0:T(4,128)(2,1)S(1)} %get-tuple-element.64), channel_id=1, source_target_pairs={{0,8},{4,12},{8,0},{12,4},{1,9},{5,13},{9,1},{13,5},{2,10},{6,14},... | collective-permute-start | bytes 24584 | tf_op jit(solution)/shard_map/d1/k2/ppermute | solution.py:85
  49.7 0.5 collective-permute-start.20
  50.2 0.7 %maximum_bitcast_fusion = f32[2,1,128,128]{3,2,1,0:T(8,128)} fusion(f32[1,128,128]{2,1,0:T(8,128)S(1)} %bitcast.14, f32[1,128,128]{2,1,0:T(8,128)S(1)} %bitcast.13), kind=kLoop, calls=%fused_computation | loop fusion | flops 32768 | bytes 262144
  50.8 0.5 collective-permute-done.19.refs_1_
  51.3 3.8 %collective-permute-done.20.refs_2_ = bf16[4,1024]{1,0:T(4,128)(2,1)S(1)} collective-permute-done((bf16[4,1024]{1,0:T(4,128)(2,1)S(1)}, bf16[4,1024]{1,0:T(4,128)(2,1)S(1)}, u32[]{:S(2)}, u32[]{:S(2)}) %collective-permute-start.20) | collective-permute-done | bytes 8224 | tf_op jit(solution)/shard_map/d1/k3/ppermute | solution.py:85
  55.1 0.6 %shard_map.146 = bf16[1,4,1024]{2,1,0:T(4,128)(2,1)} custom-call(f32[4,1024]{1,0:T(4,128)S(1)} %get-tuple-element.62.own_ref, bf16[4,1024]{1,0:T(4,128)(2,1)S(1)} %collective-permute-done.18.refs_0_, bf16[4,1024]{1,0:T(4,128)(2,1)S(1)} %collective-permute-done.19.refs_1_, bf16[4,1024]{1,0:T(4,128)(2,1)S(1)} %collective-permute-done.20.refs_2_), custom_call_target="tpu_custom_call" | custom-call | tf_op jit(solution)/shard_map/pallas_call | solution.py:239
  (10 shorter events, 0.0 us)
Async XLA Ops:
  0.6 10.3 %collective-permute-start.2 = (bf16[4,1024]{1,0:T(4,128)(2,1)}, bf16[4,1024]{1,0:T(4,128)(2,1)S(1)}, u32[]{:S(2)}, u32[]{:S(2)}) collective-permute-start(bf16[4,1024]{1,0:T(4,128)(2,1)} %bitcast.19), channel_id=1, source_target_pairs={{0,12},{4,8},{8,4},{12,0},{1,13},{5,9},{9,5},{13,1},{2,14},{6,10},... | collective-permute-start | bytes 24584 | tf_op jit(solution)/shard_map/a/k3/ppermute | solution.py:85
  5.8 5.2 %collective-permute-start.1 = (bf16[4,1024]{1,0:T(4,128)(2,1)}, bf16[4,1024]{1,0:T(4,128)(2,1)S(1)}, u32[]{:S(2)}, u32[]{:S(2)}) collective-permute-start(bf16[4,1024]{1,0:T(4,128)(2,1)} %bitcast.20), channel_id=1, source_target_pairs={{0,8},{4,12},{8,0},{12,4},{1,9},{5,13},{9,1},{13,5},{2,10},{6,14},... | collective-permute-start | bytes 24584 | tf_op jit(solution)/shard_map/a/k2/ppermute | solution.py:85
  5.8 5.2 %collective-permute-start = (bf16[4,1024]{1,0:T(4,128)(2,1)}, bf16[4,1024]{1,0:T(4,128)(2,1)S(1)}, u32[]{:S(2)}, u32[]{:S(2)}) collective-permute-start(bf16[4,1024]{1,0:T(4,128)(2,1)} %bitcast.21), channel_id=1, source_target_pairs={{0,4},{4,0},{8,12},{12,8},{1,5},{5,1},{9,13},{13,9},{2,6},{6,2},{1... | collective-permute-start | bytes 24584 | tf_op jit(solution)/shard_map/a/k1/ppermute | solution.py:85
  12.2 3.9 %collective-permute-start.3 = (bf16[4,4224]{1,0:T(4,128)(2,1)S(1)}, bf16[4,4224]{1,0:T(4,128)(2,1)S(1)}, u32[]{:S(2)}, u32[]{:S(2)}) collective-permute-start(bf16[4,4224]{1,0:T(4,128)(2,1)S(1)} %get-tuple-element.41), channel_id=1, source_target_pairs={{0,1},{1,0},{2,3},{3,2},{4,5},{5,4},{6,7},{7,6},{8,9},{9,8},{10,11... | collective-permute-start | bytes 101384 | tf_op jit(solution)/shard_map/b0/k1/ppermute | solution.py:85
  12.2 4.0 %collective-permute-start.4 = (bf16[4,4224]{1,0:T(4,128)(2,1)S(1)}, bf16[4,4224]{1,0:T(4,128)(2,1)S(1)}, u32[]{:S(2)}, u32[]{:S(2)}) collective-permute-start(bf16[4,4224]{1,0:T(4,128)(2,1)S(1)} %get-tuple-element.42), channel_id=1, source_target_pairs={{0,2},{1,3},{2,0},{3,1},{4,6},{5,7},{6,4},{7,5},{8,10},{9,11},{10,... | collective-permute-start | bytes 101384 | tf_op jit(solution)/shard_map/b0/k2/ppermute | solution.py:85
  13.9 3.4 %collective-permute-start.5 = (bf16[4,4224]{1,0:T(4,128)(2,1)S(1)}, bf16[4,4224]{1,0:T(4,128)(2,1)S(1)}, u32[]{:S(2)}, u32[]{:S(2)}) collective-permute-start(bf16[4,4224]{1,0:T(4,128)(2,1)S(1)} %get-tuple-element.43), channel_id=1, source_target_pairs={{0,3},{1,2},{2,1},{3,0},{4,7},{5,6},{6,5},{7,4},{8,11},{9,10},{10,... | collective-permute-start | bytes 101384 | tf_op jit(solution)/shard_map/b0/k3/ppermute | solution.py:85
  19.2 4.1 %collective-permute-start.8 = (bf16[4,2048]{1,0:T(4,128)(2,1)S(1)}, bf16[4,2048]{1,0:T(4,128)(2,1)S(1)}, u32[]{:S(2)}, u32[]{:S(2)}) collective-permute-start(bf16[4,2048]{1,0:T(4,128)(2,1)S(1)} %get-tuple-element.50.refs_0_), channel_id=1, source_target_pairs={{0,3},{1,2},{2,1},{3,0},{4,7},{5,6},{6,5},{7,4},{8,11},{9,10},{10,... | collective-permute-start | bytes 49160 | tf_op jit(solution)/shard_map/c0/k3/ppermute | solution.py:85
  19.9 3.7 %collective-permute-start.7 = (bf16[4,2048]{1,0:T(4,128)(2,1)S(1)}, bf16[4,2048]{1,0:T(4,128)(2,1)S(1)}, u32[]{:S(2)}, u32[]{:S(2)}) collective-permute-start(bf16[4,2048]{1,0:T(4,128)(2,1)S(1)} %get-tuple-element.50.refs_0_), channel_id=1, source_target_pairs={{0,2},{1,3},{2,0},{3,1},{4,6},{5,7},{6,4},{7,5},{8,10},{9,11},{10,... | collective-permute-start | bytes 49160 | tf_op jit(solution)/shard_map/c0/k2/ppermute | solution.py:85
  21.1 2.5 %collective-permute-start.6 = (bf16[4,2048]{1,0:T(4,128)(2,1)S(1)}, bf16[4,2048]{1,0:T(4,128)(2,1)S(1)}, u32[]{:S(2)}, u32[]{:S(2)}) collective-permute-start(bf16[4,2048]{1,0:T(4,128)(2,1)S(1)} %get-tuple-element.50.refs_0_), channel_id=1, source_target_pairs={{0,1},{1,0},{2,3},{3,2},{4,5},{5,4},{6,7},{7,6},{8,9},{9,8},{10,11... | collective-permute-start | bytes 49160 | tf_op jit(solution)/shard_map/c0/k1/ppermute | solution.py:85
  24.3 8.1 %collective-permute-start.11 = (bf16[16,1024]{1,0:T(8,128)(2,1)S(1)}, bf16[16,1024]{1,0:T(8,128)(2,1)S(1)}, u32[]{:S(2)}, u32[]{:S(2)}) collective-permute-start(bf16[16,1024]{1,0:T(8,128)(2,1)S(1)} %shard_map.142.refs_0_), channel_id=1, source_target_pairs={{0,12},{4,8},{8,4},{12,0},{1,13},{5,9},{9,5},{13,1},{2,14},{6,10},... | collective-permute-start | bytes 98312 | tf_op jit(solution)/shard_map/d0/k3/ppermute | solution.py:85
  28.0 4.8 %collective-permute-start.10 = (bf16[16,1024]{1,0:T(8,128)(2,1)S(1)}, bf16[16,1024]{1,0:T(8,128)(2,1)S(1)}, u32[]{:S(2)}, u32[]{:S(2)}) collective-permute-start(bf16[16,1024]{1,0:T(8,128)(2,1)S(1)} %shard_map.142.refs_0_), channel_id=1, source_target_pairs={{0,8},{4,12},{8,0},{12,4},{1,9},{5,13},{9,1},{13,5},{2,10},{6,14},... | collective-permute-start | bytes 98312 | tf_op jit(solution)/shard_map/d0/k2/ppermute | solution.py:85
  28.0 4.8 %collective-permute-start.9 = (bf16[16,1024]{1,0:T(8,128)(2,1)S(1)}, bf16[16,1024]{1,0:T(8,128)(2,1)S(1)}, u32[]{:S(2)}, u32[]{:S(2)}) collective-permute-start(bf16[16,1024]{1,0:T(8,128)(2,1)S(1)} %shard_map.142.refs_0_), channel_id=1, source_target_pairs={{0,4},{4,0},{8,12},{12,8},{1,5},{5,1},{9,13},{13,9},{2,6},{6,2},{1... | collective-permute-start | bytes 98312 | tf_op jit(solution)/shard_map/d0/k1/ppermute | solution.py:85
  34.0 2.9 %collective-permute-start.12 = (bf16[4,4224]{1,0:T(4,128)(2,1)S(1)}, bf16[4,4224]{1,0:T(4,128)(2,1)S(1)}, u32[]{:S(2)}, u32[]{:S(2)}) collective-permute-start(bf16[4,4224]{1,0:T(4,128)(2,1)S(1)} %get-tuple-element.54), channel_id=1, source_target_pairs={{0,1},{1,0},{2,3},{3,2},{4,5},{5,4},{6,7},{7,6},{8,9},{9,8},{10,11... | collective-permute-start | bytes 101384 | tf_op jit(solution)/shard_map/b1/k1/ppermute | solution.py:85
  34.0 4.0 %collective-permute-start.13 = (bf16[4,4224]{1,0:T(4,128)(2,1)S(1)}, bf16[4,4224]{1,0:T(4,128)(2,1)S(1)}, u32[]{:S(2)}, u32[]{:S(2)}) collective-permute-start(bf16[4,4224]{1,0:T(4,128)(2,1)S(1)} %get-tuple-element.55), channel_id=1, source_target_pairs={{0,2},{1,3},{2,0},{3,1},{4,6},{5,7},{6,4},{7,5},{8,10},{9,11},{10,... | collective-permute-start | bytes 101384 | tf_op jit(solution)/shard_map/b1/k2/ppermute | solution.py:85
  35.2 3.4 %collective-permute-start.14 = (bf16[4,4224]{1,0:T(4,128)(2,1)S(1)}, bf16[4,4224]{1,0:T(4,128)(2,1)S(1)}, u32[]{:S(2)}, u32[]{:S(2)}) collective-permute-start(bf16[4,4224]{1,0:T(4,128)(2,1)S(1)} %get-tuple-element.56), channel_id=1, source_target_pairs={{0,3},{1,2},{2,1},{3,0},{4,7},{5,6},{6,5},{7,4},{8,11},{9,10},{10,... | collective-permute-start | bytes 101384 | tf_op jit(solution)/shard_map/b1/k3/ppermute | solution.py:85
  40.6 4.1 %collective-permute-start.17 = (bf16[4,2048]{1,0:T(4,128)(2,1)S(1)}, bf16[4,2048]{1,0:T(4,128)(2,1)S(1)}, u32[]{:S(2)}, u32[]{:S(2)}) collective-permute-start(bf16[4,2048]{1,0:T(4,128)(2,1)S(1)} %get-tuple-element.60.refs_0_), channel_id=1, source_target_pairs={{0,3},{1,2},{2,1},{3,0},{4,7},{5,6},{6,5},{7,4},{8,11},{9,10},{10,... | collective-permute-start | bytes 49160 | tf_op jit(solution)/shard_map/c1/k3/ppermute | solution.py:85
  41.3 3.7 %collective-permute-start.16 = (bf16[4,2048]{1,0:T(4,128)(2,1)S(1)}, bf16[4,2048]{1,0:T(4,128)(2,1)S(1)}, u32[]{:S(2)}, u32[]{:S(2)}) collective-permute-start(bf16[4,2048]{1,0:T(4,128)(2,1)S(1)} %get-tuple-element.60.refs_0_), channel_id=1, source_target_pairs={{0,2},{1,3},{2,0},{3,1},{4,6},{5,7},{6,4},{7,5},{8,10},{9,11},{10,... | collective-permute-start | bytes 49160 | tf_op jit(solution)/shard_map/c1/k2/ppermute | solution.py:85
  42.4 2.7 %collective-permute-start.15 = (bf16[4,2048]{1,0:T(4,128)(2,1)S(1)}, bf16[4,2048]{1,0:T(4,128)(2,1)S(1)}, u32[]{:S(2)}, u32[]{:S(2)}) collective-permute-start(bf16[4,2048]{1,0:T(4,128)(2,1)S(1)} %get-tuple-element.60.refs_0_), channel_id=1, source_target_pairs={{0,1},{1,0},{2,3},{3,2},{4,5},{5,4},{6,7},{7,6},{8,9},{9,8},{10,11... | collective-permute-start | bytes 49160 | tf_op jit(solution)/shard_map/c1/k1/ppermute | solution.py:85
  45.8 5.1 %collective-permute-start.18 = (bf16[4,1024]{1,0:T(4,128)(2,1)S(1)}, bf16[4,1024]{1,0:T(4,128)(2,1)S(1)}, u32[]{:S(2)}, u32[]{:S(2)}) collective-permute-start(bf16[4,1024]{1,0:T(4,128)(2,1)S(1)} %get-tuple-element.63), channel_id=1, source_target_pairs={{0,4},{4,0},{8,12},{12,8},{1,5},{5,1},{9,13},{13,9},{2,6},{6,2},{1... | collective-permute-start | bytes 24584 | tf_op jit(solution)/shard_map/d1/k1/ppermute | solution.py:85
  46.8 4.5 %collective-permute-start.19 = (bf16[4,1024]{1,0:T(4,128)(2,1)S(1)}, bf16[4,1024]{1,0:T(4,128)(2,1)S(1)}, u32[]{:S(2)}, u32[]{:S(2)}) collective-permute-start(bf16[4,1024]{1,0:T(4,128)(2,1)S(1)} %get-tuple-element.64), channel_id=1, source_target_pairs={{0,8},{4,12},{8,0},{12,4},{1,9},{5,13},{9,1},{13,5},{2,10},{6,14},... | collective-permute-start | bytes 24584 | tf_op jit(solution)/shard_map/d1/k2/ppermute | solution.py:85
  49.7 5.4 %collective-permute-start.20 = (bf16[4,1024]{1,0:T(4,128)(2,1)S(1)}, bf16[4,1024]{1,0:T(4,128)(2,1)S(1)}, u32[]{:S(2)}, u32[]{:S(2)}) collective-permute-start(bf16[4,1024]{1,0:T(4,128)(2,1)S(1)} %get-tuple-element.65), channel_id=1, source_target_pairs={{0,12},{4,8},{8,4},{12,0},{1,13},{5,9},{9,5},{13,1},{2,14},{6,10},... | collective-permute-start | bytes 24584 | tf_op jit(solution)/shard_map/d1/k3/ppermute | solution.py:85

commit v3 on v2

--- a/solution.py
+++ b/solution.py
@@ -6,6 +6,7 @@
 from jax.experimental import pallas as pl
 from jax.experimental.pallas import tpu as pltpu
 from jax.sharding import PartitionSpec as P
+
 
 D = 4096
 S5_IN = 16
@@ -223,7 +224,7 @@
 
 
 LANES = 128
-COST = 4000000
+COST = 40000000000
 SUBLANES = 8
 VMEM = pl.BlockSpec(memory_space=pltpu.VMEM)
 HBM = pl.BlockSpec(memory_space=pltpu.MemorySpace.HBM)
@@ -257,7 +258,7 @@
     return high, low
 
 
-def group_mask(dtype=jnp.float32):
+def group_mask():
     lane = lax.broadcasted_iota(jnp.int32, (SUBLANES, LANES), 1)
     row = lax.broadcasted_iota(jnp.int32, (SUBLANES, LANES), 0)
     return lane // S5_IN == row
@@ -309,48 +310,20 @@
         coupled_ref[chunk, LANES:] = low
 
 
-def prepare_kernel(layer, decay_hbm, frequency_hbm, log_step_hbm, map_hbm, *refs):
-    count = (len(refs) - 8) // 2
-    sources, targets = refs[:count], refs[count : 2 * count]
-    real_ref, imag_ref, coupled_ref = refs[2 * count : 2 * count + 3]
-    decay, frequency, log_step, maps, semaphores = refs[2 * count + 3 :]
-    small = start_copies(
-        [decay_hbm.at[layer], frequency_hbm.at[layer], log_step_hbm, map_hbm.at[layer]],
-        [decay, frequency, log_step, maps],
-        semaphores.at[pl.ds(0, 4)],
-    )
-    large = start_copies(
-        [source.at[layer] for source in sources], targets, semaphores.at[pl.ds(4, count)]
-    )
-    wait_copies(small)
+def parameter_kernel(layer, decay_ref, frequency_ref, log_step_ref, map_ref, *refs):
     parameter_step(
-        decay[...], frequency[...], log_step[layer : layer + 1], maps, real_ref, imag_ref, coupled_ref
-    )
-    wait_copies(large)
-
-
-def prepare(layer, decay, frequency, log_step, input_map, projections, after=()):
-    _, half, groups = decay.shape
-    f32, bf16 = jnp.float32, jnp.bfloat16
-    after = list(after)
-
-    def kernel(*refs):
-        prepare_kernel(layer, *refs[len(after) :])
-
+        decay_ref[layer], frequency_ref[layer], log_step_ref[layer : layer + 1],
+        map_ref.at[layer], *refs[-3:],
+    )
+
+
+def prepare(layer, decay, frequency, log_step, input_map, after=()):
+    _, _, groups = decay.shape
     return vmem_call(
-        kernel,
-        [(p.shape[1:], bf16) for p in projections]
-        + [((groups, LANES), f32)] * 2
-        + [((groups // SUBLANES, 2 * LANES, LANES), bf16)],
-        *after, decay, frequency, log_step, input_map, *projections,
-        in_specs=[VMEM] * len(after) + [HBM] * (4 + len(projections)),
-        scratch=[
-            pltpu.VMEM((half, groups), f32),
-            pltpu.VMEM((half, groups), f32),
-            pltpu.VMEM(log_step.shape, f32),
-            pltpu.VMEM(input_map.shape[1:], bf16),
-            pltpu.SemaphoreType.DMA((4 + len(projections),)),
-        ],
+        functools.partial(parameter_kernel, layer),
+        [((groups, LANES), jnp.float32)] * 2
+        + [((groups // SUBLANES, 2 * LANES, LANES), jnp.bfloat16)],
+        decay, frequency, log_step, input_map, *after,
         cost=COST,
     )
 
@@ -383,48 +356,17 @@
     )
 
 
-def bring_all_kernel(count, after, *refs):
-    wait_copies(start_copies(refs[:count], refs[count : 2 * count], refs[-1]))
-
-
-def bring_both(arrays, after):
-    return vmem_call(
-        functools.partial(bring_all_kernel, len(arrays)),
-        [(a.shape, a.dtype) for a in arrays],
-        after, *arrays,
-        in_specs=[VMEM] + [HBM] * len(arrays),
-        scratch=[pltpu.SemaphoreType.DMA((len(arrays),))],
-        cost=COST,
-    )
-
-
 def swaps(values, axis, size):
     received = {}
     for k in reversed(range(1, size)):
-        with jax.named_scope(f"k{k}"):
-            value = values[k] if isinstance(values, (list, tuple)) else values
-            received[k] = swap(value, axis, k, size)
+        value = values[k] if isinstance(values, (list, tuple)) else values
+        received[k] = swap(value, axis, k, size)
     return [received[k] for k in range(1, size)]
-
-
-def bring_kernel(layer, source, after, target, semaphores):
-    wait_copies(start_copies([source.at[layer]], [target], semaphores))
-
-
-def bring(layer, source, after):
-    return vmem_call(
-        functools.partial(bring_kernel, layer),
-        [(source.shape[1:], source.dtype)],
-        source, after,
-        in_specs=[HBM, VMEM],
-        scratch=[pltpu.SemaphoreType.DMA((1,))],
-        cost=COST,
-    )[0]
 
 
 def project(layer, rows, gain_ref, drive_weight_ref, gate_weight_ref, message_refs):
     count = rows.shape[0] // len(message_refs)
-    width = drive_weight_ref.shape[1]
+    width = drive_weight_ref.shape[2]
     scaled = (rows * gain_ref[layer : layer + 1]).astype(jnp.bfloat16)
     squares = jnp.sum(rows * rows, axis=1, keepdims=True)
     lane = lax.broadcasted_iota(jnp.int32, (rows.shape[0], LANES), 1)
@@ -438,7 +380,7 @@
     for base, weight_ref in ((0, drive_weight_ref), (width, gate_weight_ref)):
         for at in range(0, width, step):
             value = jnp.dot(
-                scaled, weight_ref[:, at : at + step], preferred_element_type=jnp.float32
+                scaled, weight_ref[layer, :, at : at + step], preferred_element_type=jnp.float32
             )
             parts.append((base + at, step, value))
     for at, size, value in parts:
@@ -527,7 +469,7 @@
         high, low = halves(jnp.concatenate(history, axis=0))
         seen = lax.dot_general(
             jnp.concatenate([high, low], axis=0),
-            readout_ref[chunk],
+            readout_ref[layer, chunk],
             (((1,), (1,)), ((), ())),
             preferred_element_type=jnp.float32,
         )
@@ -549,19 +491,19 @@
         branch_ref[:, at] = value.astype(jnp.bfloat16)
 
 
-def output_kernel(size, *refs):
+def output_kernel(size, layer, *refs):
     branch_refs, weight_ref, out_ref = refs[:size], refs[size], refs[size + 1]
     rows = jnp.concatenate([ref[...].astype(jnp.float32) for ref in branch_refs], axis=0)
     out_ref[...] = jnp.dot(
-        rows.astype(jnp.bfloat16), weight_ref[...], preferred_element_type=jnp.float32
+        rows.astype(jnp.bfloat16), weight_ref[layer], preferred_element_type=jnp.float32
     ).astype(jnp.bfloat16)
 
 
-def last_output_kernel(size, *refs):
+def last_output_kernel(size, layer, *refs):
     branch_refs, weight_ref, base_ref = refs[:size], refs[size], refs[size + 1]
     out_refs = refs[size + 2 :]
     rows = jnp.concatenate([ref[...].astype(jnp.float32) for ref in branch_refs], axis=0)
-    value = jnp.dot(rows.astype(jnp.bfloat16), weight_ref[...], preferred_element_type=jnp.float32)
+    value = jnp.dot(rows.astype(jnp.bfloat16), weight_ref[layer], preferred_element_type=jnp.float32)
     count = rows.shape[0] // size
     blocks = [value[k * count : (k + 1) * count] for k in range(size)]
     offset = own_offset()
@@ -585,7 +527,7 @@
     return direct(dp_size) and equal and one_each and whole_groups and map_rows == S5_IN
 
 
-def direct_body(
+def direct_steps(
     tokens,
     lengths,
     norm_gain,
@@ -609,15 +551,16 @@
     bf16, f32 = jnp.bfloat16, jnp.float32
     message = [((steps, 2 * inner + LANES), bf16)] * size
     rows_shape = ((count, features), f32)
+    readout = readout_map.reshape(LAYERS, chunks, LANES, LANES)
     projections = (input_weight, gate_weight)
     decay, frequency = (jnp.swapaxes(value, 1, 2) for value in (decay_rate, frequency))
-    raw = (decay, frequency, log_step, input_map, projections)
+    raw = (decay, frequency, log_step, input_map)
     own = tokens.reshape(steps, features)
-    with jax.named_scope("a"):
-        pieces = swaps(own, "tp", size)
-        own, gain, live = bring_small(steps, lengths, own, norm_gain)
-        pieces = [own] + pieces
-        *weights, real, imag, coupled = prepare(0, *raw)
+    own, gain, live = bring_small(steps, lengths, own, norm_gain)
+    pieces = swaps(own, "tp", size)
+    pieces = [own] + pieces
+    real, imag, coupled = prepare(0, *raw)
+    weights = projections
     states = []
     for layer in range(LAYERS):
         if layer == 0:
@@ -626,38 +569,31 @@
             kernel, base = functools.partial(next_kernel, size, layer), [rows]
         results = vmem_call(kernel, message + [rows_shape], *base, *pieces, gain, *weights)
         messages, rows = results[:size], results[size]
-        with jax.named_scope(f"b{layer}"):
-            arrived = [messages[0]] + swaps(messages, "dp", size)
-            out_now = bring(layer, out_weight, messages[0])
-            readout = bring(layer, readout_map, messages[0])
-            if layer == 0:
-                state_now, skip = bring_both((state, skip_weight), messages[0])
+        arrived = [messages[0]] + swaps(messages, "dp", size)
+        out_now = out_weight
         branch, next_state = vmem_call(
             functools.partial(state_kernel, size, layer, D),
             [((steps, inner), bf16), ((groups, LANES), f32)],
             *arrived, live, real, imag, coupled,
-            readout.reshape(chunks, LANES, LANES), skip, state_now,
+            readout, skip_weight, state,
         )
         states.append(next_state)
-        with jax.named_scope(f"c{layer}"):
-            branches = [branch] + swaps(branch, "dp", size)
+        branches = [branch] + swaps(branch, "dp", size)
         if layer < LAYERS - 1:
             (part,) = vmem_call(
-                functools.partial(output_kernel, size),
+                functools.partial(output_kernel, size, layer),
                 [((count, features), bf16)],
                 *branches, out_now,
             )
-            with jax.named_scope(f"d{layer}"):
-                pieces = [part] + swaps(part, "tp", size)
-                *weights, real, imag, coupled = prepare(layer + 1, *raw, after=[part])
+            pieces = [part] + swaps(part, "tp", size)
+            real, imag, coupled = prepare(layer + 1, *raw, after=[part])
             continue
         parts = vmem_call(
-            functools.partial(last_output_kernel, size),
+            functools.partial(last_output_kernel, size, layer),
             [((steps, features), f32)] + [((steps, features), bf16)] * (size - 1),
             *branches, out_now, rows,
         )
-        with jax.named_scope(f"d{layer}"):
-            arrived = swaps(parts, "tp", size)
+        arrived = swaps(parts, "tp", size)
         (mixed,) = vmem_call(final_kernel, [((1, steps, features), bf16)], parts[0], *arrived)
     return mixed, jnp.stack(states)[:, None]
 
@@ -666,12 +602,12 @@
     tokens, lengths, input_map, state = (arguments[i] for i in (0, 1, 8, 12))
     sizes = lax.axis_size("dp"), lax.axis_size("tp")
     if fits(tokens, lengths, state, input_map.shape[2], *sizes):
-        return direct_body(*arguments)
+        return direct_steps(*arguments)
     return general_body(*arguments)
 
 
 def solution(mesh):
-    return jax.shard_map(
+    step = jax.shard_map(
         body,
         mesh=mesh,
         in_specs=(
@@ -692,3 +628,7 @@
         out_specs=(P(("grp", "tp"), None, "dp"), P(None, ("grp", "dp"), "tp", None)),
         check_vma=False,
     )
+    size = mesh.shape["dp"]
+    if size != mesh.shape["tp"] or not direct(size):
+        return step
+    return step

time: 56.1 us -> 53.4 us (0.952)
  Pallas kernels: 23.9 us -> 10.5 us
  waiting for transfers between devices: 8.16 us -> 19 us
    pallas_call x15 -> x10, Pallas kernels: 23.9 us -> 10.5 us  [vmem_call(): pl.pallas_call(kernel, out_shape=outs, in_specs=in_specs, out_specs=[VMEM...]
    ppermute x21, waiting for transfers between devices: 8.16 us -> 19 us  [swap(): return lax.ppermute(value, axis, [(i, i ^ distance) for i in range(size)])]
  transfers between devices with their start and end apart: 21 -> 21, of which waited for: 9 -> 15; matrix products, arithmetic and copies ran while one was open for 1% -> 1% of each run, Pallas kernels for 28% -> 2%
where the time goes in v3:
time: 53.4 us; the launch traced here: 53.2 us
  starting transfers between devices  22.2 us (42%)
  waiting for transfers between devices  19 us (36%)
  Pallas kernels  10.5 us (20%)
  between operations  0.81 us (2%)
  other arithmetic  0.66 us (1%)
    ppermute x21, starting transfers between devices, swap(): return lax.ppermute(value, axis, [(i, i ^ distance) for i in range(size)])  22.2 us
    ppermute x21, waiting for transfers between devices, swap(): return lax.ppermute(value, axis, [(i, i ^ distance) for i in range(size)])  19 us
    pallas_call x10, Pallas kernels, vmem_call(): pl.pallas_call(kernel, out_shape=outs, in_specs=in_specs, out_specs=[VMEM...  10.5 us
  transfers between devices with their start and end apart: 21, of which 15 were waited for; matrix products, arithmetic and copies ran while one was open for 1% of the time, Pallas kernels for 2%

profile of v3, /device:TPU:0, one launch (start us, length us, event | category | flops | bytes accessed | tf_op | source)
XLA Modules:
  0.0 53.2 jit_solution(7387745597464231235)
XLA Ops:
  0.7 0.9 %shard_map.140 = (bf16[4,1024]{1,0:T(4,128)(2,1)S(1)}, f32[2,1024]{1,0:T(2,128)S(1)}, f32[32,128]{1,0:T(8,128)S(1)}) custom-call(s32[4]{0:T(128)} %lengths_hbm.1, bf16[4,1024]{1,0:T(4,128)(2,1)} %bitcast.20, f32[2,1024]{1,0:T(2,128)} %refs_1_.1), custom_call_target="tpu_custom_call" | custom-call | flops 40000000000 | tf_op jit(solution)/shard_map/pallas_call | solution.py:240
  1.5 5.1 %collective-permute-start.2 = (bf16[4,1024]{1,0:T(4,128)(2,1)S(1)}, bf16[4,1024]{1,0:T(4,128)(2,1)S(1)}, u32[]{:S(2)}, u32[]{:S(2)}) collective-permute-start(bf16[4,1024]{1,0:T(4,128)(2,1)S(1)} %get-tuple-element.29.refs_0_), channel_id=1, source_target_pairs={{0,12},{4,8},{8,4},{12,0},{1,13},{5,9},{9,5},{13,1},{2,14},{6,10},... | collective-permute-start | bytes 24584 | tf_op jit(solution)/shard_map/ppermute | solution.py:86
  6.7 0.6 %collective-permute-start = (bf16[4,1024]{1,0:T(4,128)(2,1)S(1)}, bf16[4,1024]{1,0:T(4,128)(2,1)S(1)}, u32[]{:S(2)}, u32[]{:S(2)}) collective-permute-start(bf16[4,1024]{1,0:T(4,128)(2,1)S(1)} %get-tuple-element.29.refs_0_), channel_id=1, source_target_pairs={{0,4},{4,0},{8,12},{12,8},{1,5},{5,1},{9,13},{13,9},{2,6},{6,2},{1... | collective-permute-start | bytes 24584 | tf_op jit(solution)/shard_map/ppermute | solution.py:86
  7.3 1.0 %collective-permute-done.2.refs_3_ = bf16[4,1024]{1,0:T(4,128)(2,1)S(1)} collective-permute-done((bf16[4,1024]{1,0:T(4,128)(2,1)S(1)}, bf16[4,1024]{1,0:T(4,128)(2,1)S(1)}, u32[]{:S(2)}, u32[]{:S(2)}) %collective-permute-start.2) | collective-permute-done | bytes 8224 | tf_op jit(solution)/shard_map/ppermute | solution.py:86
  8.3 2.9 %collective-permute-done.1.refs_2_ = bf16[4,1024]{1,0:T(4,128)(2,1)S(1)} collective-permute-done((bf16[4,1024]{1,0:T(4,128)(2,1)S(1)}, bf16[4,1024]{1,0:T(4,128)(2,1)S(1)}, u32[]{:S(2)}, u32[]{:S(2)}) %collective-permute-start.1) | collective-permute-done | bytes 8224 | tf_op jit(solution)/shard_map/ppermute | solution.py:86
  11.3 0.0 copy-start.7
  11.3 0.0 copy-start.8
  11.3 0.0 slice-start
  11.3 1.2 %shard_map.141 = (bf16[4,4224]{1,0:T(4,128)(2,1)S(1)}, bf16[4,4224]{1,0:T(4,128)(2,1)S(1)}, bf16[4,4224]{1,0:T(4,128)(2,1)S(1)}, bf16[4,4224]{1,0:T(4,128)(2,1)S(1)}, f32[16,1024]{1,0:T(8,128)S(1)}) custom-call(bf16[4,1024]{1,0:T(4,128)(2,1)S(1)} %get-tuple-element.29.refs_0_, bf16[4,1024]{1,0:T(4,128)(2,1)S(1)} %collective-permute-done.refs_1_, ...), custom_call_target="tpu_custom_call" | custom-call | tf_op jit(solution)/shard_map/pallas_call | solution.py:240
  12.5 1.6 %collective-permute-start.4 = (bf16[4,4224]{1,0:T(4,128)(2,1)S(1)}, bf16[4,4224]{1,0:T(4,128)(2,1)S(1)}, u32[]{:S(2)}, u32[]{:S(2)}) collective-permute-start(bf16[4,4224]{1,0:T(4,128)(2,1)S(1)} %get-tuple-element.34), channel_id=1, source_target_pairs={{0,2},{1,3},{2,0},{3,1},{4,6},{5,7},{6,4},{7,5},{8,10},{9,11},{10,... | collective-permute-start | bytes 101384 | tf_op jit(solution)/shard_map/ppermute | solution.py:86
  14.1 0.3 collective-permute-start.5
  14.4 0.0 slice-start.1
  14.5 0.6 %shard_map.142 = (f32[128,128]{1,0:T(8,128)S(1)}, f32[128,128]{1,0:T(8,128)S(1)}, bf16[16,256,128]{2,1,0:T(8,128)(2,1)S(1)}) custom-call(f32[2,64,128]{2,1,0:T(8,128)S(1)} %bitcast.16, f32[2,64,128]{2,1,0:T(8,128)S(1)} %bitcast.18, f32[2,128]{1,0:T(2,128)S(1)} %copy-done.8, bf16[2,128,16,128]{3,2,1,0:T(8,128)(2,1)S(1)} %copy-done.5), custom_call_target="tpu_custom_call" | custom-call | flops 40000000000 | tf_op jit(solution)/shard_map/pallas_call | solution.py:240
  15.1 1.4 %collective-permute-done.4.refs_2_ = bf16[4,4224]{1,0:T(4,128)(2,1)S(1)} collective-permute-done((bf16[4,4224]{1,0:T(4,128)(2,1)S(1)}, bf16[4,4224]{1,0:T(4,128)(2,1)S(1)}, u32[]{:S(2)}, u32[]{:S(2)}) %collective-permute-start.4) | collective-permute-done | bytes 33824 | tf_op jit(solution)/shard_map/ppermute | solution.py:86
  16.5 1.0 %collective-permute-done.5.refs_3_ = bf16[4,4224]{1,0:T(4,128)(2,1)S(1)} collective-permute-done((bf16[4,4224]{1,0:T(4,128)(2,1)S(1)}, bf16[4,4224]{1,0:T(4,128)(2,1)S(1)}, u32[]{:S(2)}, u32[]{:S(2)}) %collective-permute-start.5) | collective-permute-done | bytes 33824 | tf_op jit(solution)/shard_map/ppermute | solution.py:86
  17.5 2.0 %shard_map.143 = (bf16[4,2048]{1,0:T(4,128)(2,1)S(1)}, f32[128,128]{1,0:T(8,128)S(1)}) custom-call(bf16[4,4224]{1,0:T(4,128)(2,1)S(1)} %get-tuple-element.32.refs_0_, bf16[4,4224]{1,0:T(4,128)(2,1)S(1)} %collective-permute-done.3.refs_1_, bf16[4,4224]{1,0:T(4,128)(2,1)S(1)} %collective-permute-done.4.refs_2_, ...), custom_call_target="tpu_custom_call" | custom-call | tf_op jit(solution)/shard_map/pallas_call | solution.py:240
  19.5 0.7 %collective-permute-start.8 = (bf16[4,2048]{1,0:T(4,128)(2,1)S(1)}, bf16[4,2048]{1,0:T(4,128)(2,1)S(1)}, u32[]{:S(2)}, u32[]{:S(2)}) collective-permute-start(bf16[4,2048]{1,0:T(4,128)(2,1)S(1)} %get-tuple-element.40.refs_0_), channel_id=1, source_target_pairs={{0,3},{1,2},{2,1},{3,0},{4,7},{5,6},{6,5},{7,4},{8,11},{9,10},{10,... | collective-permute-start | bytes 49160 | tf_op jit(solution)/shard_map/ppermute | solution.py:86
  20.2 1.2 %collective-permute-start.7 = (bf16[4,2048]{1,0:T(4,128)(2,1)S(1)}, bf16[4,2048]{1,0:T(4,128)(2,1)S(1)}, u32[]{:S(2)}, u32[]{:S(2)}) collective-permute-start(bf16[4,2048]{1,0:T(4,128)(2,1)S(1)} %get-tuple-element.40.refs_0_), channel_id=1, source_target_pairs={{0,2},{1,3},{2,0},{3,1},{4,6},{5,7},{6,4},{7,5},{8,10},{9,11},{10,... | collective-permute-start | bytes 49160 | tf_op jit(solution)/shard_map/ppermute | solution.py:86
  21.3 0.1 collective-permute-start.6
  21.4 1.3 %collective-permute-done.8.refs_3_ = bf16[4,2048]{1,0:T(4,128)(2,1)S(1)} collective-permute-done((bf16[4,2048]{1,0:T(4,128)(2,1)S(1)}, bf16[4,2048]{1,0:T(4,128)(2,1)S(1)}, u32[]{:S(2)}, u32[]{:S(2)}) %collective-permute-start.8) | collective-permute-done | bytes 16416 | tf_op jit(solution)/shard_map/ppermute | solution.py:86
  22.7 1.2 %collective-permute-done.7.refs_2_ = bf16[4,2048]{1,0:T(4,128)(2,1)S(1)} collective-permute-done((bf16[4,2048]{1,0:T(4,128)(2,1)S(1)}, bf16[4,2048]{1,0:T(4,128)(2,1)S(1)}, u32[]{:S(2)}, u32[]{:S(2)}) %collective-permute-start.7) | collective-permute-done | bytes 16416 | tf_op jit(solution)/shard_map/ppermute | solution.py:86
  23.9 0.6 %shard_map.144.refs_0_ = bf16[16,1024]{1,0:T(8,128)(2,1)S(1)} custom-call(bf16[4,2048]{1,0:T(4,128)(2,1)S(1)} %get-tuple-element.40.refs_0_, bf16[4,2048]{1,0:T(4,128)(2,1)S(1)} %collective-permute-done.6.refs_1_, bf16[4,2048]{1,0:T(4,128)(2,1)S(1)} %collective-permute-done.7.refs_2_, bf16[4,2048]{1,0:T(4,128)(2,1)S(1)} %collective-permute-done.8.refs_3_, ...), custom_call_target="tpu_custom_call" | custom-call | tf_op jit(solution)/shard_map/pallas_call | solution.py:240
  24.6 1.5 %collective-permute-start.11 = (bf16[16,1024]{1,0:T(8,128)(2,1)S(1)}, bf16[16,1024]{1,0:T(8,128)(2,1)S(1)}, u32[]{:S(2)}, u32[]{:S(2)}) collective-permute-start(bf16[16,1024]{1,0:T(8,128)(2,1)S(1)} %shard_map.144.refs_0_), channel_id=1, source_target_pairs={{0,12},{4,8},{8,4},{12,0},{1,13},{5,9},{9,5},{13,1},{2,14},{6,10},... | collective-permute-start | bytes 98312 | tf_op jit(solution)/shard_map/ppermute | solution.py:86
  26.1 0.6 %collective-permute-start.10 = (bf16[16,1024]{1,0:T(8,128)(2,1)S(1)}, bf16[16,1024]{1,0:T(8,128)(2,1)S(1)}, u32[]{:S(2)}, u32[]{:S(2)}) collective-permute-start(bf16[16,1024]{1,0:T(8,128)(2,1)S(1)} %shard_map.144.refs_0_), channel_id=1, source_target_pairs={{0,8},{4,12},{8,0},{12,4},{1,9},{5,13},{9,1},{13,5},{2,10},{6,14},... | collective-permute-start | bytes 98312 | tf_op jit(solution)/shard_map/ppermute | solution.py:86
  26.6 2.4 %collective-permute-start.9 = (bf16[16,1024]{1,0:T(8,128)(2,1)S(1)}, bf16[16,1024]{1,0:T(8,128)(2,1)S(1)}, u32[]{:S(2)}, u32[]{:S(2)}) collective-permute-start(bf16[16,1024]{1,0:T(8,128)(2,1)S(1)} %shard_map.144.refs_0_), channel_id=1, source_target_pairs={{0,4},{4,0},{8,12},{12,8},{1,5},{5,1},{9,13},{13,9},{2,6},{6,2},{1... | collective-permute-start | bytes 98312 | tf_op jit(solution)/shard_map/ppermute | solution.py:86
  29.0 1.3 %collective-permute-done.11.refs_3_ = bf16[16,1024]{1,0:T(8,128)(2,1)S(1)} collective-permute-done((bf16[16,1024]{1,0:T(8,128)(2,1)S(1)}, bf16[16,1024]{1,0:T(8,128)(2,1)S(1)}, u32[]{:S(2)}, u32[]{:S(2)}) %collective-permute-start.11) | collective-permute-done | bytes 32800 | tf_op jit(solution)/shard_map/ppermute | solution.py:86
  30.3 0.5 collective-permute-done.10.refs_2_
  30.9 0.4 collective-permute-done.9.refs_1_
  31.2 1.2 %shard_map.145 = (bf16[4,4224]{1,0:T(4,128)(2,1)S(1)}, bf16[4,4224]{1,0:T(4,128)(2,1)S(1)}, bf16[4,4224]{1,0:T(4,128)(2,1)S(1)}, bf16[4,4224]{1,0:T(4,128)(2,1)S(1)}, f32[16,1024]{1,0:T(8,128)S(1)}) custom-call(f32[16,1024]{1,0:T(8,128)S(1)} %get-tuple-element.31.base_ref, bf16[16,1024]{1,0:T(8,128)(2,1)S(1)} %shard_map.144.refs_0_, ...), custom_call_target="tpu_custom_call" | custom-call | tf_op jit(solution)/shard_map/pallas_call | solution.py:240
  32.4 1.2 %collective-permute-start.13 = (bf16[4,4224]{1,0:T(4,128)(2,1)S(1)}, bf16[4,4224]{1,0:T(4,128)(2,1)S(1)}, u32[]{:S(2)}, u32[]{:S(2)}) collective-permute-start(bf16[4,4224]{1,0:T(4,128)(2,1)S(1)} %get-tuple-element.43), channel_id=1, source_target_pairs={{0,2},{1,3},{2,0},{3,1},{4,6},{5,7},{6,4},{7,5},{8,10},{9,11},{10,... | collective-permute-start | bytes 101384 | tf_op jit(solution)/shard_map/ppermute | solution.py:86
  33.6 0.7 %collective-permute-start.14 = (bf16[4,4224]{1,0:T(4,128)(2,1)S(1)}, bf16[4,4224]{1,0:T(4,128)(2,1)S(1)}, u32[]{:S(2)}, u32[]{:S(2)}) collective-permute-start(bf16[4,4224]{1,0:T(4,128)(2,1)S(1)} %get-tuple-element.44), channel_id=1, source_target_pairs={{0,3},{1,2},{2,1},{3,0},{4,7},{5,6},{6,5},{7,4},{8,11},{9,10},{10,... | collective-permute-start | bytes 101384 | tf_op jit(solution)/shard_map/ppermute | solution.py:86
  34.3 0.6 %shard_map.146 = (f32[128,128]{1,0:T(8,128)S(1)}, f32[128,128]{1,0:T(8,128)S(1)}, bf16[16,256,128]{2,1,0:T(8,128)(2,1)S(1)}) custom-call(f32[2,64,128]{2,1,0:T(8,128)S(1)} %bitcast.17, f32[2,64,128]{2,1,0:T(8,128)S(1)} %bitcast.19, f32[2,128]{1,0:T(2,128)S(1)} %copy-done.8, bf16[2,128,16,128]{3,2,1,0:T(8,128)(2,1)S(1)} %copy-done.5, ...), custom_call_target="tpu_custom_call" | custom-call | flops 40000000000 | tf_op jit(solution)/shard_map/pallas_call | solution.py:240
  35.0 1.5 %collective-permute-done.13.refs_2_ = bf16[4,4224]{1,0:T(4,128)(2,1)S(1)} collective-permute-done((bf16[4,4224]{1,0:T(4,128)(2,1)S(1)}, bf16[4,4224]{1,0:T(4,128)(2,1)S(1)}, u32[]{:S(2)}, u32[]{:S(2)}) %collective-permute-start.13) | collective-permute-done | bytes 33824 | tf_op jit(solution)/shard_map/ppermute | solution.py:86
  36.4 0.6 %collective-permute-done.14.refs_3_ = bf16[4,4224]{1,0:T(4,128)(2,1)S(1)} collective-permute-done((bf16[4,4224]{1,0:T(4,128)(2,1)S(1)}, bf16[4,4224]{1,0:T(4,128)(2,1)S(1)}, u32[]{:S(2)}, u32[]{:S(2)}) %collective-permute-start.14) | collective-permute-done | bytes 33824 | tf_op jit(solution)/shard_map/ppermute | solution.py:86
  37.0 2.0 %shard_map.147 = (bf16[4,2048]{1,0:T(4,128)(2,1)S(1)}, f32[128,128]{1,0:T(8,128)S(1)}) custom-call(bf16[4,4224]{1,0:T(4,128)(2,1)S(1)} %get-tuple-element.41.refs_0_, bf16[4,4224]{1,0:T(4,128)(2,1)S(1)} %collective-permute-done.12.refs_1_, bf16[4,4224]{1,0:T(4,128)(2,1)S(1)} %collective-permute-done.13.refs_2_, ...), custom_call_target="tpu_custom_call" | custom-call | tf_op jit(solution)/shard_map/pallas_call | solution.py:240
  39.0 0.8 %collective-permute-start.17 = (bf16[4,2048]{1,0:T(4,128)(2,1)S(1)}, bf16[4,2048]{1,0:T(4,128)(2,1)S(1)}, u32[]{:S(2)}, u32[]{:S(2)}) collective-permute-start(bf16[4,2048]{1,0:T(4,128)(2,1)S(1)} %get-tuple-element.48.refs_0_), channel_id=1, source_target_pairs={{0,3},{1,2},{2,1},{3,0},{4,7},{5,6},{6,5},{7,4},{8,11},{9,10},{10,... | collective-permute-start | bytes 49160 | tf_op jit(solution)/shard_map/ppermute | solution.py:86
  39.8 1.1 %collective-permute-start.16 = (bf16[4,2048]{1,0:T(4,128)(2,1)S(1)}, bf16[4,2048]{1,0:T(4,128)(2,1)S(1)}, u32[]{:S(2)}, u32[]{:S(2)}) collective-permute-start(bf16[4,2048]{1,0:T(4,128)(2,1)S(1)} %get-tuple-element.48.refs_0_), channel_id=1, source_target_pairs={{0,2},{1,3},{2,0},{3,1},{4,6},{5,7},{6,4},{7,5},{8,10},{9,11},{10,... | collective-permute-start | bytes 49160 | tf_op jit(solution)/shard_map/ppermute | solution.py:86
  40.9 0.0 collective-permute-start.15
  40.9 1.3 %collective-permute-done.17.refs_3_ = bf16[4,2048]{1,0:T(4,128)(2,1)S(1)} collective-permute-done((bf16[4,2048]{1,0:T(4,128)(2,1)S(1)}, bf16[4,2048]{1,0:T(4,128)(2,1)S(1)}, u32[]{:S(2)}, u32[]{:S(2)}) %collective-permute-start.17) | collective-permute-done | bytes 16416 | tf_op jit(solution)/shard_map/ppermute | solution.py:86
  42.2 1.3 %collective-permute-done.16.refs_2_ = bf16[4,2048]{1,0:T(4,128)(2,1)S(1)} collective-permute-done((bf16[4,2048]{1,0:T(4,128)(2,1)S(1)}, bf16[4,2048]{1,0:T(4,128)(2,1)S(1)}, u32[]{:S(2)}, u32[]{:S(2)}) %collective-permute-start.16) | collective-permute-done | bytes 16416 | tf_op jit(solution)/shard_map/ppermute | solution.py:86
  43.5 0.7 %shard_map.148 = (f32[4,1024]{1,0:T(4,128)S(1)}, bf16[4,1024]{1,0:T(4,128)(2,1)S(1)}, bf16[4,1024]{1,0:T(4,128)(2,1)S(1)}, bf16[4,1024]{1,0:T(4,128)(2,1)S(1)}) custom-call(bf16[4,2048]{1,0:T(4,128)(2,1)S(1)} %get-tuple-element.48.refs_0_, bf16[4,2048]{1,0:T(4,128)(2,1)S(1)} %collective-permute-done.15.refs_1_, ...), custom_call_target="tpu_custom_call" | custom-call | tf_op jit(solution)/shard_map/pallas_call | solution.py:240
  44.2 1.7 %collective-permute-start.18 = (bf16[4,1024]{1,0:T(4,128)(2,1)S(1)}, bf16[4,1024]{1,0:T(4,128)(2,1)S(1)}, u32[]{:S(2)}, u32[]{:S(2)}) collective-permute-start(bf16[4,1024]{1,0:T(4,128)(2,1)S(1)} %get-tuple-element.51), channel_id=1, source_target_pairs={{0,4},{4,0},{8,12},{12,8},{1,5},{5,1},{9,13},{13,9},{2,6},{6,2},{1... | collective-permute-start | bytes 24584 | tf_op jit(solution)/shard_map/ppermute | solution.py:86
  45.9 1.2 %collective-permute-start.19 = (bf16[4,1024]{1,0:T(4,128)(2,1)S(1)}, bf16[4,1024]{1,0:T(4,128)(2,1)S(1)}, u32[]{:S(2)}, u32[]{:S(2)}) collective-permute-start(bf16[4,1024]{1,0:T(4,128)(2,1)S(1)} %get-tuple-element.52), channel_id=1, source_target_pairs={{0,8},{4,12},{8,0},{12,4},{1,9},{5,13},{9,1},{13,5},{2,10},{6,14},... | collective-permute-start | bytes 24584 | tf_op jit(solution)/shard_map/ppermute | solution.py:86
  47.2 1.4 %collective-permute-start.20 = (bf16[4,1024]{1,0:T(4,128)(2,1)S(1)}, bf16[4,1024]{1,0:T(4,128)(2,1)S(1)}, u32[]{:S(2)}, u32[]{:S(2)}) collective-permute-start(bf16[4,1024]{1,0:T(4,128)(2,1)S(1)} %get-tuple-element.53), channel_id=1, source_target_pairs={{0,12},{4,8},{8,4},{12,0},{1,13},{5,9},{9,5},{13,1},{2,14},{6,10},... | collective-permute-start | bytes 24584 | tf_op jit(solution)/shard_map/ppermute | solution.py:86
  48.6 0.7 %maximum_bitcast_fusion = f32[2,1,128,128]{3,2,1,0:T(8,128)} fusion(f32[1,128,128]{2,1,0:T(8,128)S(1)} %bitcast.15, f32[1,128,128]{2,1,0:T(8,128)S(1)} %bitcast.14), kind=kLoop, calls=%fused_computation | loop fusion | flops 32768 | bytes 262144
  49.3 1.2 %collective-permute-done.19.refs_1_ = bf16[4,1024]{1,0:T(4,128)(2,1)S(1)} collective-permute-done((bf16[4,1024]{1,0:T(4,128)(2,1)S(1)}, bf16[4,1024]{1,0:T(4,128)(2,1)S(1)}, u32[]{:S(2)}, u32[]{:S(2)}) %collective-permute-start.19) | collective-permute-done | bytes 8224 | tf_op jit(solution)/shard_map/ppermute | solution.py:86
  50.5 2.1 %collective-permute-done.20.refs_2_ = bf16[4,1024]{1,0:T(4,128)(2,1)S(1)} collective-permute-done((bf16[4,1024]{1,0:T(4,128)(2,1)S(1)}, bf16[4,1024]{1,0:T(4,128)(2,1)S(1)}, u32[]{:S(2)}, u32[]{:S(2)}) %collective-permute-start.20) | collective-permute-done | bytes 8224 | tf_op jit(solution)/shard_map/ppermute | solution.py:86
  52.6 0.6 %shard_map.149 = bf16[1,4,1024]{2,1,0:T(4,128)(2,1)} custom-call(f32[4,1024]{1,0:T(4,128)S(1)} %get-tuple-element.50.own_ref, bf16[4,1024]{1,0:T(4,128)(2,1)S(1)} %collective-permute-done.18.refs_0_, bf16[4,1024]{1,0:T(4,128)(2,1)S(1)} %collective-permute-done.19.refs_1_, bf16[4,1024]{1,0:T(4,128)(2,1)S(1)} %collective-permute-done.20.refs_2_), custom_call_target="tpu_custom_call" | custom-call | tf_op jit(solution)/shard_map/pallas_call | solution.py:240
  (28 shorter events, 0.1 us)
Async XLA Ops:
  0.6 10.6 %copy-start = (bf16[2,1024,2048]{2,1,0:T(8,128)(2,1)S(1)}, bf16[2,1024,2048]{2,1,0:T(8,128)(2,1)}, u32[]{:S(2)}) copy-start(bf16[2,1024,2048]{2,1,0:T(8,128)(2,1)} %refs_5_.3) | copy-start | bytes 25165828
  0.6 10.6 %copy-start.1 = (bf16[2,1024,2048]{2,1,0:T(8,128)(2,1)S(1)}, bf16[2,1024,2048]{2,1,0:T(8,128)(2,1)}, u32[]{:S(2)}) copy-start(bf16[2,1024,2048]{2,1,0:T(8,128)(2,1)} %refs_6_.3) | copy-start | bytes 25165828
  1.5 6.8 %collective-permute-start.2 = (bf16[4,1024]{1,0:T(4,128)(2,1)S(1)}, bf16[4,1024]{1,0:T(4,128)(2,1)S(1)}, u32[]{:S(2)}, u32[]{:S(2)}) collective-permute-start(bf16[4,1024]{1,0:T(4,128)(2,1)S(1)} %get-tuple-element.29.refs_0_), channel_id=1, source_target_pairs={{0,12},{4,8},{8,4},{12,0},{1,13},{5,9},{9,5},{13,1},{2,14},{6,10},... | collective-permute-start | bytes 24584 | tf_op jit(solution)/shard_map/ppermute | solution.py:86
  6.7 4.5 %collective-permute-start.1 = (bf16[4,1024]{1,0:T(4,128)(2,1)S(1)}, bf16[4,1024]{1,0:T(4,128)(2,1)S(1)}, u32[]{:S(2)}, u32[]{:S(2)}) collective-permute-start(bf16[4,1024]{1,0:T(4,128)(2,1)S(1)} %get-tuple-element.29.refs_0_), channel_id=1, source_target_pairs={{0,8},{4,12},{8,0},{12,4},{1,9},{5,13},{9,1},{13,5},{2,10},{6,14},... | collective-permute-start | bytes 24584 | tf_op jit(solution)/shard_map/ppermute | solution.py:86
  6.7 4.5 %collective-permute-start = (bf16[4,1024]{1,0:T(4,128)(2,1)S(1)}, bf16[4,1024]{1,0:T(4,128)(2,1)S(1)}, u32[]{:S(2)}, u32[]{:S(2)}) collective-permute-start(bf16[4,1024]{1,0:T(4,128)(2,1)S(1)} %get-tuple-element.29.refs_0_), channel_id=1, source_target_pairs={{0,4},{4,0},{8,12},{12,8},{1,5},{5,1},{9,13},{13,9},{2,6},{6,2},{1... | collective-permute-start | bytes 24584 | tf_op jit(solution)/shard_map/ppermute | solution.py:86
  11.3 3.1 %copy-start.5 = (bf16[2,128,16,128]{3,2,1,0:T(8,128)(2,1)S(1)}, bf16[2,128,16,128]{3,2,1,0:T(8,128)(2,1)}, u32[]{:S(2)}) copy-start(bf16[2,128,16,128]{3,2,1,0:T(8,128)(2,1)} %map_ref.3) | copy-start | bytes 3145732
  11.3 3.1 %copy-start.6 = (f32[2,128,64]{1,2,0:T(8,128)S(1)}, f32[2,128,64]{1,2,0:T(8,128)}, u32[]{:S(2)}) copy-start(f32[2,128,64]{1,2,0:T(8,128)} %param.18) | copy-start | bytes 196612
  11.3 3.1 %copy-start.7 = (f32[2,128,64]{1,2,0:T(8,128)S(1)}, f32[2,128,64]{1,2,0:T(8,128)}, u32[]{:S(2)}) copy-start(f32[2,128,64]{1,2,0:T(8,128)} %param.19) | copy-start | bytes 196612
  11.3 3.1 %copy-start.8 = (f32[2,128]{1,0:T(2,128)S(1)}, f32[2,128]{1,0:T(2,128)}, u32[]{:S(2)}) copy-start(f32[2,128]{1,0:T(2,128)} %log_step_ref.3) | copy-start | bytes 3076
  11.3 12.6 %slice-start = ((s8[8388608]{0:T(1024)(128)(4,1)}), s8[4194304]{0:T(1024)(128)(4,1)S(1)}, s32[]{:S(2)}) async-start(s8[8388608]{0:T(1024)(128)(4,1)} %bitcast.10), calls=%async_computation | async-start | bytes 8388608
  12.5 2.6 %collective-permute-start.3 = (bf16[4,4224]{1,0:T(4,128)(2,1)S(1)}, bf16[4,4224]{1,0:T(4,128)(2,1)S(1)}, u32[]{:S(2)}, u32[]{:S(2)}) collective-permute-start(bf16[4,4224]{1,0:T(4,128)(2,1)S(1)} %get-tuple-element.33), channel_id=1, source_target_pairs={{0,1},{1,0},{2,3},{3,2},{4,5},{5,4},{6,7},{7,6},{8,9},{9,8},{10,11... | collective-permute-start | bytes 101384 | tf_op jit(solution)/shard_map/ppermute | solution.py:86
  12.5 4.0 %collective-permute-start.4 = (bf16[4,4224]{1,0:T(4,128)(2,1)S(1)}, bf16[4,4224]{1,0:T(4,128)(2,1)S(1)}, u32[]{:S(2)}, u32[]{:S(2)}) collective-permute-start(bf16[4,4224]{1,0:T(4,128)(2,1)S(1)} %get-tuple-element.34), channel_id=1, source_target_pairs={{0,2},{1,3},{2,0},{3,1},{4,6},{5,7},{6,4},{7,5},{8,10},{9,11},{10,... | collective-permute-start | bytes 101384 | tf_op jit(solution)/shard_map/ppermute | solution.py:86
  14.1 3.4 %collective-permute-start.5 = (bf16[4,4224]{1,0:T(4,128)(2,1)S(1)}, bf16[4,4224]{1,0:T(4,128)(2,1)S(1)}, u32[]{:S(2)}, u32[]{:S(2)}) collective-permute-start(bf16[4,4224]{1,0:T(4,128)(2,1)S(1)} %get-tuple-element.35), channel_id=1, source_target_pairs={{0,3},{1,2},{2,1},{3,0},{4,7},{5,6},{6,5},{7,4},{8,11},{9,10},{10,... | collective-permute-start | bytes 101384 | tf_op jit(solution)/shard_map/ppermute | solution.py:86
  14.4 3.1 %copy-start.2 = (bf16[2,128,16,128]{3,2,1,0:T(8,128)(2,1)S(1)}, bf16[2,128,16,128]{3,2,1,0:T(8,128)(2,1)}, u32[]{:S(2)}) copy-start(bf16[2,128,16,128]{3,2,1,0:T(8,128)(2,1)} %param.22) | copy-start | bytes 3145732
  14.4 3.1 %copy-start.3 = (f32[2,1,128,128]{3,2,1,0:T(8,128)S(1)}, f32[2,1,128,128]{3,2,1,0:T(8,128)}, u32[]{:S(2)}) copy-start(f32[2,1,128,128]{3,2,1,0:T(8,128)} %refs_10_.3) | copy-start | bytes 393220
  14.4 3.0 %copy-start.4 = (bf16[2,2048]{1,0:T(2,128)(2,1)S(1)}, bf16[2,2048]{1,0:T(2,128)(2,1)}, u32[]{:S(2)}) copy-start(bf16[2,2048]{1,0:T(2,128)(2,1)} %refs_9_.3) | copy-start | bytes 24580
  14.4 9.5 %slice-start.1 = ((s8[8388608]{0:T(1024)(128)(4,1)}), s8[4194304]{0:T(1024)(128)(4,1)S(1)}, s32[]{:S(2)}) async-start(s8[8388608]{0:T(1024)(128)(4,1)} %bitcast.10), calls=%async_computation.1 | async-start | bytes 8388608
  19.5 3.2 %collective-permute-start.8 = (bf16[4,2048]{1,0:T(4,128)(2,1)S(1)}, bf16[4,2048]{1,0:T(4,128)(2,1)S(1)}, u32[]{:S(2)}, u32[]{:S(2)}) collective-permute-start(bf16[4,2048]{1,0:T(4,128)(2,1)S(1)} %get-tuple-element.40.refs_0_), channel_id=1, source_target_pairs={{0,3},{1,2},{2,1},{3,0},{4,7},{5,6},{6,5},{7,4},{8,11},{9,10},{10,... | collective-permute-start | bytes 49160 | tf_op jit(solution)/shard_map/ppermute | solution.py:86
  20.2 3.7 %collective-permute-start.7 = (bf16[4,2048]{1,0:T(4,128)(2,1)S(1)}, bf16[4,2048]{1,0:T(4,128)(2,1)S(1)}, u32[]{:S(2)}, u32[]{:S(2)}) collective-permute-start(bf16[4,2048]{1,0:T(4,128)(2,1)S(1)} %get-tuple-element.40.refs_0_), channel_id=1, source_target_pairs={{0,2},{1,3},{2,0},{3,1},{4,6},{5,7},{6,4},{7,5},{8,10},{9,11},{10,... | collective-permute-start | bytes 49160 | tf_op jit(solution)/shard_map/ppermute | solution.py:86
  21.3 2.6 %collective-permute-start.6 = (bf16[4,2048]{1,0:T(4,128)(2,1)S(1)}, bf16[4,2048]{1,0:T(4,128)(2,1)S(1)}, u32[]{:S(2)}, u32[]{:S(2)}) collective-permute-start(bf16[4,2048]{1,0:T(4,128)(2,1)S(1)} %get-tuple-element.40.refs_0_), channel_id=1, source_target_pairs={{0,1},{1,0},{2,3},{3,2},{4,5},{5,4},{6,7},{7,6},{8,9},{9,8},{10,11... | collective-permute-start | bytes 49160 | tf_op jit(solution)/shard_map/ppermute | solution.py:86
  24.6 5.7 %collective-permute-start.11 = (bf16[16,1024]{1,0:T(8,128)(2,1)S(1)}, bf16[16,1024]{1,0:T(8,128)(2,1)S(1)}, u32[]{:S(2)}, u32[]{:S(2)}) collective-permute-start(bf16[16,1024]{1,0:T(8,128)(2,1)S(1)} %shard_map.144.refs_0_), channel_id=1, source_target_pairs={{0,12},{4,8},{8,4},{12,0},{1,13},{5,9},{9,5},{13,1},{2,14},{6,10},... | collective-permute-start | bytes 98312 | tf_op jit(solution)/shard_map/ppermute | solution.py:86
  26.1 4.8 %collective-permute-start.10 = (bf16[16,1024]{1,0:T(8,128)(2,1)S(1)}, bf16[16,1024]{1,0:T(8,128)(2,1)S(1)}, u32[]{:S(2)}, u32[]{:S(2)}) collective-permute-start(bf16[16,1024]{1,0:T(8,128)(2,1)S(1)} %shard_map.144.refs_0_), channel_id=1, source_target_pairs={{0,8},{4,12},{8,0},{12,4},{1,9},{5,13},{9,1},{13,5},{2,10},{6,14},... | collective-permute-start | bytes 98312 | tf_op jit(solution)/shard_map/ppermute | solution.py:86
  26.6 4.6 %collective-permute-start.9 = (bf16[16,1024]{1,0:T(8,128)(2,1)S(1)}, bf16[16,1024]{1,0:T(8,128)(2,1)S(1)}, u32[]{:S(2)}, u32[]{:S(2)}) collective-permute-start(bf16[16,1024]{1,0:T(8,128)(2,1)S(1)} %shard_map.144.refs_0_), channel_id=1, source_target_pairs={{0,4},{4,0},{8,12},{12,8},{1,5},{5,1},{9,13},{13,9},{2,6},{6,2},{1... | collective-permute-start | bytes 98312 | tf_op jit(solution)/shard_map/ppermute | solution.py:86
  32.4 2.5 %collective-permute-start.12 = (bf16[4,4224]{1,0:T(4,128)(2,1)S(1)}, bf16[4,4224]{1,0:T(4,128)(2,1)S(1)}, u32[]{:S(2)}, u32[]{:S(2)}) collective-permute-start(bf16[4,4224]{1,0:T(4,128)(2,1)S(1)} %get-tuple-element.42), channel_id=1, source_target_pairs={{0,1},{1,0},{2,3},{3,2},{4,5},{5,4},{6,7},{7,6},{8,9},{9,8},{10,11... | collective-permute-start | bytes 101384 | tf_op jit(solution)/shard_map/ppermute | solution.py:86
  32.4 4.0 %collective-permute-start.13 = (bf16[4,4224]{1,0:T(4,128)(2,1)S(1)}, bf16[4,4224]{1,0:T(4,128)(2,1)S(1)}, u32[]{:S(2)}, u32[]{:S(2)}) collective-permute-start(bf16[4,4224]{1,0:T(4,128)(2,1)S(1)} %get-tuple-element.43), channel_id=1, source_target_pairs={{0,2},{1,3},{2,0},{3,1},{4,6},{5,7},{6,4},{7,5},{8,10},{9,11},{10,... | collective-permute-start | bytes 101384 | tf_op jit(solution)/shard_map/ppermute | solution.py:86
  33.6 3.4 %collective-permute-start.14 = (bf16[4,4224]{1,0:T(4,128)(2,1)S(1)}, bf16[4,4224]{1,0:T(4,128)(2,1)S(1)}, u32[]{:S(2)}, u32[]{:S(2)}) collective-permute-start(bf16[4,4224]{1,0:T(4,128)(2,1)S(1)} %get-tuple-element.44), channel_id=1, source_target_pairs={{0,3},{1,2},{2,1},{3,0},{4,7},{5,6},{6,5},{7,4},{8,11},{9,10},{10,... | collective-permute-start | bytes 101384 | tf_op jit(solution)/shard_map/ppermute | solution.py:86
  39.0 3.2 %collective-permute-start.17 = (bf16[4,2048]{1,0:T(4,128)(2,1)S(1)}, bf16[4,2048]{1,0:T(4,128)(2,1)S(1)}, u32[]{:S(2)}, u32[]{:S(2)}) collective-permute-start(bf16[4,2048]{1,0:T(4,128)(2,1)S(1)} %get-tuple-element.48.refs_0_), channel_id=1, source_target_pairs={{0,3},{1,2},{2,1},{3,0},{4,7},{5,6},{6,5},{7,4},{8,11},{9,10},{10,... | collective-permute-start | bytes 49160 | tf_op jit(solution)/shard_map/ppermute | solution.py:86
  39.8 3.7 %collective-permute-start.16 = (bf16[4,2048]{1,0:T(4,128)(2,1)S(1)}, bf16[4,2048]{1,0:T(4,128)(2,1)S(1)}, u32[]{:S(2)}, u32[]{:S(2)}) collective-permute-start(bf16[4,2048]{1,0:T(4,128)(2,1)S(1)} %get-tuple-element.48.refs_0_), channel_id=1, source_target_pairs={{0,2},{1,3},{2,0},{3,1},{4,6},{5,7},{6,4},{7,5},{8,10},{9,11},{10,... | collective-permute-start | bytes 49160 | tf_op jit(solution)/shard_map/ppermute | solution.py:86
  40.9 2.7 %collective-permute-start.15 = (bf16[4,2048]{1,0:T(4,128)(2,1)S(1)}, bf16[4,2048]{1,0:T(4,128)(2,1)S(1)}, u32[]{:S(2)}, u32[]{:S(2)}) collective-permute-start(bf16[4,2048]{1,0:T(4,128)(2,1)S(1)} %get-tuple-element.48.refs_0_), channel_id=1, source_target_pairs={{0,1},{1,0},{2,3},{3,2},{4,5},{5,4},{6,7},{7,6},{8,9},{9,8},{10,11... | collective-permute-start | bytes 49160 | tf_op jit(solution)/shard_map/ppermute | solution.py:86
  44.2 5.1 %collective-permute-start.18 = (bf16[4,1024]{1,0:T(4,128)(2,1)S(1)}, bf16[4,1024]{1,0:T(4,128)(2,1)S(1)}, u32[]{:S(2)}, u32[]{:S(2)}) collective-permute-start(bf16[4,1024]{1,0:T(4,128)(2,1)S(1)} %get-tuple-element.51), channel_id=1, source_target_pairs={{0,4},{4,0},{8,12},{12,8},{1,5},{5,1},{9,13},{13,9},{2,6},{6,2},{1... | collective-permute-start | bytes 24584 | tf_op jit(solution)/shard_map/ppermute | solution.py:86
  45.9 4.5 %collective-permute-start.19 = (bf16[4,1024]{1,0:T(4,128)(2,1)S(1)}, bf16[4,1024]{1,0:T(4,128)(2,1)S(1)}, u32[]{:S(2)}, u32[]{:S(2)}) collective-permute-start(bf16[4,1024]{1,0:T(4,128)(2,1)S(1)} %get-tuple-element.52), channel_id=1, source_target_pairs={{0,8},{4,12},{8,0},{12,4},{1,9},{5,13},{9,1},{13,5},{2,10},{6,14},... | collective-permute-start | bytes 24584 | tf_op jit(solution)/shard_map/ppermute | solution.py:86
  47.2 5.4 %collective-permute-start.20 = (bf16[4,1024]{1,0:T(4,128)(2,1)S(1)}, bf16[4,1024]{1,0:T(4,128)(2,1)S(1)}, u32[]{:S(2)}, u32[]{:S(2)}) collective-permute-start(bf16[4,1024]{1,0:T(4,128)(2,1)S(1)} %get-tuple-element.53), channel_id=1, source_target_pairs={{0,12},{4,8},{8,4},{12,0},{1,13},{5,9},{9,5},{13,1},{2,14},{6,10},... | collective-permute-start | bytes 24584 | tf_op jit(solution)/shard_map/ppermute | solution.py:86

commit v4 on v3

--- a/solution.py
+++ b/solution.py
@@ -279,7 +279,9 @@
         copy.wait()
 
 
-def parameter_step(decay, frequency, log_step, map_ref, real_ref, imag_ref, coupled_ref):
+def parameter_step(
+    decay, frequency, log_step, map_ref, readout_ref, real_ref, imag_ref, coupled_ref, seen_ref
+):
     half, groups = decay.shape
     step = jnp.exp(log_step)
     magnitude = jnp.exp(-decay * step)
@@ -297,6 +299,7 @@
     imag_ref[...] = across(-imag, imag)
     scale_real = across(coeff_real, coeff_real)
     scale_imag = across(-coeff_imag, coeff_imag)
+    upper = lax.broadcasted_iota(jnp.int32, (LANES, LANES), 0) < half
     for chunk in range(groups // SUBLANES):
         rows = slice(chunk * SUBLANES, (chunk + 1) * SUBLANES)
         values = map_ref[rows].astype(jnp.float32).reshape(LANES, LANES)
@@ -308,22 +311,26 @@
         high, low = halves(coupled)
         coupled_ref[chunk, :LANES] = high
         coupled_ref[chunk, LANES:] = low
-
-
-def parameter_kernel(layer, decay_ref, frequency_ref, log_step_ref, map_ref, *refs):
+        seen = jnp.transpose(readout_ref[rows].astype(jnp.float32).reshape(LANES, LANES))
+        seen_ref[chunk] = jnp.where(upper, seen, -seen).astype(jnp.bfloat16)
+
+
+def parameter_kernel(
+    layer, decay_ref, frequency_ref, log_step_ref, map_ref, readout_ref, *refs
+):
     parameter_step(
         decay_ref[layer], frequency_ref[layer], log_step_ref[layer : layer + 1],
-        map_ref.at[layer], *refs[-3:],
-    )
-
-
-def prepare(layer, decay, frequency, log_step, input_map, after=()):
+        map_ref.at[layer], readout_ref.at[layer], *refs[-4:],
+    )
+
+
+def prepare(layer, decay, frequency, log_step, input_map, readout_map, after=()):
     _, _, groups = decay.shape
     return vmem_call(
         functools.partial(parameter_kernel, layer),
         [((groups, LANES), jnp.float32)] * 2
-        + [((groups // SUBLANES, 2 * LANES, LANES), jnp.bfloat16)],
-        decay, frequency, log_step, input_map, *after,
+        + [((groups // SUBLANES, rows, LANES), jnp.bfloat16) for rows in (2 * LANES, LANES)],
+        decay, frequency, log_step, input_map, readout_map, *after,
         cost=COST,
     )
 
@@ -423,7 +430,7 @@
 
 def state_kernel(size, layer, features, *refs):
     message_refs = refs[:size]
-    live_ref, real_ref, imag_ref, coupled_ref, readout_ref, skip_ref, state_ref = refs[size:-2]
+    live_ref, real_ref, imag_ref, coupled_ref, seen_ref, skip_ref, state_ref = refs[size:-2]
     branch_ref, next_ref = refs[-2:]
     steps = message_refs[0].shape[0]
     width = branch_ref.shape[1]
@@ -434,14 +441,11 @@
     drive = (inverse * total[:, :width]).astype(jnp.bfloat16).astype(jnp.float32)
     gate = (inverse * total[:, width : 2 * width]).astype(jnp.bfloat16).astype(jnp.float32)
     live = live_ref[...]
-    lane = lax.broadcasted_iota(jnp.int32, (SUBLANES, LANES), 1)
-    row = lax.broadcasted_iota(jnp.int32, (SUBLANES, LANES), 0)
     own_group = group_mask()
     keeps = [live[t * SUBLANES : (t + 1) * SUBLANES] > 0.5 for t in range(steps)]
     live_rows = jnp.concatenate(
         [live[t * SUBLANES : t * SUBLANES + 1] for t in range(steps)], axis=0
     )
-    sign = jnp.where(lane < half, 1.0, -1.0)
     for chunk in range(width // LANES):
         at = slice(chunk * LANES, (chunk + 1) * LANES)
         groups = slice(chunk * SUBLANES, (chunk + 1) * SUBLANES)
@@ -464,14 +468,11 @@
             new_other = real * other - imag * value + turned[now]
             value = jnp.where(keeps[t], new_value, value)
             other = jnp.where(keeps[t], new_other, other)
-            history.append(value * sign)
+            history.append(value)
         next_ref[groups] = value
         high, low = halves(jnp.concatenate(history, axis=0))
-        seen = lax.dot_general(
-            jnp.concatenate([high, low], axis=0),
-            readout_ref[layer, chunk],
-            (((1,), (1,)), ((), ())),
-            preferred_element_type=jnp.float32,
+        seen = jnp.dot(
+            jnp.concatenate([high, low], axis=0), seen_ref[chunk], preferred_element_type=jnp.float32
         )
         count = steps * SUBLANES
         seen = seen[:count] + seen[count:]
@@ -546,20 +547,18 @@
     _, steps, features = tokens.shape
     inner = input_weight.shape[2]
     groups = state.shape[2]
-    chunks = groups // SUBLANES
     count = size * steps
     bf16, f32 = jnp.bfloat16, jnp.float32
     message = [((steps, 2 * inner + LANES), bf16)] * size
     rows_shape = ((count, features), f32)
-    readout = readout_map.reshape(LAYERS, chunks, LANES, LANES)
     projections = (input_weight, gate_weight)
     decay, frequency = (jnp.swapaxes(value, 1, 2) for value in (decay_rate, frequency))
-    raw = (decay, frequency, log_step, input_map)
+    raw = (decay, frequency, log_step, input_map, readout_map)
     own = tokens.reshape(steps, features)
     own, gain, live = bring_small(steps, lengths, own, norm_gain)
     pieces = swaps(own, "tp", size)
     pieces = [own] + pieces
-    real, imag, coupled = prepare(0, *raw)
+    real, imag, coupled, seen = prepare(0, *raw)
     weights = projections
     states = []
     for layer in range(LAYERS):
@@ -575,7 +574,7 @@
             functools.partial(state_kernel, size, layer, D),
             [((steps, inner), bf16), ((groups, LANES), f32)],
             *arrived, live, real, imag, coupled,
-            readout, skip_weight, state,
+            seen, skip_weight, state,
         )
         states.append(next_state)
         branches = [branch] + swaps(branch, "dp", size)
@@ -586,7 +585,7 @@
                 *branches, out_now,
             )
             pieces = [part] + swaps(part, "tp", size)
-            real, imag, coupled = prepare(layer + 1, *raw, after=[part])
+            real, imag, coupled, seen = prepare(layer + 1, *raw, after=[part])
             continue
         parts = vmem_call(
             functools.partial(last_output_kernel, size, layer),

time: 53.4 us -> 50.9 us (0.953)
  Pallas kernels: 10.5 us -> 8.14 us
    pallas_call x10, Pallas kernels: 10.5 us -> 8.14 us  [vmem_call(): pl.pallas_call(kernel, out_shape=outs, in_specs=in_specs, out_specs=[VMEM...]
  transfers between devices with their start and end apart: 21 -> 21, of which waited for: 15 -> 15; matrix products, arithmetic and copies ran while one was open for 1% -> 1% of each run, Pallas kernels for 2% -> 3%
where the time goes in v4:
time: 50.9 us; the launch traced here: 50.7 us
  starting transfers between devices  22.2 us (44%)
  waiting for transfers between devices  18.8 us (37%)
  Pallas kernels  8.14 us (16%)
  between operations  0.81 us (2%)
  other arithmetic  0.66 us (1%)
    ppermute x21, starting transfers between devices, swap(): return lax.ppermute(value, axis, [(i, i ^ distance) for i in range(size)])  22.2 us
    ppermute x21, waiting for transfers between devices, swap(): return lax.ppermute(value, axis, [(i, i ^ distance) for i in range(size)])  18.8 us
    pallas_call x10, Pallas kernels, vmem_call(): pl.pallas_call(kernel, out_shape=outs, in_specs=in_specs, out_specs=[VMEM...  8.14 us
  transfers between devices with their start and end apart: 21, of which 15 were waited for; matrix products, arithmetic and copies ran while one was open for 1% of the time, Pallas kernels for 3%

profile of v4, /device:TPU:0, one launch (start us, length us, event | category | flops | bytes accessed | tf_op | source)
XLA Modules:
  0.0 50.7 jit_solution(9462379124166371763)
XLA Ops:
  0.7 0.9 %shard_map.140 = (bf16[4,1024]{1,0:T(4,128)(2,1)S(1)}, f32[2,1024]{1,0:T(2,128)S(1)}, f32[32,128]{1,0:T(8,128)S(1)}) custom-call(s32[4]{0:T(128)} %lengths_hbm.1, bf16[4,1024]{1,0:T(4,128)(2,1)} %bitcast.17, f32[2,1024]{1,0:T(2,128)} %refs_1_.1), custom_call_target="tpu_custom_call" | custom-call | flops 40000000000 | tf_op jit(solution)/shard_map/pallas_call | solution.py:240
  1.5 5.1 %collective-permute-start.2 = (bf16[4,1024]{1,0:T(4,128)(2,1)S(1)}, bf16[4,1024]{1,0:T(4,128)(2,1)S(1)}, u32[]{:S(2)}, u32[]{:S(2)}) collective-permute-start(bf16[4,1024]{1,0:T(4,128)(2,1)S(1)} %get-tuple-element.31.refs_0_), channel_id=1, source_target_pairs={{0,12},{4,8},{8,4},{12,0},{1,13},{5,9},{9,5},{13,1},{2,14},{6,10},... | collective-permute-start | bytes 24584 | tf_op jit(solution)/shard_map/ppermute | solution.py:86
  6.7 0.6 %collective-permute-start = (bf16[4,1024]{1,0:T(4,128)(2,1)S(1)}, bf16[4,1024]{1,0:T(4,128)(2,1)S(1)}, u32[]{:S(2)}, u32[]{:S(2)}) collective-permute-start(bf16[4,1024]{1,0:T(4,128)(2,1)S(1)} %get-tuple-element.31.refs_0_), channel_id=1, source_target_pairs={{0,4},{4,0},{8,12},{12,8},{1,5},{5,1},{9,13},{13,9},{2,6},{6,2},{1... | collective-permute-start | bytes 24584 | tf_op jit(solution)/shard_map/ppermute | solution.py:86
  7.3 1.0 %collective-permute-done.2.refs_3_ = bf16[4,1024]{1,0:T(4,128)(2,1)S(1)} collective-permute-done((bf16[4,1024]{1,0:T(4,128)(2,1)S(1)}, bf16[4,1024]{1,0:T(4,128)(2,1)S(1)}, u32[]{:S(2)}, u32[]{:S(2)}) %collective-permute-start.2) | collective-permute-done | bytes 8224 | tf_op jit(solution)/shard_map/ppermute | solution.py:86
  8.3 2.9 %collective-permute-done.1.refs_2_ = bf16[4,1024]{1,0:T(4,128)(2,1)S(1)} collective-permute-done((bf16[4,1024]{1,0:T(4,128)(2,1)S(1)}, bf16[4,1024]{1,0:T(4,128)(2,1)S(1)}, u32[]{:S(2)}, u32[]{:S(2)}) %collective-permute-start.1) | collective-permute-done | bytes 8224 | tf_op jit(solution)/shard_map/ppermute | solution.py:86
  11.3 0.0 copy-start.6
  11.3 0.0 copy-start.7
  11.3 0.0 slice-start
  11.3 1.2 %shard_map.141 = (bf16[4,4224]{1,0:T(4,128)(2,1)S(1)}, bf16[4,4224]{1,0:T(4,128)(2,1)S(1)}, bf16[4,4224]{1,0:T(4,128)(2,1)S(1)}, bf16[4,4224]{1,0:T(4,128)(2,1)S(1)}, f32[16,1024]{1,0:T(8,128)S(1)}) custom-call(bf16[4,1024]{1,0:T(4,128)(2,1)S(1)} %get-tuple-element.31.refs_0_, bf16[4,1024]{1,0:T(4,128)(2,1)S(1)} %collective-permute-done.refs_1_, ...), custom_call_target="tpu_custom_call" | custom-call | tf_op jit(solution)/shard_map/pallas_call | solution.py:240
  12.5 1.6 %collective-permute-start.4 = (bf16[4,4224]{1,0:T(4,128)(2,1)S(1)}, bf16[4,4224]{1,0:T(4,128)(2,1)S(1)}, u32[]{:S(2)}, u32[]{:S(2)}) collective-permute-start(bf16[4,4224]{1,0:T(4,128)(2,1)S(1)} %get-tuple-element.36), channel_id=1, source_target_pairs={{0,2},{1,3},{2,0},{3,1},{4,6},{5,7},{6,4},{7,5},{8,10},{9,11},{10,... | collective-permute-start | bytes 101384 | tf_op jit(solution)/shard_map/ppermute | solution.py:86
  14.1 0.3 collective-permute-start.5
  14.5 0.0 slice-start.1
  14.5 0.8 %shard_map.142 = (f32[128,128]{1,0:T(8,128)S(1)}, f32[128,128]{1,0:T(8,128)S(1)}, bf16[16,256,128]{2,1,0:T(8,128)(2,1)S(1)}, bf16[16,128,128]{2,1,0:T(8,128)(2,1)S(1)}) custom-call(f32[2,64,128]{2,1,0:T(8,128)S(1)} %bitcast.13, f32[2,64,128]{2,1,0:T(8,128)S(1)} %bitcast.15, f32[2,128]{1,0:T(2,128)S(1)} %copy-done.8, bf16[2,128,16,128]{3,2,1,0:T(8,128)(2,1)S(1)} %copy-done.4, ...), custom_call_target="tpu_custom_call" | custom-call | flops 40000000000 | tf_op jit(solution)/shard_map/pallas_call | solution.py:240
  15.2 1.3 %collective-permute-done.4.refs_2_ = bf16[4,4224]{1,0:T(4,128)(2,1)S(1)} collective-permute-done((bf16[4,4224]{1,0:T(4,128)(2,1)S(1)}, bf16[4,4224]{1,0:T(4,128)(2,1)S(1)}, u32[]{:S(2)}, u32[]{:S(2)}) %collective-permute-start.4) | collective-permute-done | bytes 33824 | tf_op jit(solution)/shard_map/ppermute | solution.py:86
  16.5 1.0 %collective-permute-done.5.refs_3_ = bf16[4,4224]{1,0:T(4,128)(2,1)S(1)} collective-permute-done((bf16[4,4224]{1,0:T(4,128)(2,1)S(1)}, bf16[4,4224]{1,0:T(4,128)(2,1)S(1)}, u32[]{:S(2)}, u32[]{:S(2)}) %collective-permute-start.5) | collective-permute-done | bytes 33824 | tf_op jit(solution)/shard_map/ppermute | solution.py:86
  17.5 0.7 %shard_map.143 = (bf16[4,2048]{1,0:T(4,128)(2,1)S(1)}, f32[128,128]{1,0:T(8,128)S(1)}) custom-call(bf16[4,4224]{1,0:T(4,128)(2,1)S(1)} %get-tuple-element.34.refs_0_, bf16[4,4224]{1,0:T(4,128)(2,1)S(1)} %collective-permute-done.3.refs_1_, bf16[4,4224]{1,0:T(4,128)(2,1)S(1)} %collective-permute-done.4.refs_2_, ...), custom_call_target="tpu_custom_call" | custom-call | tf_op jit(solution)/shard_map/pallas_call | solution.py:240
  18.2 0.7 %collective-permute-start.8 = (bf16[4,2048]{1,0:T(4,128)(2,1)S(1)}, bf16[4,2048]{1,0:T(4,128)(2,1)S(1)}, u32[]{:S(2)}, u32[]{:S(2)}) collective-permute-start(bf16[4,2048]{1,0:T(4,128)(2,1)S(1)} %get-tuple-element.43.refs_0_), channel_id=1, source_target_pairs={{0,3},{1,2},{2,1},{3,0},{4,7},{5,6},{6,5},{7,4},{8,11},{9,10},{10,... | collective-permute-start | bytes 49160 | tf_op jit(solution)/shard_map/ppermute | solution.py:86
  18.9 1.2 %collective-permute-start.7 = (bf16[4,2048]{1,0:T(4,128)(2,1)S(1)}, bf16[4,2048]{1,0:T(4,128)(2,1)S(1)}, u32[]{:S(2)}, u32[]{:S(2)}) collective-permute-start(bf16[4,2048]{1,0:T(4,128)(2,1)S(1)} %get-tuple-element.43.refs_0_), channel_id=1, source_target_pairs={{0,2},{1,3},{2,0},{3,1},{4,6},{5,7},{6,4},{7,5},{8,10},{9,11},{10,... | collective-permute-start | bytes 49160 | tf_op jit(solution)/shard_map/ppermute | solution.py:86
  20.1 0.1 collective-permute-start.6
  20.1 1.3 %collective-permute-done.8.refs_3_ = bf16[4,2048]{1,0:T(4,128)(2,1)S(1)} collective-permute-done((bf16[4,2048]{1,0:T(4,128)(2,1)S(1)}, bf16[4,2048]{1,0:T(4,128)(2,1)S(1)}, u32[]{:S(2)}, u32[]{:S(2)}) %collective-permute-start.8) | collective-permute-done | bytes 16416 | tf_op jit(solution)/shard_map/ppermute | solution.py:86
  21.4 1.2 %collective-permute-done.7.refs_2_ = bf16[4,2048]{1,0:T(4,128)(2,1)S(1)} collective-permute-done((bf16[4,2048]{1,0:T(4,128)(2,1)S(1)}, bf16[4,2048]{1,0:T(4,128)(2,1)S(1)}, u32[]{:S(2)}, u32[]{:S(2)}) %collective-permute-start.7) | collective-permute-done | bytes 16416 | tf_op jit(solution)/shard_map/ppermute | solution.py:86
  22.7 0.6 %shard_map.144.refs_0_ = bf16[16,1024]{1,0:T(8,128)(2,1)S(1)} custom-call(bf16[4,2048]{1,0:T(4,128)(2,1)S(1)} %get-tuple-element.43.refs_0_, bf16[4,2048]{1,0:T(4,128)(2,1)S(1)} %collective-permute-done.6.refs_1_, bf16[4,2048]{1,0:T(4,128)(2,1)S(1)} %collective-permute-done.7.refs_2_, bf16[4,2048]{1,0:T(4,128)(2,1)S(1)} %collective-permute-done.8.refs_3_, ...), custom_call_target="tpu_custom_call" | custom-call | tf_op jit(solution)/shard_map/pallas_call | solution.py:240
  23.3 1.5 %collective-permute-start.11 = (bf16[16,1024]{1,0:T(8,128)(2,1)S(1)}, bf16[16,1024]{1,0:T(8,128)(2,1)S(1)}, u32[]{:S(2)}, u32[]{:S(2)}) collective-permute-start(bf16[16,1024]{1,0:T(8,128)(2,1)S(1)} %shard_map.144.refs_0_), channel_id=1, source_target_pairs={{0,12},{4,8},{8,4},{12,0},{1,13},{5,9},{9,5},{13,1},{2,14},{6,10},... | collective-permute-start | bytes 98312 | tf_op jit(solution)/shard_map/ppermute | solution.py:86
  24.8 0.6 %collective-permute-start.10 = (bf16[16,1024]{1,0:T(8,128)(2,1)S(1)}, bf16[16,1024]{1,0:T(8,128)(2,1)S(1)}, u32[]{:S(2)}, u32[]{:S(2)}) collective-permute-start(bf16[16,1024]{1,0:T(8,128)(2,1)S(1)} %shard_map.144.refs_0_), channel_id=1, source_target_pairs={{0,8},{4,12},{8,0},{12,4},{1,9},{5,13},{9,1},{13,5},{2,10},{6,14},... | collective-permute-start | bytes 98312 | tf_op jit(solution)/shard_map/ppermute | solution.py:86
  25.4 2.4 %collective-permute-start.9 = (bf16[16,1024]{1,0:T(8,128)(2,1)S(1)}, bf16[16,1024]{1,0:T(8,128)(2,1)S(1)}, u32[]{:S(2)}, u32[]{:S(2)}) collective-permute-start(bf16[16,1024]{1,0:T(8,128)(2,1)S(1)} %shard_map.144.refs_0_), channel_id=1, source_target_pairs={{0,4},{4,0},{8,12},{12,8},{1,5},{5,1},{9,13},{13,9},{2,6},{6,2},{1... | collective-permute-start | bytes 98312 | tf_op jit(solution)/shard_map/ppermute | solution.py:86
  27.7 1.3 %collective-permute-done.11.refs_3_ = bf16[16,1024]{1,0:T(8,128)(2,1)S(1)} collective-permute-done((bf16[16,1024]{1,0:T(8,128)(2,1)S(1)}, bf16[16,1024]{1,0:T(8,128)(2,1)S(1)}, u32[]{:S(2)}, u32[]{:S(2)}) %collective-permute-start.11) | collective-permute-done | bytes 32800 | tf_op jit(solution)/shard_map/ppermute | solution.py:86
  29.1 0.5 %collective-permute-done.10.refs_2_ = bf16[16,1024]{1,0:T(8,128)(2,1)S(1)} collective-permute-done((bf16[16,1024]{1,0:T(8,128)(2,1)S(1)}, bf16[16,1024]{1,0:T(8,128)(2,1)S(1)}, u32[]{:S(2)}, u32[]{:S(2)}) %collective-permute-start.10) | collective-permute-done | bytes 32800 | tf_op jit(solution)/shard_map/ppermute | solution.py:86
  29.6 0.4 collective-permute-done.9.refs_1_
  29.9 1.2 %shard_map.145 = (bf16[4,4224]{1,0:T(4,128)(2,1)S(1)}, bf16[4,4224]{1,0:T(4,128)(2,1)S(1)}, bf16[4,4224]{1,0:T(4,128)(2,1)S(1)}, bf16[4,4224]{1,0:T(4,128)(2,1)S(1)}, f32[16,1024]{1,0:T(8,128)S(1)}) custom-call(f32[16,1024]{1,0:T(8,128)S(1)} %get-tuple-element.33.base_ref, bf16[16,1024]{1,0:T(8,128)(2,1)S(1)} %shard_map.144.refs_0_, ...), custom_call_target="tpu_custom_call" | custom-call | tf_op jit(solution)/shard_map/pallas_call | solution.py:240
  31.1 1.2 %collective-permute-start.13 = (bf16[4,4224]{1,0:T(4,128)(2,1)S(1)}, bf16[4,4224]{1,0:T(4,128)(2,1)S(1)}, u32[]{:S(2)}, u32[]{:S(2)}) collective-permute-start(bf16[4,4224]{1,0:T(4,128)(2,1)S(1)} %get-tuple-element.46), channel_id=1, source_target_pairs={{0,2},{1,3},{2,0},{3,1},{4,6},{5,7},{6,4},{7,5},{8,10},{9,11},{10,... | collective-permute-start | bytes 101384 | tf_op jit(solution)/shard_map/ppermute | solution.py:86
  32.4 0.7 %collective-permute-start.14 = (bf16[4,4224]{1,0:T(4,128)(2,1)S(1)}, bf16[4,4224]{1,0:T(4,128)(2,1)S(1)}, u32[]{:S(2)}, u32[]{:S(2)}) collective-permute-start(bf16[4,4224]{1,0:T(4,128)(2,1)S(1)} %get-tuple-element.47), channel_id=1, source_target_pairs={{0,3},{1,2},{2,1},{3,0},{4,7},{5,6},{6,5},{7,4},{8,11},{9,10},{10,... | collective-permute-start | bytes 101384 | tf_op jit(solution)/shard_map/ppermute | solution.py:86
  33.0 0.8 %shard_map.146 = (f32[128,128]{1,0:T(8,128)S(1)}, f32[128,128]{1,0:T(8,128)S(1)}, bf16[16,256,128]{2,1,0:T(8,128)(2,1)S(1)}, bf16[16,128,128]{2,1,0:T(8,128)(2,1)S(1)}) custom-call(f32[2,64,128]{2,1,0:T(8,128)S(1)} %bitcast.14, f32[2,64,128]{2,1,0:T(8,128)S(1)} %bitcast.16, f32[2,128]{1,0:T(2,128)S(1)} %copy-done.8, bf16[2,128,16,128]{3,2,1,0:T(8,128)(2,1)S(1)} %copy-done.4, ...), custom_call_target="tpu_custom_call" | custom-call | flops 40000000000 | tf_op jit(solution)/shard_map/pallas_call | solution.py:240
  33.8 1.3 %collective-permute-done.13.refs_2_ = bf16[4,4224]{1,0:T(4,128)(2,1)S(1)} collective-permute-done((bf16[4,4224]{1,0:T(4,128)(2,1)S(1)}, bf16[4,4224]{1,0:T(4,128)(2,1)S(1)}, u32[]{:S(2)}, u32[]{:S(2)}) %collective-permute-start.13) | collective-permute-done | bytes 33824 | tf_op jit(solution)/shard_map/ppermute | solution.py:86
  35.1 0.6 %collective-permute-done.14.refs_3_ = bf16[4,4224]{1,0:T(4,128)(2,1)S(1)} collective-permute-done((bf16[4,4224]{1,0:T(4,128)(2,1)S(1)}, bf16[4,4224]{1,0:T(4,128)(2,1)S(1)}, u32[]{:S(2)}, u32[]{:S(2)}) %collective-permute-start.14) | collective-permute-done | bytes 33824 | tf_op jit(solution)/shard_map/ppermute | solution.py:86
  35.7 0.7 %shard_map.147 = (bf16[4,2048]{1,0:T(4,128)(2,1)S(1)}, f32[128,128]{1,0:T(8,128)S(1)}) custom-call(bf16[4,4224]{1,0:T(4,128)(2,1)S(1)} %get-tuple-element.44.refs_0_, bf16[4,4224]{1,0:T(4,128)(2,1)S(1)} %collective-permute-done.12.refs_1_, bf16[4,4224]{1,0:T(4,128)(2,1)S(1)} %collective-permute-done.13.refs_2_, ...), custom_call_target="tpu_custom_call" | custom-call | tf_op jit(solution)/shard_map/pallas_call | solution.py:240
  36.4 0.8 %collective-permute-start.17 = (bf16[4,2048]{1,0:T(4,128)(2,1)S(1)}, bf16[4,2048]{1,0:T(4,128)(2,1)S(1)}, u32[]{:S(2)}, u32[]{:S(2)}) collective-permute-start(bf16[4,2048]{1,0:T(4,128)(2,1)S(1)} %get-tuple-element.52.refs_0_), channel_id=1, source_target_pairs={{0,3},{1,2},{2,1},{3,0},{4,7},{5,6},{6,5},{7,4},{8,11},{9,10},{10,... | collective-permute-start | bytes 49160 | tf_op jit(solution)/shard_map/ppermute | solution.py:86
  37.2 1.1 %collective-permute-start.16 = (bf16[4,2048]{1,0:T(4,128)(2,1)S(1)}, bf16[4,2048]{1,0:T(4,128)(2,1)S(1)}, u32[]{:S(2)}, u32[]{:S(2)}) collective-permute-start(bf16[4,2048]{1,0:T(4,128)(2,1)S(1)} %get-tuple-element.52.refs_0_), channel_id=1, source_target_pairs={{0,2},{1,3},{2,0},{3,1},{4,6},{5,7},{6,4},{7,5},{8,10},{9,11},{10,... | collective-permute-start | bytes 49160 | tf_op jit(solution)/shard_map/ppermute | solution.py:86
  38.3 0.0 collective-permute-start.15
  38.3 1.3 %collective-permute-done.17.refs_3_ = bf16[4,2048]{1,0:T(4,128)(2,1)S(1)} collective-permute-done((bf16[4,2048]{1,0:T(4,128)(2,1)S(1)}, bf16[4,2048]{1,0:T(4,128)(2,1)S(1)}, u32[]{:S(2)}, u32[]{:S(2)}) %collective-permute-start.17) | collective-permute-done | bytes 16416 | tf_op jit(solution)/shard_map/ppermute | solution.py:86
  39.6 1.3 %collective-permute-done.16.refs_2_ = bf16[4,2048]{1,0:T(4,128)(2,1)S(1)} collective-permute-done((bf16[4,2048]{1,0:T(4,128)(2,1)S(1)}, bf16[4,2048]{1,0:T(4,128)(2,1)S(1)}, u32[]{:S(2)}, u32[]{:S(2)}) %collective-permute-start.16) | collective-permute-done | bytes 16416 | tf_op jit(solution)/shard_map/ppermute | solution.py:86
  41.0 0.7 %shard_map.148 = (f32[4,1024]{1,0:T(4,128)S(1)}, bf16[4,1024]{1,0:T(4,128)(2,1)S(1)}, bf16[4,1024]{1,0:T(4,128)(2,1)S(1)}, bf16[4,1024]{1,0:T(4,128)(2,1)S(1)}) custom-call(bf16[4,2048]{1,0:T(4,128)(2,1)S(1)} %get-tuple-element.52.refs_0_, bf16[4,2048]{1,0:T(4,128)(2,1)S(1)} %collective-permute-done.15.refs_1_, ...), custom_call_target="tpu_custom_call" | custom-call | tf_op jit(solution)/shard_map/pallas_call | solution.py:240
  41.6 1.7 %collective-permute-start.18 = (bf16[4,1024]{1,0:T(4,128)(2,1)S(1)}, bf16[4,1024]{1,0:T(4,128)(2,1)S(1)}, u32[]{:S(2)}, u32[]{:S(2)}) collective-permute-start(bf16[4,1024]{1,0:T(4,128)(2,1)S(1)} %get-tuple-element.55), channel_id=1, source_target_pairs={{0,4},{4,0},{8,12},{12,8},{1,5},{5,1},{9,13},{13,9},{2,6},{6,2},{1... | collective-permute-start | bytes 24584 | tf_op jit(solution)/shard_map/ppermute | solution.py:86
  43.3 1.2 %collective-permute-start.19 = (bf16[4,1024]{1,0:T(4,128)(2,1)S(1)}, bf16[4,1024]{1,0:T(4,128)(2,1)S(1)}, u32[]{:S(2)}, u32[]{:S(2)}) collective-permute-start(bf16[4,1024]{1,0:T(4,128)(2,1)S(1)} %get-tuple-element.56), channel_id=1, source_target_pairs={{0,8},{4,12},{8,0},{12,4},{1,9},{5,13},{9,1},{13,5},{2,10},{6,14},... | collective-permute-start | bytes 24584 | tf_op jit(solution)/shard_map/ppermute | solution.py:86
  44.6 1.4 %collective-permute-start.20 = (bf16[4,1024]{1,0:T(4,128)(2,1)S(1)}, bf16[4,1024]{1,0:T(4,128)(2,1)S(1)}, u32[]{:S(2)}, u32[]{:S(2)}) collective-permute-start(bf16[4,1024]{1,0:T(4,128)(2,1)S(1)} %get-tuple-element.57), channel_id=1, source_target_pairs={{0,12},{4,8},{8,4},{12,0},{1,13},{5,9},{9,5},{13,1},{2,14},{6,10},... | collective-permute-start | bytes 24584 | tf_op jit(solution)/shard_map/ppermute | solution.py:86
  46.0 0.7 %maximum_bitcast_fusion = f32[2,1,128,128]{3,2,1,0:T(8,128)} fusion(f32[1,128,128]{2,1,0:T(8,128)S(1)} %bitcast.12, f32[1,128,128]{2,1,0:T(8,128)S(1)} %bitcast.11), kind=kLoop, calls=%fused_computation | loop fusion | flops 32768 | bytes 262144
  46.7 1.2 %collective-permute-done.19.refs_1_ = bf16[4,1024]{1,0:T(4,128)(2,1)S(1)} collective-permute-done((bf16[4,1024]{1,0:T(4,128)(2,1)S(1)}, bf16[4,1024]{1,0:T(4,128)(2,1)S(1)}, u32[]{:S(2)}, u32[]{:S(2)}) %collective-permute-start.19) | collective-permute-done | bytes 8224 | tf_op jit(solution)/shard_map/ppermute | solution.py:86
  47.9 2.1 %collective-permute-done.20.refs_2_ = bf16[4,1024]{1,0:T(4,128)(2,1)S(1)} collective-permute-done((bf16[4,1024]{1,0:T(4,128)(2,1)S(1)}, bf16[4,1024]{1,0:T(4,128)(2,1)S(1)}, u32[]{:S(2)}, u32[]{:S(2)}) %collective-permute-start.20) | collective-permute-done | bytes 8224 | tf_op jit(solution)/shard_map/ppermute | solution.py:86
  50.0 0.6 %shard_map.149 = bf16[1,4,1024]{2,1,0:T(4,128)(2,1)} custom-call(f32[4,1024]{1,0:T(4,128)S(1)} %get-tuple-element.54.own_ref, bf16[4,1024]{1,0:T(4,128)(2,1)S(1)} %collective-permute-done.18.refs_0_, bf16[4,1024]{1,0:T(4,128)(2,1)S(1)} %collective-permute-done.19.refs_1_, bf16[4,1024]{1,0:T(4,128)(2,1)S(1)} %collective-permute-done.20.refs_2_), custom_call_target="tpu_custom_call" | custom-call | tf_op jit(solution)/shard_map/pallas_call | solution.py:240
  (28 shorter events, 0.1 us)
Async XLA Ops:
  0.6 10.6 %copy-start = (bf16[2,1024,2048]{2,1,0:T(8,128)(2,1)S(1)}, bf16[2,1024,2048]{2,1,0:T(8,128)(2,1)}, u32[]{:S(2)}) copy-start(bf16[2,1024,2048]{2,1,0:T(8,128)(2,1)} %refs_5_.3) | copy-start | bytes 25165828
  0.6 10.6 %copy-start.1 = (bf16[2,1024,2048]{2,1,0:T(8,128)(2,1)S(1)}, bf16[2,1024,2048]{2,1,0:T(8,128)(2,1)}, u32[]{:S(2)}) copy-start(bf16[2,1024,2048]{2,1,0:T(8,128)(2,1)} %refs_6_.3) | copy-start | bytes 25165828
  1.5 6.8 %collective-permute-start.2 = (bf16[4,1024]{1,0:T(4,128)(2,1)S(1)}, bf16[4,1024]{1,0:T(4,128)(2,1)S(1)}, u32[]{:S(2)}, u32[]{:S(2)}) collective-permute-start(bf16[4,1024]{1,0:T(4,128)(2,1)S(1)} %get-tuple-element.31.refs_0_), channel_id=1, source_target_pairs={{0,12},{4,8},{8,4},{12,0},{1,13},{5,9},{9,5},{13,1},{2,14},{6,10},... | collective-permute-start | bytes 24584 | tf_op jit(solution)/shard_map/ppermute | solution.py:86
  6.7 4.5 %collective-permute-start.1 = (bf16[4,1024]{1,0:T(4,128)(2,1)S(1)}, bf16[4,1024]{1,0:T(4,128)(2,1)S(1)}, u32[]{:S(2)}, u32[]{:S(2)}) collective-permute-start(bf16[4,1024]{1,0:T(4,128)(2,1)S(1)} %get-tuple-element.31.refs_0_), channel_id=1, source_target_pairs={{0,8},{4,12},{8,0},{12,4},{1,9},{5,13},{9,1},{13,5},{2,10},{6,14},... | collective-permute-start | bytes 24584 | tf_op jit(solution)/shard_map/ppermute | solution.py:86
  6.7 4.5 %collective-permute-start = (bf16[4,1024]{1,0:T(4,128)(2,1)S(1)}, bf16[4,1024]{1,0:T(4,128)(2,1)S(1)}, u32[]{:S(2)}, u32[]{:S(2)}) collective-permute-start(bf16[4,1024]{1,0:T(4,128)(2,1)S(1)} %get-tuple-element.31.refs_0_), channel_id=1, source_target_pairs={{0,4},{4,0},{8,12},{12,8},{1,5},{5,1},{9,13},{13,9},{2,6},{6,2},{1... | collective-permute-start | bytes 24584 | tf_op jit(solution)/shard_map/ppermute | solution.py:86
  11.3 3.2 %copy-start.4 = (bf16[2,128,16,128]{3,2,1,0:T(8,128)(2,1)S(1)}, bf16[2,128,16,128]{3,2,1,0:T(8,128)(2,1)}, u32[]{:S(2)}) copy-start(bf16[2,128,16,128]{3,2,1,0:T(8,128)(2,1)} %map_ref.3) | copy-start | bytes 3145732
  11.3 3.1 %copy-start.5 = (bf16[2,128,16,128]{3,2,1,0:T(8,128)(2,1)S(1)}, bf16[2,128,16,128]{3,2,1,0:T(8,128)(2,1)}, u32[]{:S(2)}) copy-start(bf16[2,128,16,128]{3,2,1,0:T(8,128)(2,1)} %readout_ref.3) | copy-start | bytes 3145732
  11.3 3.1 %copy-start.6 = (f32[2,128,64]{1,2,0:T(8,128)S(1)}, f32[2,128,64]{1,2,0:T(8,128)}, u32[]{:S(2)}) copy-start(f32[2,128,64]{1,2,0:T(8,128)} %param.18) | copy-start | bytes 196612
  11.3 3.1 %copy-start.7 = (f32[2,128,64]{1,2,0:T(8,128)S(1)}, f32[2,128,64]{1,2,0:T(8,128)}, u32[]{:S(2)}) copy-start(f32[2,128,64]{1,2,0:T(8,128)} %param.19) | copy-start | bytes 196612
  11.3 3.1 %copy-start.8 = (f32[2,128]{1,0:T(2,128)S(1)}, f32[2,128]{1,0:T(2,128)}, u32[]{:S(2)}) copy-start(f32[2,128]{1,0:T(2,128)} %log_step_ref.3) | copy-start | bytes 3076
  11.3 11.3 %slice-start = ((s8[8388608]{0:T(1024)(128)(4,1)}), s8[4194304]{0:T(1024)(128)(4,1)S(1)}, s32[]{:S(2)}) async-start(s8[8388608]{0:T(1024)(128)(4,1)} %bitcast.9), calls=%async_computation | async-start | bytes 8388608
  12.5 2.7 %collective-permute-start.3 = (bf16[4,4224]{1,0:T(4,128)(2,1)S(1)}, bf16[4,4224]{1,0:T(4,128)(2,1)S(1)}, u32[]{:S(2)}, u32[]{:S(2)}) collective-permute-start(bf16[4,4224]{1,0:T(4,128)(2,1)S(1)} %get-tuple-element.35), channel_id=1, source_target_pairs={{0,1},{1,0},{2,3},{3,2},{4,5},{5,4},{6,7},{7,6},{8,9},{9,8},{10,11... | collective-permute-start | bytes 101384 | tf_op jit(solution)/shard_map/ppermute | solution.py:86
  12.5 4.0 %collective-permute-start.4 = (bf16[4,4224]{1,0:T(4,128)(2,1)S(1)}, bf16[4,4224]{1,0:T(4,128)(2,1)S(1)}, u32[]{:S(2)}, u32[]{:S(2)}) collective-permute-start(bf16[4,4224]{1,0:T(4,128)(2,1)S(1)} %get-tuple-element.36), channel_id=1, source_target_pairs={{0,2},{1,3},{2,0},{3,1},{4,6},{5,7},{6,4},{7,5},{8,10},{9,11},{10,... | collective-permute-start | bytes 101384 | tf_op jit(solution)/shard_map/ppermute | solution.py:86
  14.1 3.4 %collective-permute-start.5 = (bf16[4,4224]{1,0:T(4,128)(2,1)S(1)}, bf16[4,4224]{1,0:T(4,128)(2,1)S(1)}, u32[]{:S(2)}, u32[]{:S(2)}) collective-permute-start(bf16[4,4224]{1,0:T(4,128)(2,1)S(1)} %get-tuple-element.37), channel_id=1, source_target_pairs={{0,3},{1,2},{2,1},{3,0},{4,7},{5,6},{6,5},{7,4},{8,11},{9,10},{10,... | collective-permute-start | bytes 101384 | tf_op jit(solution)/shard_map/ppermute | solution.py:86
  14.4 3.1 %copy-start.2 = (f32[2,1,128,128]{3,2,1,0:T(8,128)S(1)}, f32[2,1,128,128]{3,2,1,0:T(8,128)}, u32[]{:S(2)}) copy-start(f32[2,1,128,128]{3,2,1,0:T(8,128)} %refs_10_.3) | copy-start | bytes 393220
  14.4 3.0 %copy-start.3 = (bf16[2,2048]{1,0:T(2,128)(2,1)S(1)}, bf16[2,2048]{1,0:T(2,128)(2,1)}, u32[]{:S(2)}) copy-start(bf16[2,2048]{1,0:T(2,128)(2,1)} %refs_9_.3) | copy-start | bytes 24580
  14.5 8.2 %slice-start.1 = ((s8[8388608]{0:T(1024)(128)(4,1)}), s8[4194304]{0:T(1024)(128)(4,1)S(1)}, s32[]{:S(2)}) async-start(s8[8388608]{0:T(1024)(128)(4,1)} %bitcast.9), calls=%async_computation.1 | async-start | bytes 8388608
  18.2 3.2 %collective-permute-start.8 = (bf16[4,2048]{1,0:T(4,128)(2,1)S(1)}, bf16[4,2048]{1,0:T(4,128)(2,1)S(1)}, u32[]{:S(2)}, u32[]{:S(2)}) collective-permute-start(bf16[4,2048]{1,0:T(4,128)(2,1)S(1)} %get-tuple-element.43.refs_0_), channel_id=1, source_target_pairs={{0,3},{1,2},{2,1},{3,0},{4,7},{5,6},{6,5},{7,4},{8,11},{9,10},{10,... | collective-permute-start | bytes 49160 | tf_op jit(solution)/shard_map/ppermute | solution.py:86
  18.9 3.7 %collective-permute-start.7 = (bf16[4,2048]{1,0:T(4,128)(2,1)S(1)}, bf16[4,2048]{1,0:T(4,128)(2,1)S(1)}, u32[]{:S(2)}, u32[]{:S(2)}) collective-permute-start(bf16[4,2048]{1,0:T(4,128)(2,1)S(1)} %get-tuple-element.43.refs_0_), channel_id=1, source_target_pairs={{0,2},{1,3},{2,0},{3,1},{4,6},{5,7},{6,4},{7,5},{8,10},{9,11},{10,... | collective-permute-start | bytes 49160 | tf_op jit(solution)/shard_map/ppermute | solution.py:86
  20.1 2.6 %collective-permute-start.6 = (bf16[4,2048]{1,0:T(4,128)(2,1)S(1)}, bf16[4,2048]{1,0:T(4,128)(2,1)S(1)}, u32[]{:S(2)}, u32[]{:S(2)}) collective-permute-start(bf16[4,2048]{1,0:T(4,128)(2,1)S(1)} %get-tuple-element.43.refs_0_), channel_id=1, source_target_pairs={{0,1},{1,0},{2,3},{3,2},{4,5},{5,4},{6,7},{7,6},{8,9},{9,8},{10,11... | collective-permute-start | bytes 49160 | tf_op jit(solution)/shard_map/ppermute | solution.py:86
  23.3 5.7 %collective-permute-start.11 = (bf16[16,1024]{1,0:T(8,128)(2,1)S(1)}, bf16[16,1024]{1,0:T(8,128)(2,1)S(1)}, u32[]{:S(2)}, u32[]{:S(2)}) collective-permute-start(bf16[16,1024]{1,0:T(8,128)(2,1)S(1)} %shard_map.144.refs_0_), channel_id=1, source_target_pairs={{0,12},{4,8},{8,4},{12,0},{1,13},{5,9},{9,5},{13,1},{2,14},{6,10},... | collective-permute-start | bytes 98312 | tf_op jit(solution)/shard_map/ppermute | solution.py:86
  24.8 4.8 %collective-permute-start.10 = (bf16[16,1024]{1,0:T(8,128)(2,1)S(1)}, bf16[16,1024]{1,0:T(8,128)(2,1)S(1)}, u32[]{:S(2)}, u32[]{:S(2)}) collective-permute-start(bf16[16,1024]{1,0:T(8,128)(2,1)S(1)} %shard_map.144.refs_0_), channel_id=1, source_target_pairs={{0,8},{4,12},{8,0},{12,4},{1,9},{5,13},{9,1},{13,5},{2,10},{6,14},... | collective-permute-start | bytes 98312 | tf_op jit(solution)/shard_map/ppermute | solution.py:86
  25.4 4.6 %collective-permute-start.9 = (bf16[16,1024]{1,0:T(8,128)(2,1)S(1)}, bf16[16,1024]{1,0:T(8,128)(2,1)S(1)}, u32[]{:S(2)}, u32[]{:S(2)}) collective-permute-start(bf16[16,1024]{1,0:T(8,128)(2,1)S(1)} %shard_map.144.refs_0_), channel_id=1, source_target_pairs={{0,4},{4,0},{8,12},{12,8},{1,5},{5,1},{9,13},{13,9},{2,6},{6,2},{1... | collective-permute-start | bytes 98312 | tf_op jit(solution)/shard_map/ppermute | solution.py:86
  31.1 2.6 %collective-permute-start.12 = (bf16[4,4224]{1,0:T(4,128)(2,1)S(1)}, bf16[4,4224]{1,0:T(4,128)(2,1)S(1)}, u32[]{:S(2)}, u32[]{:S(2)}) collective-permute-start(bf16[4,4224]{1,0:T(4,128)(2,1)S(1)} %get-tuple-element.45), channel_id=1, source_target_pairs={{0,1},{1,0},{2,3},{3,2},{4,5},{5,4},{6,7},{7,6},{8,9},{9,8},{10,11... | collective-permute-start | bytes 101384 | tf_op jit(solution)/shard_map/ppermute | solution.py:86
  31.1 4.0 %collective-permute-start.13 = (bf16[4,4224]{1,0:T(4,128)(2,1)S(1)}, bf16[4,4224]{1,0:T(4,128)(2,1)S(1)}, u32[]{:S(2)}, u32[]{:S(2)}) collective-permute-start(bf16[4,4224]{1,0:T(4,128)(2,1)S(1)} %get-tuple-element.46), channel_id=1, source_target_pairs={{0,2},{1,3},{2,0},{3,1},{4,6},{5,7},{6,4},{7,5},{8,10},{9,11},{10,... | collective-permute-start | bytes 101384 | tf_op jit(solution)/shard_map/ppermute | solution.py:86
  32.4 3.4 %collective-permute-start.14 = (bf16[4,4224]{1,0:T(4,128)(2,1)S(1)}, bf16[4,4224]{1,0:T(4,128)(2,1)S(1)}, u32[]{:S(2)}, u32[]{:S(2)}) collective-permute-start(bf16[4,4224]{1,0:T(4,128)(2,1)S(1)} %get-tuple-element.47), channel_id=1, source_target_pairs={{0,3},{1,2},{2,1},{3,0},{4,7},{5,6},{6,5},{7,4},{8,11},{9,10},{10,... | collective-permute-start | bytes 101384 | tf_op jit(solution)/shard_map/ppermute | solution.py:86
  36.4 3.2 %collective-permute-start.17 = (bf16[4,2048]{1,0:T(4,128)(2,1)S(1)}, bf16[4,2048]{1,0:T(4,128)(2,1)S(1)}, u32[]{:S(2)}, u32[]{:S(2)}) collective-permute-start(bf16[4,2048]{1,0:T(4,128)(2,1)S(1)} %get-tuple-element.52.refs_0_), channel_id=1, source_target_pairs={{0,3},{1,2},{2,1},{3,0},{4,7},{5,6},{6,5},{7,4},{8,11},{9,10},{10,... | collective-permute-start | bytes 49160 | tf_op jit(solution)/shard_map/ppermute | solution.py:86
  37.2 3.7 %collective-permute-start.16 = (bf16[4,2048]{1,0:T(4,128)(2,1)S(1)}, bf16[4,2048]{1,0:T(4,128)(2,1)S(1)}, u32[]{:S(2)}, u32[]{:S(2)}) collective-permute-start(bf16[4,2048]{1,0:T(4,128)(2,1)S(1)} %get-tuple-element.52.refs_0_), channel_id=1, source_target_pairs={{0,2},{1,3},{2,0},{3,1},{4,6},{5,7},{6,4},{7,5},{8,10},{9,11},{10,... | collective-permute-start | bytes 49160 | tf_op jit(solution)/shard_map/ppermute | solution.py:86
  38.3 2.7 %collective-permute-start.15 = (bf16[4,2048]{1,0:T(4,128)(2,1)S(1)}, bf16[4,2048]{1,0:T(4,128)(2,1)S(1)}, u32[]{:S(2)}, u32[]{:S(2)}) collective-permute-start(bf16[4,2048]{1,0:T(4,128)(2,1)S(1)} %get-tuple-element.52.refs_0_), channel_id=1, source_target_pairs={{0,1},{1,0},{2,3},{3,2},{4,5},{5,4},{6,7},{7,6},{8,9},{9,8},{10,11... | collective-permute-start | bytes 49160 | tf_op jit(solution)/shard_map/ppermute | solution.py:86
  41.6 5.1 %collective-permute-start.18 = (bf16[4,1024]{1,0:T(4,128)(2,1)S(1)}, bf16[4,1024]{1,0:T(4,128)(2,1)S(1)}, u32[]{:S(2)}, u32[]{:S(2)}) collective-permute-start(bf16[4,1024]{1,0:T(4,128)(2,1)S(1)} %get-tuple-element.55), channel_id=1, source_target_pairs={{0,4},{4,0},{8,12},{12,8},{1,5},{5,1},{9,13},{13,9},{2,6},{6,2},{1... | collective-permute-start | bytes 24584 | tf_op jit(solution)/shard_map/ppermute | solution.py:86
  43.3 4.5 %collective-permute-start.19 = (bf16[4,1024]{1,0:T(4,128)(2,1)S(1)}, bf16[4,1024]{1,0:T(4,128)(2,1)S(1)}, u32[]{:S(2)}, u32[]{:S(2)}) collective-permute-start(bf16[4,1024]{1,0:T(4,128)(2,1)S(1)} %get-tuple-element.56), channel_id=1, source_target_pairs={{0,8},{4,12},{8,0},{12,4},{1,9},{5,13},{9,1},{13,5},{2,10},{6,14},... | collective-permute-start | bytes 24584 | tf_op jit(solution)/shard_map/ppermute | solution.py:86
  44.6 5.4 %collective-permute-start.20 = (bf16[4,1024]{1,0:T(4,128)(2,1)S(1)}, bf16[4,1024]{1,0:T(4,128)(2,1)S(1)}, u32[]{:S(2)}, u32[]{:S(2)}) collective-permute-start(bf16[4,1024]{1,0:T(4,128)(2,1)S(1)} %get-tuple-element.57), channel_id=1, source_target_pairs={{0,12},{4,8},{8,4},{12,0},{1,13},{5,9},{9,5},{13,1},{2,14},{6,10},... | collective-permute-start | bytes 24584 | tf_op jit(solution)/shard_map/ppermute | solution.py:86

commit v5 on v4

--- a/solution.py
+++ b/solution.py
@@ -315,44 +315,100 @@
         seen_ref[chunk] = jnp.where(upper, seen, -seen).astype(jnp.bfloat16)
 
 
+def mark_row(marks_ref, index):
+    return jnp.broadcast_to(marks_ref[index : index + 1], (SUBLANES, LANES))
+
+
 def parameter_kernel(
-    layer, decay_ref, frequency_ref, log_step_ref, map_ref, readout_ref, *refs
+    layer, rows, decay_ref, frequency_ref, log_step_ref, map_ref, readout_ref, marks_ref, *refs
 ):
+    state_refs, (real_ref, imag_ref, coupled_ref, seen_ref, carried_ref) = refs[:-5], refs[-5:]
     parameter_step(
         decay_ref[layer], frequency_ref[layer], log_step_ref[layer : layer + 1],
-        map_ref.at[layer], readout_ref.at[layer], *refs[-4:],
-    )
-
-
-def prepare(layer, decay, frequency, log_step, input_map, readout_map, after=()):
-    _, _, groups = decay.shape
+        map_ref.at[layer], readout_ref.at[layer], real_ref, imag_ref, coupled_ref, seen_ref,
+    )
+    groups = real_ref.shape[0]
+    for chunk in range(groups // SUBLANES):
+        at = slice(chunk * SUBLANES, (chunk + 1) * SUBLANES)
+        real, imag = real_ref[at], imag_ref[at]
+        decayed = []
+        for state_ref in state_refs:
+            value = state_ref[layer, at].astype(jnp.float32)
+            decayed.append(real * value + imag * pltpu.roll(value, LANES // 2, 1))
+        for r in range(rows):
+            carried_ref[r, at] = sum(
+                jnp.where(mark_row(marks_ref, k * rows + r) > 0.5, value, 0.0)
+                for k, value in enumerate(decayed)
+            )
+
+
+def prepare(layer, rows, decay, frequency, log_step, input_map, readout_map, marks, states):
+    groups = decay.shape[2]
+    chunks = groups // SUBLANES
     return vmem_call(
-        functools.partial(parameter_kernel, layer),
+        functools.partial(parameter_kernel, layer, rows),
         [((groups, LANES), jnp.float32)] * 2
-        + [((groups // SUBLANES, rows, LANES), jnp.bfloat16) for rows in (2 * LANES, LANES)],
-        decay, frequency, log_step, input_map, readout_map, *after,
+        + [((chunks, size, LANES), jnp.bfloat16) for size in (2 * LANES, LANES)]
+        + [((rows, groups, LANES), jnp.float32)],
+        decay, frequency, log_step, input_map, readout_map, marks, *states,
         cost=COST,
     )
 
 
-def small_kernel(steps, lengths_hbm, *refs):
-    count = (len(refs) - 3) // 2
+def narrow_kernel(state_ref, out_ref):
+    out_ref[...] = state_ref[...].astype(jnp.bfloat16)
+
+
+def small_kernel(size, steps, lengths_hbm, *refs):
+    count = (len(refs) - 5) // 2
     sources, targets = refs[:count], refs[count : 2 * count]
-    live_ref, lengths, semaphores = refs[2 * count :]
-    copies = start_copies(
-        [lengths_hbm, *sources], [lengths, *targets], semaphores
-    )
+    pick_ref, spread_ref, marks_ref, lengths, semaphores = refs[2 * count :]
+    copies = start_copies([lengths_hbm, *sources], [lengths, *targets], semaphores)
     copies[0].wait()
-    length = lengths[lax.axis_index("dp")]
-    place = lax.broadcasted_iota(jnp.int32, (steps * SUBLANES, LANES), 0) // SUBLANES
-    live_ref[...] = (place < length).astype(jnp.float32)
+    dp_index, tp_index = lax.axis_index("dp"), lax.axis_index("tp")
+    rows = pick_ref.shape[0]
+    length = [lengths[s] for s in range(size)]
+    offset = [sum(length[:s], 0 * length[0]) for s in range(size)]
+
+    def of(values, index):
+        return sum(jnp.where(index == s, values[s], 0) for s in range(size))
+
+    def places(shape):
+        return [lax.broadcasted_iota(jnp.int32, shape, axis) for axis in (0, 1)]
+
+    row, lane = places((rows, LANES))
+    chosen = jnp.zeros((rows, LANES), jnp.float32)
+    for s in range(size):
+        t = lane - s * steps
+        hit = (t >= 0) & (t < length[s]) & (row == offset[s] + t)
+        chosen = jnp.where(hit, 1.0, chosen)
+    pick_ref[...] = chosen.astype(jnp.bfloat16)
+    row, lane = places((size * steps, LANES))
+    chosen = jnp.zeros((size * steps, LANES), jnp.float32)
+    for k in range(size):
+        t = row - k * steps
+        start, live = of(offset, tp_index ^ k), of(length, tp_index ^ k)
+        hit = (t >= 0) & (t < live) & (lane == start + t)
+        chosen = jnp.where(hit, 1.0, chosen)
+    spread_ref[...] = chosen.astype(jnp.bfloat16)
+    row, _ = places((rows, LANES))
+    for k in range(size):
+        marks_ref[k * rows : (k + 1) * rows] = (row == of(offset, dp_index ^ k)).astype(jnp.float32)
+    fresh = row == offset[0]
+    for s in range(1, size):
+        fresh = fresh | (row == offset[s])
+    marks_ref[size * rows : (size + 1) * rows] = jnp.where(fresh, 0.0, 1.0)
+    last = of(offset, dp_index) + of(length, dp_index) - 1
+    marks_ref[(size + 1) * rows :] = (row == last).astype(jnp.float32)
     wait_copies(copies[1:])
 
 
-def bring_small(steps, lengths, *arrays):
+def bring_small(size, steps, rows, lengths, *arrays):
     return vmem_call(
-        functools.partial(small_kernel, steps),
-        [(a.shape, a.dtype) for a in arrays] + [((steps * SUBLANES, LANES), jnp.float32)],
+        functools.partial(small_kernel, size, steps),
+        [(a.shape, a.dtype) for a in arrays]
+        + [((rows, LANES), jnp.bfloat16), ((size * steps, LANES), jnp.bfloat16)]
+        + [(((size + 2) * rows, LANES), jnp.float32)],
         lengths, *arrays,
         in_specs=[HBM] * (1 + len(arrays)),
         scratch=[
@@ -363,6 +419,13 @@
     )
 
 
+def far_swaps(value, axis, size):
+    received = {}
+    for k in range(2, size, 2):
+        received[k] = swap(value, axis, k, size)
+    return received
+
+
 def swaps(values, axis, size):
     received = {}
     for k in reversed(range(1, size)):
@@ -371,8 +434,7 @@
     return [received[k] for k in range(1, size)]
 
 
-def project(layer, rows, gain_ref, drive_weight_ref, gate_weight_ref, message_refs):
-    count = rows.shape[0] // len(message_refs)
+def project(layer, rows, gain_ref, drive_weight_ref, gate_weight_ref, message_ref):
     width = drive_weight_ref.shape[2]
     scaled = (rows * gain_ref[layer : layer + 1]).astype(jnp.bfloat16)
     squares = jnp.sum(rows * rows, axis=1, keepdims=True)
@@ -382,18 +444,14 @@
         piece = squares.astype(jnp.bfloat16).astype(jnp.float32)
         extra = jnp.where(lane == place, piece, extra)
         squares = squares - piece
+    message_ref[:, 2 * width :] = extra.astype(jnp.bfloat16)
     step = min(width, 512)
-    parts = [(2 * width, LANES, extra)]
     for base, weight_ref in ((0, drive_weight_ref), (width, gate_weight_ref)):
         for at in range(0, width, step):
             value = jnp.dot(
                 scaled, weight_ref[layer, :, at : at + step], preferred_element_type=jnp.float32
             )
-            parts.append((base + at, step, value))
-    for at, size, value in parts:
-        for k, message_ref in enumerate(message_refs):
-            block = value[k * count : (k + 1) * count]
-            message_ref[:, at : at + size] = block.astype(jnp.bfloat16)
+            message_ref[:, base + at : base + at + step] = value.astype(jnp.bfloat16)
 
 
 def pick(blocks, offset):
@@ -405,115 +463,106 @@
     return blocks
 
 
-def own_offset():
-    return lax.axis_index("dp") ^ lax.axis_index("tp")
-
-
-def first_kernel(size, *refs):
+def first_kernel(size, pick_ref, *refs):
     block_refs, (gain_ref, drive_ref, gate_ref) = refs[:size], refs[size : size + 3]
-    message_refs, rows_ref = refs[size + 3 : -1], refs[-1]
-    blocks = [ref[...].astype(jnp.float32).reshape(ref.shape[-2:]) for ref in block_refs]
-    rows = jnp.concatenate(pick(blocks, own_offset()), axis=0)
+    message_ref, rows_ref = refs[size + 3 :]
+    blocks = [ref[...].astype(jnp.float32) for ref in block_refs]
+    blocks = jnp.concatenate(pick(blocks, lax.axis_index("tp")), axis=0).astype(jnp.bfloat16)
+    chosen = pick_ref[:, : blocks.shape[0]]
+    rows = jnp.dot(chosen, blocks, preferred_element_type=jnp.float32)
     rows_ref[...] = rows
-    project(0, rows, gain_ref, drive_ref, gate_ref, message_refs)
+    project(0, rows, gain_ref, drive_ref, gate_ref, message_ref)
 
 
 def next_kernel(size, layer, base_ref, *refs):
     part_refs, (gain_ref, drive_ref, gate_ref) = refs[:size], refs[size : size + 3]
-    message_refs, rows_ref = refs[size + 3 : -1], refs[-1]
-    rows = base_ref[...]
-    rows = rows + sum(ref[...].astype(jnp.float32) for ref in part_refs)
+    message_ref, rows_ref = refs[size + 3 :]
+    rows = base_ref[...] + sum(ref[...].astype(jnp.float32) for ref in part_refs)
     rows = rows.astype(jnp.bfloat16).astype(jnp.float32)
     rows_ref[...] = rows
-    project(layer, rows, gain_ref, drive_ref, gate_ref, message_refs)
-
-
-def state_kernel(size, layer, features, *refs):
+    project(layer, rows, gain_ref, drive_ref, gate_ref, message_ref)
+
+
+def advance(size, layer, features, refs, next_ref, branch_ref):
     message_refs = refs[:size]
-    live_ref, real_ref, imag_ref, coupled_ref, seen_ref, skip_ref, state_ref = refs[size:-2]
-    branch_ref, next_ref = refs[-2:]
-    steps = message_refs[0].shape[0]
-    width = branch_ref.shape[1]
+    marks_ref, real_ref, imag_ref, coupled_ref, seen_ref, carried_ref, skip_ref = refs[size:]
+    rows, width = branch_ref.shape
     half = LANES // 2
     total = sum(ref[...].astype(jnp.float32) for ref in message_refs)
     squares = jnp.sum(total[:, 2 * width :], axis=1, keepdims=True)
     inverse = lax.rsqrt(squares / features + epsilon)
     drive = (inverse * total[:, :width]).astype(jnp.bfloat16).astype(jnp.float32)
     gate = (inverse * total[:, width : 2 * width]).astype(jnp.bfloat16).astype(jnp.float32)
-    live = live_ref[...]
     own_group = group_mask()
-    keeps = [live[t * SUBLANES : (t + 1) * SUBLANES] > 0.5 for t in range(steps)]
-    live_rows = jnp.concatenate(
-        [live[t * SUBLANES : t * SUBLANES + 1] for t in range(steps)], axis=0
-    )
+    goes_on = [mark_row(marks_ref, size * rows + r) for r in range(rows)]
+    is_last = [mark_row(marks_ref, (size + 1) * rows + r) > 0.5 for r in range(rows)]
+    tiles = [slice(r * SUBLANES, (r + 1) * SUBLANES) for r in range(rows)]
     for chunk in range(width // LANES):
         at = slice(chunk * LANES, (chunk + 1) * LANES)
         groups = slice(chunk * SUBLANES, (chunk + 1) * SUBLANES)
         fed = jnp.concatenate(
             [
-                jnp.where(own_group, jnp.broadcast_to(drive[t : t + 1, at], (SUBLANES, LANES)), 0.0)
-                for t in range(steps)
+                jnp.where(own_group, jnp.broadcast_to(drive[r : r + 1, at], (SUBLANES, LANES)), 0.0)
+                for r in range(rows)
             ],
             axis=0,
         ).astype(jnp.bfloat16)
         pushed = jnp.dot(twice(fed), coupled_ref[chunk], preferred_element_type=jnp.float32)
-        turned = pltpu.roll(pushed, half, 1)
         real, imag = real_ref[groups], imag_ref[groups]
-        value = state_ref[layer, 0, groups]
-        other = pltpu.roll(value, half, 1)
+        value = other = final = jnp.zeros((SUBLANES, LANES), jnp.float32)
         history = []
-        for t in range(steps):
-            now = slice(t * SUBLANES, (t + 1) * SUBLANES)
-            new_value = real * value + imag * other + pushed[now]
-            new_other = real * other - imag * value + turned[now]
-            value = jnp.where(keeps[t], new_value, value)
-            other = jnp.where(keeps[t], new_other, other)
+        for r in range(rows):
+            entering = pushed[tiles[r]] + carried_ref[r, groups]
+            turned = pltpu.roll(entering, half, 1)
+            value, other = (
+                goes_on[r] * (real * value + imag * other) + entering,
+                goes_on[r] * (real * other - imag * value) + turned,
+            )
             history.append(value)
-        next_ref[groups] = value
+            final = jnp.where(is_last[r], value, final)
+        next_ref[groups] = final
         high, low = halves(jnp.concatenate(history, axis=0))
         seen = jnp.dot(
             jnp.concatenate([high, low], axis=0), seen_ref[chunk], preferred_element_type=jnp.float32
         )
-        count = steps * SUBLANES
-        seen = seen[:count] + seen[count:]
+        seen = seen[: rows * SUBLANES] + seen[rows * SUBLANES :]
         read = jnp.concatenate(
-            [
-                jnp.sum(
-                    jnp.where(own_group, seen[t * SUBLANES : (t + 1) * SUBLANES], 0.0),
-                    axis=0,
-                    keepdims=True,
-                )
-                for t in range(steps)
-            ],
+            [jnp.sum(jnp.where(own_group, seen[tile], 0.0), axis=0, keepdims=True) for tile in tiles],
             axis=0,
         )
         response = read + skip_ref[layer : layer + 1, at].astype(jnp.float32) * drive[:, at]
-        value = jax.nn.gelu(response) * jax.nn.silu(gate[:, at]) * live_rows
-        branch_ref[:, at] = value.astype(jnp.bfloat16)
-
-
-def output_kernel(size, layer, *refs):
-    branch_refs, weight_ref, out_ref = refs[:size], refs[size], refs[size + 1]
-    rows = jnp.concatenate([ref[...].astype(jnp.float32) for ref in branch_refs], axis=0)
-    out_ref[...] = jnp.dot(
-        rows.astype(jnp.bfloat16), weight_ref[layer], preferred_element_type=jnp.float32
+        result = jax.nn.gelu(response) * jax.nn.silu(gate[:, at])
+        branch_ref[:, at] = result.astype(jnp.bfloat16)
+
+
+def state_kernel(size, layer, features, *refs):
+    part_ref, next_ref, branch_ref = refs[-3:]
+    advance(size, layer, features, refs[:-4], next_ref, branch_ref)
+    part_ref[...] = jnp.dot(
+        branch_ref[...], refs[-4][layer], preferred_element_type=jnp.float32
     ).astype(jnp.bfloat16)
 
 
-def last_output_kernel(size, layer, *refs):
-    branch_refs, weight_ref, base_ref = refs[:size], refs[size], refs[size + 1]
-    out_refs = refs[size + 2 :]
-    rows = jnp.concatenate([ref[...].astype(jnp.float32) for ref in branch_refs], axis=0)
-    value = jnp.dot(rows.astype(jnp.bfloat16), weight_ref[layer], preferred_element_type=jnp.float32)
-    count = rows.shape[0] // size
-    blocks = [value[k * count : (k + 1) * count] for k in range(size)]
-    offset = own_offset()
-    blocks = pick(blocks, offset)
-    base = base_ref[...]
-    bases = pick([base[k * count : (k + 1) * count] for k in range(size)], offset)
-    out_refs[0][...] = bases[0] + blocks[0]
-    for out_ref, block in zip(out_refs[1:], blocks[1:]):
-        out_ref[...] = block.astype(jnp.bfloat16)
+def last_state_kernel(size, layer, features, *refs):
+    ahead = len(refs) - (size + 2)
+    spread_ref, base_ref, own_ref, weight_ref = refs[ahead - 4 : ahead]
+    out_refs, (next_ref, branch_ref) = refs[ahead:-2], refs[-2:]
+    advance(size, layer, features, refs[: ahead - 4], next_ref, branch_ref)
+    part = jnp.dot(branch_ref[...], weight_ref[layer], preferred_element_type=jnp.float32)
+    steps = own_ref.shape[0]
+    spread = spread_ref[:, : 2 * part.shape[0]]
+
+    def place(chosen, rows):
+        rows = jnp.concatenate([rows, jnp.zeros_like(rows)], axis=0).astype(jnp.bfloat16)
+        return jnp.dot(chosen, rows, preferred_element_type=jnp.float32)
+
+    placed = place(spread, part)
+    base = place(spread, base_ref[...])[:steps]
+    live = jnp.sum(spread[:steps].astype(jnp.float32), axis=1, keepdims=True)
+    base = base + jnp.where(live > 0.5, 0.0, own_ref[...].astype(jnp.float32))
+    out_refs[0][...] = base + placed[:steps]
+    for k in range(1, size):
+        out_refs[k][...] = placed[k * steps : (k + 1) * steps].astype(jnp.bfloat16)
 
 
 def final_kernel(own_ref, *refs):
@@ -525,7 +574,9 @@
     whole_groups = state.shape[2] % LANES == 0 and state.shape[3] == LANES
     one_each = tokens.shape[0] == 1 and state.shape[1] == 1
     equal = dp_size == tp_size == lengths.shape[0]
-    return direct(dp_size) and equal and one_each and whole_groups and map_rows == S5_IN
+    one_tile = 2 * lengths.shape[0] == SUBLANES
+    whole_maps = one_tile and whole_groups and map_rows == S5_IN
+    return direct(dp_size) and equal and one_each and whole_maps
 
 
 def direct_steps(
@@ -547,51 +598,55 @@
     _, steps, features = tokens.shape
     inner = input_weight.shape[2]
     groups = state.shape[2]
-    count = size * steps
+    count = 2 * size
     bf16, f32 = jnp.bfloat16, jnp.float32
-    message = [((steps, 2 * inner + LANES), bf16)] * size
-    rows_shape = ((count, features), f32)
-    projections = (input_weight, gate_weight)
     decay, frequency = (jnp.swapaxes(value, 1, 2) for value in (decay_rate, frequency))
     raw = (decay, frequency, log_step, input_map, readout_map)
-    own = tokens.reshape(steps, features)
-    own, gain, live = bring_small(steps, lengths, own, norm_gain)
-    pieces = swaps(own, "tp", size)
-    pieces = [own] + pieces
-    real, imag, coupled, seen = prepare(0, *raw)
-    weights = projections
+    wide = state.reshape(LAYERS, groups, LANES)
+    own, gain, chosen, spread, marks = bring_small(
+        size, steps, count, lengths, tokens.reshape(steps, features), norm_gain
+    )
+    pieces = [own] + swaps(own, "tp", size)
+    (narrow,) = vmem_call(narrow_kernel, [(wide.shape, bf16)], wide, cost=COST)
+    carried = {0: wide}
+    carried.update(far_swaps(narrow, "dp", size))
+    weights = (gain, input_weight, gate_weight)
     states = []
     for layer in range(LAYERS):
         if layer == 0:
-            kernel, base = functools.partial(first_kernel, size), []
+            kernel, base = functools.partial(first_kernel, size), [chosen]
         else:
             kernel, base = functools.partial(next_kernel, size, layer), [rows]
-        results = vmem_call(kernel, message + [rows_shape], *base, *pieces, gain, *weights)
-        messages, rows = results[:size], results[size]
-        arrived = [messages[0]] + swaps(messages, "dp", size)
-        out_now = out_weight
-        branch, next_state = vmem_call(
-            functools.partial(state_kernel, size, layer, D),
-            [((steps, inner), bf16), ((groups, LANES), f32)],
-            *arrived, live, real, imag, coupled,
-            seen, skip_weight, state,
+        message, rows = vmem_call(
+            kernel,
+            [((count, 2 * inner + LANES), bf16), ((count, features), f32)],
+            *base, *pieces, *weights,
+        )
+        arrived = [message] + swaps(message, "dp", size)
+        if layer == 0:
+            near = [0] + [k for k in range(2, size, 2)]
+            for k in near:
+                carried[k + 1] = swap(carried[k] if k else narrow, "dp", 1, size)
+        fixed = prepare(layer, count, *raw, marks, [carried[k] for k in range(size)])
+        operands = [*arrived, marks, *fixed, skip_weight]
+        last = layer == LAYERS - 1
+        outs = [((groups, LANES), f32)]
+        scratch = [pltpu.VMEM((count, inner), bf16)]
+        if not last:
+            part, next_state = vmem_call(
+                functools.partial(state_kernel, size, layer, D),
+                [((count, features), bf16)] + outs,
+                *operands, out_weight, scratch=scratch,
+            )
+            states.append(next_state)
+            pieces = [part] + swaps(part, "tp", size)
+            continue
+        *parts, next_state = vmem_call(
+            functools.partial(last_state_kernel, size, layer, D),
+            [((steps, features), f32)] + [((steps, features), bf16)] * (size - 1) + outs,
+            *operands, spread, rows, own, out_weight, scratch=scratch,
         )
         states.append(next_state)
-        branches = [branch] + swaps(branch, "dp", size)
-        if layer < LAYERS - 1:
-            (part,) = vmem_call(
-                functools.partial(output_kernel, size, layer),
-                [((count, features), bf16)],
-                *branches, out_now,
-            )
-            pieces = [part] + swaps(part, "tp", size)
-            real, imag, coupled, seen = prepare(layer + 1, *raw, after=[part])
-            continue
-        parts = vmem_call(
-            functools.partial(last_output_kernel, size, layer),
-            [((steps, features), f32)] + [((steps, features), bf16)] * (size - 1),
-            *branches, out_now, rows,
-        )
         arrived = swaps(parts, "tp", size)
         (mixed,) = vmem_call(final_kernel, [((1, steps, features), bf16)], parts[0], *arrived)
     return mixed, jnp.stack(states)[:, None]

time: 50.9 us -> 51.7 us (1.016)
  starting transfers between devices: 22.2 us -> 20.4 us
  waiting for transfers between devices: 18.8 us -> 19.8 us
  local copies, waits for them, and re-layouts: 0.07 us -> 0.97 us
  Pallas kernels: 8.14 us -> 8.83 us
    ppermute x21 -> x18, starting transfers between devices: 22.2 us -> 20.4 us  [swap(): return lax.ppermute(value, axis, [(i, i ^ distance) for i in range(size)])]
    ppermute x21 -> x18, waiting for transfers between devices: 18.8 us -> 19.8 us  [swap(): return lax.ppermute(value, axis, [(i, i ^ distance) for i in range(size)])]
    unnamed x22 -> x28, local copies, waits for them, and re-layouts: 0.07 us -> 0.97 us
    pallas_call x10 -> x9, Pallas kernels: 8.14 us -> 8.83 us  [vmem_call(): pl.pallas_call(kernel, out_shape=outs, in_specs=in_specs, out_specs=[VMEM...]
  transfers between devices with their start and end apart: 21 -> 18, of which waited for: 15 -> 11; matrix products, arithmetic and copies ran while one was open for 1% -> 1% of each run, Pallas kernels for 3% -> 8%
where the time goes in v5:
time: 51.7 us; the launch traced here: 51.5 us
  starting transfers between devices  20.4 us (39%)
  waiting for transfers between devices  19.8 us (38%)
  Pallas kernels  8.83 us (17%)
  local copies, waits for them, and re-layouts  0.97 us (2%)
  between operations  0.86 us (2%)
  other arithmetic  0.67 us (1%)
    ppermute x18, starting transfers between devices, swap(): return lax.ppermute(value, axis, [(i, i ^ distance) for i in range(size)])  20.4 us
    ppermute x18, waiting for transfers between devices, swap(): return lax.ppermute(value, axis, [(i, i ^ distance) for i in range(size)])  19.8 us
    pallas_call x9, Pallas kernels, vmem_call(): pl.pallas_call(kernel, out_shape=outs, in_specs=in_specs, out_specs=[VMEM...  8.83 us
  transfers between devices with their start and end apart: 18, of which 11 were waited for; matrix products, arithmetic and copies ran while one was open for 1% of the time, Pallas kernels for 8%

profile of v5, /device:TPU:0, one launch (start us, length us, event | category | flops | bytes accessed | tf_op | source)
XLA Modules:
  0.0 51.5 jit_solution(18044968605309900552)
XLA Ops:
  0.6 0.0 copy-start.3
  0.6 0.9 %copy-done.3 = f32[2,1,128,128]{3,2,1,0:T(8,128)S(1)} copy-done((f32[2,1,128,128]{3,2,1,0:T(8,128)S(1)}, f32[2,1,128,128]{3,2,1,0:T(8,128)}, u32[]{:S(2)}) %copy-start.3) | copy-done | bytes 131096
  1.6 3.1 %collective-permute-start.7 = (bf16[2,128,128]{2,1,0:T(8,128)(2,1)S(1)}, bf16[2,128,128]{2,1,0:T(8,128)(2,1)S(1)}, u32[]{:S(2)}, u32[]{:S(2)}) collective-permute-start(bf16[2,128,128]{2,1,0:T(8,128)(2,1)S(1)} %shard_map.142), channel_id=1, source_target_pairs={{0,2},{1,3},{2,0},{3,1},{4,6},{5,7},{6,4},{7,5},{8,10},{9,11},{10,... | collective-permute-start | bytes 196616 | tf_op jit(solution)/shard_map/ppermute | solution.py:86
  4.6 0.0 collective-permute-start.6
  4.6 2.2 %collective-permute-done.7.refs_2_ = bf16[2,128,128]{2,1,0:T(8,128)(2,1)S(1)} collective-permute-done((bf16[2,128,128]{2,1,0:T(8,128)(2,1)S(1)}, bf16[2,128,128]{2,1,0:T(8,128)(2,1)S(1)}, u32[]{:S(2)}, u32[]{:S(2)}) %collective-permute-start.7) | collective-permute-done | bytes 65568 | tf_op jit(solution)/shard_map/ppermute | solution.py:86
  6.9 0.9 %shard_map.140 = (bf16[4,1024]{1,0:T(4,128)(2,1)S(1)}, f32[2,1024]{1,0:T(2,128)S(1)}, bf16[8,128]{1,0:T(8,128)(2,1)S(1)}, bf16[16,128]{1,0:T(8,128)(2,1)S(1)}, f32[48,128]{1,0:T(8,128)S(1)}) custom-call(s32[4]{0:T(128)} %lengths_hbm.1, bf16[4,1024]{1,0:T(4,128)(2,1)} %bitcast.25, f32[2,1024]{1,0:T(2,128)} %refs_1_.1), custom_call_target="tpu_custom_call" | custom-call | flops 40000000000 | tf_op jit(solution)/shard_map/pallas_call | solution.py:240
  7.8 2.1 %collective-permute-start = (bf16[4,1024]{1,0:T(4,128)(2,1)S(1)}, bf16[4,1024]{1,0:T(4,128)(2,1)S(1)}, u32[]{:S(2)}, u32[]{:S(2)}) collective-permute-start(bf16[4,1024]{1,0:T(4,128)(2,1)S(1)} %get-tuple-element.29.refs_0_.refs_13_), channel_id=1, source_target_pairs={{0,4},{4,0},{8,12},{12,8},{1,5},{5,1},{9,13},{13,9},{2,6},{6,2},{1... | collective-permute-start | bytes 24584 | tf_op jit(solution)/shard_map/ppermute | solution.py:86
  9.9 2.6 %collective-permute-start.1 = (bf16[4,1024]{1,0:T(4,128)(2,1)S(1)}, bf16[4,1024]{1,0:T(4,128)(2,1)S(1)}, u32[]{:S(2)}, u32[]{:S(2)}) collective-permute-start(bf16[4,1024]{1,0:T(4,128)(2,1)S(1)} %get-tuple-element.29.refs_0_.refs_13_), channel_id=1, source_target_pairs={{0,8},{4,12},{8,0},{12,4},{1,9},{5,13},{9,1},{13,5},{2,10},{6,14},... | collective-permute-start | bytes 24584 | tf_op jit(solution)/shard_map/ppermute | solution.py:86
  12.5 0.0 collective-permute-start.2
  12.5 0.0 collective-permute-done.refs_1_
  12.5 2.0 %collective-permute-done.1.refs_2_ = bf16[4,1024]{1,0:T(4,128)(2,1)S(1)} collective-permute-done((bf16[4,1024]{1,0:T(4,128)(2,1)S(1)}, bf16[4,1024]{1,0:T(4,128)(2,1)S(1)}, u32[]{:S(2)}, u32[]{:S(2)}) %collective-permute-start.1) | collective-permute-done | bytes 8224 | tf_op jit(solution)/shard_map/ppermute | solution.py:86
  14.5 3.5 %collective-permute-done.2.refs_3_ = bf16[4,1024]{1,0:T(4,128)(2,1)S(1)} collective-permute-done((bf16[4,1024]{1,0:T(4,128)(2,1)S(1)}, bf16[4,1024]{1,0:T(4,128)(2,1)S(1)}, u32[]{:S(2)}, u32[]{:S(2)}) %collective-permute-start.2) | collective-permute-done | bytes 8224 | tf_op jit(solution)/shard_map/ppermute | solution.py:86
  18.0 0.0 copy-start.1
  18.0 0.0 copy-start.2
  18.0 0.0 copy-start.4
  18.0 0.0 copy-start.5
  18.0 0.0 copy-start.6
  18.0 0.0 copy-start.7
  18.1 0.0 slice-start.4
  18.1 1.3 %shard_map.141 = (bf16[8,4224]{1,0:T(8,128)(2,1)S(1)}, f32[8,1024]{1,0:T(8,128)S(1)}) custom-call(bf16[8,128]{1,0:T(8,128)(2,1)S(1)} %get-tuple-element.28.pick_ref, bf16[4,1024]{1,0:T(4,128)(2,1)S(1)} %get-tuple-element.29.refs_0_.refs_13_, bf16[4,1024]{1,0:T(4,128)(2,1)S(1)} %collective-permute-done.refs_1_, ...), custom_call_target="tpu_custom_call" | custom-call | tf_op jit(solution)/shard_map/pallas_call | solution.py:240
  19.4 0.0 collective-permute-start.3
  19.4 1.6 %collective-permute-start.4 = (bf16[8,4224]{1,0:T(8,128)(2,1)S(1)}, bf16[8,4224]{1,0:T(8,128)(2,1)S(1)}, u32[]{:S(2)}, u32[]{:S(2)}) collective-permute-start(bf16[8,4224]{1,0:T(8,128)(2,1)S(1)} %get-tuple-element.32.refs_0_), channel_id=1, source_target_pairs={{0,2},{1,3},{2,0},{3,1},{4,6},{5,7},{6,4},{7,5},{8,10},{9,11},{10,... | collective-permute-start | bytes 202760 | tf_op jit(solution)/shard_map/ppermute | solution.py:86
  20.9 0.3 collective-permute-start.5
  21.2 0.0 collective-permute-done.6.refs_1_
  21.3 0.0 slice-start.5
  21.3 0.0 copy-start
  21.3 1.0 %shard_map.143 = (f32[128,128]{1,0:T(8,128)S(1)}, f32[128,128]{1,0:T(8,128)S(1)}, bf16[16,256,128]{2,1,0:T(8,128)(2,1)S(1)}, bf16[16,128,128]{2,1,0:T(8,128)(2,1)S(1)}, f32[8,128,128]{2,1,0:T(8,128)S(1)}) custom-call(f32[2,64,128]{2,1,0:T(8,128)S(1)} %bitcast.21, f32[2,64,128]{2,1,0:T(8,128)S(1)} %bitcast.23, f32[2,128]{1,0:T(2,128)S(1)} %copy-done.7, ...), custom_call_target="tpu_custom_call" | custom-call | flops 40000000000 | tf_op jit(solution)/shard_map/pallas_call | solution.py:240
  22.3 1.6 %collective-permute-done.4.refs_2_ = bf16[8,4224]{1,0:T(8,128)(2,1)S(1)} collective-permute-done((bf16[8,4224]{1,0:T(8,128)(2,1)S(1)}, bf16[8,4224]{1,0:T(8,128)(2,1)S(1)}, u32[]{:S(2)}, u32[]{:S(2)}) %collective-permute-start.4) | collective-permute-done | bytes 67616 | tf_op jit(solution)/shard_map/ppermute | solution.py:86
  23.9 1.1 %collective-permute-done.5.refs_3_ = bf16[8,4224]{1,0:T(8,128)(2,1)S(1)} collective-permute-done((bf16[8,4224]{1,0:T(8,128)(2,1)S(1)}, bf16[8,4224]{1,0:T(8,128)(2,1)S(1)}, u32[]{:S(2)}, u32[]{:S(2)}) %collective-permute-start.5) | collective-permute-done | bytes 67616 | tf_op jit(solution)/shard_map/ppermute | solution.py:86
  25.0 1.4 %shard_map.144 = (bf16[8,1024]{1,0:T(8,128)(2,1)S(1)}, f32[128,128]{1,0:T(8,128)S(1)}) custom-call(bf16[8,4224]{1,0:T(8,128)(2,1)S(1)} %get-tuple-element.32.refs_0_, bf16[8,4224]{1,0:T(8,128)(2,1)S(1)} %collective-permute-done.3.refs_1_, bf16[8,4224]{1,0:T(8,128)(2,1)S(1)} %collective-permute-done.4.refs_2_, ...), custom_call_target="tpu_custom_call" | custom-call | tf_op jit(solution)/shard_map/pallas_call | solution.py:240
  26.4 0.8 %collective-permute-start.10 = (bf16[8,1024]{1,0:T(8,128)(2,1)S(1)}, bf16[8,1024]{1,0:T(8,128)(2,1)S(1)}, u32[]{:S(2)}, u32[]{:S(2)}) collective-permute-start(bf16[8,1024]{1,0:T(8,128)(2,1)S(1)} %get-tuple-element.39.refs_0_), channel_id=1, source_target_pairs={{0,8},{4,12},{8,0},{12,4},{1,9},{5,13},{9,1},{13,5},{2,10},{6,14},... | collective-permute-start | bytes 49160 | tf_op jit(solution)/shard_map/ppermute | solution.py:86
  27.2 3.6 %collective-permute-start.11 = (bf16[8,1024]{1,0:T(8,128)(2,1)S(1)}, bf16[8,1024]{1,0:T(8,128)(2,1)S(1)}, u32[]{:S(2)}, u32[]{:S(2)}) collective-permute-start(bf16[8,1024]{1,0:T(8,128)(2,1)S(1)} %get-tuple-element.39.refs_0_), channel_id=1, source_target_pairs={{0,12},{4,8},{8,4},{12,0},{1,13},{5,9},{9,5},{13,1},{2,14},{6,10},... | collective-permute-start | bytes 49160 | tf_op jit(solution)/shard_map/ppermute | solution.py:86
  30.8 0.3 collective-permute-done.10.refs_2_
  31.1 1.6 %collective-permute-done.11.refs_3_ = bf16[8,1024]{1,0:T(8,128)(2,1)S(1)} collective-permute-done((bf16[8,1024]{1,0:T(8,128)(2,1)S(1)}, bf16[8,1024]{1,0:T(8,128)(2,1)S(1)}, u32[]{:S(2)}, u32[]{:S(2)}) %collective-permute-start.11) | collective-permute-done | bytes 16416 | tf_op jit(solution)/shard_map/ppermute | solution.py:86
  32.7 1.2 %shard_map.145 = (bf16[8,4224]{1,0:T(8,128)(2,1)S(1)}, f32[8,1024]{1,0:T(8,128)S(1)}) custom-call(f32[8,1024]{1,0:T(8,128)S(1)} %get-tuple-element.31.base_ref, bf16[8,1024]{1,0:T(8,128)(2,1)S(1)} %get-tuple-element.39.refs_0_, bf16[8,1024]{1,0:T(8,128)(2,1)S(1)} %collective-permute-done.9.refs_1_, bf16[8,1024]{1,0:T(8,128)(2,1)S(1)} %collective-permute-done.10.refs_2_, ...), custom_call_target="tpu_custom_call" | custom-call | tf_op jit(solution)/shard_map/pallas_call | solution.py:240
  33.9 1.5 %collective-permute-start.13 = (bf16[8,4224]{1,0:T(8,128)(2,1)S(1)}, bf16[8,4224]{1,0:T(8,128)(2,1)S(1)}, u32[]{:S(2)}, u32[]{:S(2)}) collective-permute-start(bf16[8,4224]{1,0:T(8,128)(2,1)S(1)} %get-tuple-element.40.refs_0_), channel_id=1, source_target_pairs={{0,2},{1,3},{2,0},{3,1},{4,6},{5,7},{6,4},{7,5},{8,10},{9,11},{10,... | collective-permute-start | bytes 202760 | tf_op jit(solution)/shard_map/ppermute | solution.py:86
  35.4 0.4 collective-permute-start.14
  35.8 1.0 %shard_map.146 = (f32[128,128]{1,0:T(8,128)S(1)}, f32[128,128]{1,0:T(8,128)S(1)}, bf16[16,256,128]{2,1,0:T(8,128)(2,1)S(1)}, bf16[16,128,128]{2,1,0:T(8,128)(2,1)S(1)}, f32[8,128,128]{2,1,0:T(8,128)S(1)}) custom-call(f32[2,64,128]{2,1,0:T(8,128)S(1)} %bitcast.22, f32[2,64,128]{2,1,0:T(8,128)S(1)} %bitcast.24, f32[2,128]{1,0:T(2,128)S(1)} %copy-done.7, ...), custom_call_target="tpu_custom_call" | custom-call | flops 40000000000 | tf_op jit(solution)/shard_map/pallas_call | solution.py:240
  36.8 1.8 %collective-permute-done.13.refs_2_ = bf16[8,4224]{1,0:T(8,128)(2,1)S(1)} collective-permute-done((bf16[8,4224]{1,0:T(8,128)(2,1)S(1)}, bf16[8,4224]{1,0:T(8,128)(2,1)S(1)}, u32[]{:S(2)}, u32[]{:S(2)}) %collective-permute-start.13) | collective-permute-done | bytes 67616 | tf_op jit(solution)/shard_map/ppermute | solution.py:86
  38.6 1.1 %collective-permute-done.14.refs_3_ = bf16[8,4224]{1,0:T(8,128)(2,1)S(1)} collective-permute-done((bf16[8,4224]{1,0:T(8,128)(2,1)S(1)}, bf16[8,4224]{1,0:T(8,128)(2,1)S(1)}, u32[]{:S(2)}, u32[]{:S(2)}) %collective-permute-start.14) | collective-permute-done | bytes 67616 | tf_op jit(solution)/shard_map/ppermute | solution.py:86
  39.7 1.5 %shard_map.147 = (f32[4,1024]{1,0:T(4,128)S(1)}, bf16[4,1024]{1,0:T(4,128)(2,1)S(1)}, bf16[4,1024]{1,0:T(4,128)(2,1)S(1)}, bf16[4,1024]{1,0:T(4,128)(2,1)S(1)}, f32[128,128]{1,0:T(8,128)S(1)}) custom-call(bf16[8,4224]{1,0:T(8,128)(2,1)S(1)} %get-tuple-element.40.refs_0_, bf16[8,4224]{1,0:T(8,128)(2,1)S(1)} %collective-permute-done.12.refs_1_, ...), custom_call_target="tpu_custom_call" | custom-call | tf_op jit(solution)/shard_map/pallas_call | solution.py:240
  41.2 0.5 collective-permute-start.15
  41.6 3.8 %collective-permute-start.16 = (bf16[4,1024]{1,0:T(4,128)(2,1)S(1)}, bf16[4,1024]{1,0:T(4,128)(2,1)S(1)}, u32[]{:S(2)}, u32[]{:S(2)}) collective-permute-start(bf16[4,1024]{1,0:T(4,128)(2,1)S(1)} %get-tuple-element.50), channel_id=1, source_target_pairs={{0,8},{4,12},{8,0},{12,4},{1,9},{5,13},{9,1},{13,5},{2,10},{6,14},... | collective-permute-start | bytes 24584 | tf_op jit(solution)/shard_map/ppermute | solution.py:86
  45.4 0.2 collective-permute-start.17
  45.6 0.7 %maximum_bitcast_fusion = f32[2,1,128,128]{3,2,1,0:T(8,128)} fusion(f32[1,128,128]{2,1,0:T(8,128)S(1)} %bitcast.17, f32[1,128,128]{2,1,0:T(8,128)S(1)} %bitcast.16), kind=kLoop, calls=%fused_computation | loop fusion | flops 32768 | bytes 262144
  46.3 0.8 %collective-permute-done.16.refs_1_ = bf16[4,1024]{1,0:T(4,128)(2,1)S(1)} collective-permute-done((bf16[4,1024]{1,0:T(4,128)(2,1)S(1)}, bf16[4,1024]{1,0:T(4,128)(2,1)S(1)}, u32[]{:S(2)}, u32[]{:S(2)}) %collective-permute-start.16) | collective-permute-done | bytes 8224 | tf_op jit(solution)/shard_map/ppermute | solution.py:86
  47.1 3.8 %collective-permute-done.17.refs_2_ = bf16[4,1024]{1,0:T(4,128)(2,1)S(1)} collective-permute-done((bf16[4,1024]{1,0:T(4,128)(2,1)S(1)}, bf16[4,1024]{1,0:T(4,128)(2,1)S(1)}, u32[]{:S(2)}, u32[]{:S(2)}) %collective-permute-start.17) | collective-permute-done | bytes 8224 | tf_op jit(solution)/shard_map/ppermute | solution.py:86
  50.9 0.6 %shard_map.148 = bf16[1,4,1024]{2,1,0:T(4,128)(2,1)} custom-call(f32[4,1024]{1,0:T(4,128)S(1)} %get-tuple-element.48.own_ref, bf16[4,1024]{1,0:T(4,128)(2,1)S(1)} %collective-permute-done.15.refs_0_, bf16[4,1024]{1,0:T(4,128)(2,1)S(1)} %collective-permute-done.16.refs_1_, bf16[4,1024]{1,0:T(4,128)(2,1)S(1)} %collective-permute-done.17.refs_2_), custom_call_target="tpu_custom_call" | custom-call | tf_op jit(solution)/shard_map/pallas_call | solution.py:240
  (29 shorter events, 0.1 us)
Async XLA Ops:
  0.6 0.9 %copy-start.3 = (f32[2,1,128,128]{3,2,1,0:T(8,128)S(1)}, f32[2,1,128,128]{3,2,1,0:T(8,128)}, u32[]{:S(2)}) copy-start(f32[2,1,128,128]{3,2,1,0:T(8,128)} %param.25) | copy-start | bytes 393220
  1.5 16.4 %slice-start = ((s8[8388608]{0:T(1024)(128)(4,1)}), s8[4194304]{0:T(1024)(128)(4,1)S(1)}, s32[]{:S(2)}) async-start(s8[8388608]{0:T(1024)(128)(4,1)} %bitcast.10), calls=%async_computation | async-start | bytes 8388608
  1.5 16.4 %slice-start.2 = ((s8[8388608]{0:T(1024)(128)(4,1)}), s8[4194304]{0:T(1024)(128)(4,1)S(1)}, s32[]{:S(2)}) async-start(s8[8388608]{0:T(1024)(128)(4,1)} %bitcast.12), calls=%async_computation.2 | async-start | bytes 8388608
  1.6 5.3 %collective-permute-start.7 = (bf16[2,128,128]{2,1,0:T(8,128)(2,1)S(1)}, bf16[2,128,128]{2,1,0:T(8,128)(2,1)S(1)}, u32[]{:S(2)}, u32[]{:S(2)}) collective-permute-start(bf16[2,128,128]{2,1,0:T(8,128)(2,1)S(1)} %shard_map.142), channel_id=1, source_target_pairs={{0,2},{1,3},{2,0},{3,1},{4,6},{5,7},{6,4},{7,5},{8,10},{9,11},{10,... | collective-permute-start | bytes 196616 | tf_op jit(solution)/shard_map/ppermute | solution.py:86
  4.6 16.6 %collective-permute-start.6 = (bf16[2,128,128]{2,1,0:T(8,128)(2,1)S(1)}, bf16[2,128,128]{2,1,0:T(8,128)(2,1)S(1)}, u32[]{:S(2)}, u32[]{:S(2)}) collective-permute-start(bf16[2,128,128]{2,1,0:T(8,128)(2,1)S(1)} %shard_map.142), channel_id=1, source_target_pairs={{0,1},{1,0},{2,3},{3,2},{4,5},{5,4},{6,7},{7,6},{8,9},{9,8},{10,11... | collective-permute-start | bytes 196616 | tf_op jit(solution)/shard_map/ppermute | solution.py:86
  6.9 14.4 %collective-permute-start.8 = (bf16[2,128,128]{2,1,0:T(8,128)(2,1)S(1)}, bf16[2,128,128]{2,1,0:T(8,128)(2,1)S(1)}, u32[]{:S(2)}, u32[]{:S(2)}) collective-permute-start(bf16[2,128,128]{2,1,0:T(8,128)(2,1)S(1)} %collective-permute-done.7.refs_2_), channel_id=1, source_target_pairs={{0,1},{1,0},{2,3},{3,2},{4,5},{5,4},{6,7},{7,6},{8,9},{9,8},{10,11... | collective-permute-start | bytes 196616 | tf_op jit(solution)/shard_map/ppermute | solution.py:86
  6.9 11.1 %slice-start.1 = ((s8[8388608]{0:T(1024)(128)(4,1)}), s8[4194304]{0:T(1024)(128)(4,1)S(1)}, s32[]{:S(2)}) async-start(s8[8388608]{0:T(1024)(128)(4,1)} %bitcast.10), calls=%async_computation.1 | async-start | bytes 8388608
  6.9 11.1 %slice-start.3 = ((s8[8388608]{0:T(1024)(128)(4,1)}), s8[4194304]{0:T(1024)(128)(4,1)S(1)}, s32[]{:S(2)}) async-start(s8[8388608]{0:T(1024)(128)(4,1)} %bitcast.12), calls=%async_computation.3 | async-start | bytes 8388608
  7.8 4.7 %collective-permute-start = (bf16[4,1024]{1,0:T(4,128)(2,1)S(1)}, bf16[4,1024]{1,0:T(4,128)(2,1)S(1)}, u32[]{:S(2)}, u32[]{:S(2)}) collective-permute-start(bf16[4,1024]{1,0:T(4,128)(2,1)S(1)} %get-tuple-element.29.refs_0_.refs_13_), channel_id=1, source_target_pairs={{0,4},{4,0},{8,12},{12,8},{1,5},{5,1},{9,13},{13,9},{2,6},{6,2},{1... | collective-permute-start | bytes 24584 | tf_op jit(solution)/shard_map/ppermute | solution.py:86
  9.9 4.5 %collective-permute-start.1 = (bf16[4,1024]{1,0:T(4,128)(2,1)S(1)}, bf16[4,1024]{1,0:T(4,128)(2,1)S(1)}, u32[]{:S(2)}, u32[]{:S(2)}) collective-permute-start(bf16[4,1024]{1,0:T(4,128)(2,1)S(1)} %get-tuple-element.29.refs_0_.refs_13_), channel_id=1, source_target_pairs={{0,8},{4,12},{8,0},{12,4},{1,9},{5,13},{9,1},{13,5},{2,10},{6,14},... | collective-permute-start | bytes 24584 | tf_op jit(solution)/shard_map/ppermute | solution.py:86
  12.5 5.4 %collective-permute-start.2 = (bf16[4,1024]{1,0:T(4,128)(2,1)S(1)}, bf16[4,1024]{1,0:T(4,128)(2,1)S(1)}, u32[]{:S(2)}, u32[]{:S(2)}) collective-permute-start(bf16[4,1024]{1,0:T(4,128)(2,1)S(1)} %get-tuple-element.29.refs_0_.refs_13_), channel_id=1, source_target_pairs={{0,12},{4,8},{8,4},{12,0},{1,13},{5,9},{9,5},{13,1},{2,14},{6,10},... | collective-permute-start | bytes 24584 | tf_op jit(solution)/shard_map/ppermute | solution.py:86
  18.0 3.3 %copy-start.1 = (bf16[2,128,16,128]{3,2,1,0:T(8,128)(2,1)S(1)}, bf16[2,128,16,128]{3,2,1,0:T(8,128)(2,1)}, u32[]{:S(2)}) copy-start(bf16[2,128,16,128]{3,2,1,0:T(8,128)(2,1)} %map_ref.3) | copy-start | bytes 3145732
  18.0 3.3 %copy-start.2 = (bf16[2,128,16,128]{3,2,1,0:T(8,128)(2,1)S(1)}, bf16[2,128,16,128]{3,2,1,0:T(8,128)(2,1)}, u32[]{:S(2)}) copy-start(bf16[2,128,16,128]{3,2,1,0:T(8,128)(2,1)} %readout_ref.3) | copy-start | bytes 3145732
  18.0 3.3 %copy-start.4 = (f32[2,1,128,128]{3,2,1,0:T(8,128)S(1)}, f32[2,1,128,128]{3,2,1,0:T(8,128)}, u32[]{:S(2)}) copy-start(f32[2,1,128,128]{3,2,1,0:T(8,128)} %param.25) | copy-start | bytes 393220
  18.0 3.3 %copy-start.5 = (f32[2,128,64]{1,2,0:T(8,128)S(1)}, f32[2,128,64]{1,2,0:T(8,128)}, u32[]{:S(2)}) copy-start(f32[2,128,64]{1,2,0:T(8,128)} %param.18) | copy-start | bytes 196612
  18.0 3.3 %copy-start.6 = (f32[2,128,64]{1,2,0:T(8,128)S(1)}, f32[2,128,64]{1,2,0:T(8,128)}, u32[]{:S(2)}) copy-start(f32[2,128,64]{1,2,0:T(8,128)} %param.19) | copy-start | bytes 196612
  18.0 3.3 %copy-start.7 = (f32[2,128]{1,0:T(2,128)S(1)}, f32[2,128]{1,0:T(2,128)}, u32[]{:S(2)}) copy-start(f32[2,128]{1,0:T(2,128)} %log_step_ref.3) | copy-start | bytes 3076
  18.1 7.0 %slice-start.4 = ((s8[8388608]{0:T(1024)(128)(4,1)}), s8[4194304]{0:T(1024)(128)(4,1)S(1)}, s32[]{:S(2)}) async-start(s8[8388608]{0:T(1024)(128)(4,1)} %bitcast.14), calls=%async_computation.4 | async-start | bytes 8388608
  19.4 3.0 %collective-permute-start.3 = (bf16[8,4224]{1,0:T(8,128)(2,1)S(1)}, bf16[8,4224]{1,0:T(8,128)(2,1)S(1)}, u32[]{:S(2)}, u32[]{:S(2)}) collective-permute-start(bf16[8,4224]{1,0:T(8,128)(2,1)S(1)} %get-tuple-element.32.refs_0_), channel_id=1, source_target_pairs={{0,1},{1,0},{2,3},{3,2},{4,5},{5,4},{6,7},{7,6},{8,9},{9,8},{10,11... | collective-permute-start | bytes 202760 | tf_op jit(solution)/shard_map/ppermute | solution.py:86
  19.4 4.6 %collective-permute-start.4 = (bf16[8,4224]{1,0:T(8,128)(2,1)S(1)}, bf16[8,4224]{1,0:T(8,128)(2,1)S(1)}, u32[]{:S(2)}, u32[]{:S(2)}) collective-permute-start(bf16[8,4224]{1,0:T(8,128)(2,1)S(1)} %get-tuple-element.32.refs_0_), channel_id=1, source_target_pairs={{0,2},{1,3},{2,0},{3,1},{4,6},{5,7},{6,4},{7,5},{8,10},{9,11},{10,... | collective-permute-start | bytes 202760 | tf_op jit(solution)/shard_map/ppermute | solution.py:86
  20.9 4.1 %collective-permute-start.5 = (bf16[8,4224]{1,0:T(8,128)(2,1)S(1)}, bf16[8,4224]{1,0:T(8,128)(2,1)S(1)}, u32[]{:S(2)}, u32[]{:S(2)}) collective-permute-start(bf16[8,4224]{1,0:T(8,128)(2,1)S(1)} %get-tuple-element.32.refs_0_), channel_id=1, source_target_pairs={{0,3},{1,2},{2,1},{3,0},{4,7},{5,6},{6,5},{7,4},{8,11},{9,10},{10,... | collective-permute-start | bytes 202760 | tf_op jit(solution)/shard_map/ppermute | solution.py:86
  21.3 3.7 %slice-start.5 = ((s8[8388608]{0:T(1024)(128)(4,1)}), s8[4194304]{0:T(1024)(128)(4,1)S(1)}, s32[]{:S(2)}) async-start(s8[8388608]{0:T(1024)(128)(4,1)} %bitcast.14), calls=%async_computation.5 | async-start | bytes 8388608
  21.3 3.7 %copy-start = (bf16[2,2048]{1,0:T(2,128)(2,1)S(1)}, bf16[2,2048]{1,0:T(2,128)(2,1)}, u32[]{:S(2)}) copy-start(bf16[2,2048]{1,0:T(2,128)(2,1)} %refs_10_.3) | copy-start | bytes 24580
  26.4 4.4 %collective-permute-start.9 = (bf16[8,1024]{1,0:T(8,128)(2,1)S(1)}, bf16[8,1024]{1,0:T(8,128)(2,1)S(1)}, u32[]{:S(2)}, u32[]{:S(2)}) collective-permute-start(bf16[8,1024]{1,0:T(8,128)(2,1)S(1)} %get-tuple-element.39.refs_0_), channel_id=1, source_target_pairs={{0,4},{4,0},{8,12},{12,8},{1,5},{5,1},{9,13},{13,9},{2,6},{6,2},{1... | collective-permute-start | bytes 49160 | tf_op jit(solution)/shard_map/ppermute | solution.py:86
  26.4 4.7 %collective-permute-start.10 = (bf16[8,1024]{1,0:T(8,128)(2,1)S(1)}, bf16[8,1024]{1,0:T(8,128)(2,1)S(1)}, u32[]{:S(2)}, u32[]{:S(2)}) collective-permute-start(bf16[8,1024]{1,0:T(8,128)(2,1)S(1)} %get-tuple-element.39.refs_0_), channel_id=1, source_target_pairs={{0,8},{4,12},{8,0},{12,4},{1,9},{5,13},{9,1},{13,5},{2,10},{6,14},... | collective-permute-start | bytes 49160 | tf_op jit(solution)/shard_map/ppermute | solution.py:86
  27.2 5.5 %collective-permute-start.11 = (bf16[8,1024]{1,0:T(8,128)(2,1)S(1)}, bf16[8,1024]{1,0:T(8,128)(2,1)S(1)}, u32[]{:S(2)}, u32[]{:S(2)}) collective-permute-start(bf16[8,1024]{1,0:T(8,128)(2,1)S(1)} %get-tuple-element.39.refs_0_), channel_id=1, source_target_pairs={{0,12},{4,8},{8,4},{12,0},{1,13},{5,9},{9,5},{13,1},{2,14},{6,10},... | collective-permute-start | bytes 49160 | tf_op jit(solution)/shard_map/ppermute | solution.py:86
  33.9 2.9 %collective-permute-start.12 = (bf16[8,4224]{1,0:T(8,128)(2,1)S(1)}, bf16[8,4224]{1,0:T(8,128)(2,1)S(1)}, u32[]{:S(2)}, u32[]{:S(2)}) collective-permute-start(bf16[8,4224]{1,0:T(8,128)(2,1)S(1)} %get-tuple-element.40.refs_0_), channel_id=1, source_target_pairs={{0,1},{1,0},{2,3},{3,2},{4,5},{5,4},{6,7},{7,6},{8,9},{9,8},{10,11... | collective-permute-start | bytes 202760 | tf_op jit(solution)/shard_map/ppermute | solution.py:86
  33.9 4.7 %collective-permute-start.13 = (bf16[8,4224]{1,0:T(8,128)(2,1)S(1)}, bf16[8,4224]{1,0:T(8,128)(2,1)S(1)}, u32[]{:S(2)}, u32[]{:S(2)}) collective-permute-start(bf16[8,4224]{1,0:T(8,128)(2,1)S(1)} %get-tuple-element.40.refs_0_), channel_id=1, source_target_pairs={{0,2},{1,3},{2,0},{3,1},{4,6},{5,7},{6,4},{7,5},{8,10},{9,11},{10,... | collective-permute-start | bytes 202760 | tf_op jit(solution)/shard_map/ppermute | solution.py:86
  35.4 4.3 %collective-permute-start.14 = (bf16[8,4224]{1,0:T(8,128)(2,1)S(1)}, bf16[8,4224]{1,0:T(8,128)(2,1)S(1)}, u32[]{:S(2)}, u32[]{:S(2)}) collective-permute-start(bf16[8,4224]{1,0:T(8,128)(2,1)S(1)} %get-tuple-element.40.refs_0_), channel_id=1, source_target_pairs={{0,3},{1,2},{2,1},{3,0},{4,7},{5,6},{6,5},{7,4},{8,11},{9,10},{10,... | collective-permute-start | bytes 202760 | tf_op jit(solution)/shard_map/ppermute | solution.py:86
  41.2 5.1 %collective-permute-start.15 = (bf16[4,1024]{1,0:T(4,128)(2,1)S(1)}, bf16[4,1024]{1,0:T(4,128)(2,1)S(1)}, u32[]{:S(2)}, u32[]{:S(2)}) collective-permute-start(bf16[4,1024]{1,0:T(4,128)(2,1)S(1)} %get-tuple-element.49), channel_id=1, source_target_pairs={{0,4},{4,0},{8,12},{12,8},{1,5},{5,1},{9,13},{13,9},{2,6},{6,2},{1... | collective-permute-start | bytes 24584 | tf_op jit(solution)/shard_map/ppermute | solution.py:86
  41.6 5.4 %collective-permute-start.16 = (bf16[4,1024]{1,0:T(4,128)(2,1)S(1)}, bf16[4,1024]{1,0:T(4,128)(2,1)S(1)}, u32[]{:S(2)}, u32[]{:S(2)}) collective-permute-start(bf16[4,1024]{1,0:T(4,128)(2,1)S(1)} %get-tuple-element.50), channel_id=1, source_target_pairs={{0,8},{4,12},{8,0},{12,4},{1,9},{5,13},{9,1},{13,5},{2,10},{6,14},... | collective-permute-start | bytes 24584 | tf_op jit(solution)/shard_map/ppermute | solution.py:86
  45.4 5.4 %collective-permute-start.17 = (bf16[4,1024]{1,0:T(4,128)(2,1)S(1)}, bf16[4,1024]{1,0:T(4,128)(2,1)S(1)}, u32[]{:S(2)}, u32[]{:S(2)}) collective-permute-start(bf16[4,1024]{1,0:T(4,128)(2,1)S(1)} %get-tuple-element.51), channel_id=1, source_target_pairs={{0,12},{4,8},{8,4},{12,0},{1,13},{5,9},{9,5},{13,1},{2,14},{6,10},... | collective-permute-start | bytes 24584 | tf_op jit(solution)/shard_map/ppermute | solution.py:86

commit v6 on v5

--- a/solution.py
+++ b/solution.py
@@ -223,6 +223,7 @@
     return (own_block, jnp.stack(states))
 
 
+SMALL_COST = 4000000
 LANES = 128
 COST = 40000000000
 SUBLANES = 8
@@ -351,15 +352,19 @@
         + [((chunks, size, LANES), jnp.bfloat16) for size in (2 * LANES, LANES)]
         + [((rows, groups, LANES), jnp.float32)],
         decay, frequency, log_step, input_map, readout_map, marks, *states,
-        cost=COST,
-    )
+        cost=SMALL_COST,
+    )
+
+
+def primer_kernel(out_ref):
+    out_ref[...] = jnp.zeros_like(out_ref)
 
 
 def narrow_kernel(state_ref, out_ref):
     out_ref[...] = state_ref[...].astype(jnp.bfloat16)
 
 
-def small_kernel(size, steps, lengths_hbm, *refs):
+def small_kernel(size, steps, primer_ref, lengths_hbm, *refs):
     count = (len(refs) - 5) // 2
     sources, targets = refs[:count], refs[count : 2 * count]
     pick_ref, spread_ref, marks_ref, lengths, semaphores = refs[2 * count :]
@@ -378,9 +383,10 @@
 
     row, lane = places((rows, LANES))
     chosen = jnp.zeros((rows, LANES), jnp.float32)
-    for s in range(size):
-        t = lane - s * steps
-        hit = (t >= 0) & (t < length[s]) & (row == offset[s] + t)
+    for k in range(size):
+        t = lane - k * steps
+        start, live = of(offset, tp_index ^ k), of(length, tp_index ^ k)
+        hit = (t >= 0) & (t < live) & (row == start + t)
         chosen = jnp.where(hit, 1.0, chosen)
     pick_ref[...] = chosen.astype(jnp.bfloat16)
     row, lane = places((size * steps, LANES))
@@ -403,25 +409,25 @@
     wait_copies(copies[1:])
 
 
-def bring_small(size, steps, rows, lengths, *arrays):
+def bring_small(size, steps, rows, primer, lengths, *arrays):
     return vmem_call(
         functools.partial(small_kernel, size, steps),
         [(a.shape, a.dtype) for a in arrays]
         + [((rows, LANES), jnp.bfloat16), ((size * steps, LANES), jnp.bfloat16)]
         + [(((size + 2) * rows, LANES), jnp.float32)],
-        lengths, *arrays,
-        in_specs=[HBM] * (1 + len(arrays)),
+        primer, lengths, *arrays,
+        in_specs=[VMEM] + [HBM] * (1 + len(arrays)),
         scratch=[
             pltpu.SMEM(lengths.shape, jnp.int32),
             pltpu.SemaphoreType.DMA((1 + len(arrays),)),
         ],
-        cost=COST,
+        cost=SMALL_COST,
     )
 
 
 def far_swaps(value, axis, size):
     received = {}
-    for k in range(2, size, 2):
+    for k in range(3, size, 2):
         received[k] = swap(value, axis, k, size)
     return received
 
@@ -454,20 +460,11 @@
             message_ref[:, base + at : base + at + step] = value.astype(jnp.bfloat16)
 
 
-def pick(blocks, offset):
-    bit = 1
-    while bit < len(blocks):
-        on = (offset & bit) != 0
-        blocks = [jnp.where(on, blocks[k ^ bit], blocks[k]) for k in range(len(blocks))]
-        bit *= 2
-    return blocks
-
-
 def first_kernel(size, pick_ref, *refs):
     block_refs, (gain_ref, drive_ref, gate_ref) = refs[:size], refs[size : size + 3]
     message_ref, rows_ref = refs[size + 3 :]
     blocks = [ref[...].astype(jnp.float32) for ref in block_refs]
-    blocks = jnp.concatenate(pick(blocks, lax.axis_index("tp")), axis=0).astype(jnp.bfloat16)
+    blocks = jnp.concatenate(blocks, axis=0).astype(jnp.bfloat16)
     chosen = pick_ref[:, : blocks.shape[0]]
     rows = jnp.dot(chosen, blocks, preferred_element_type=jnp.float32)
     rows_ref[...] = rows
@@ -603,11 +600,14 @@
     decay, frequency = (jnp.swapaxes(value, 1, 2) for value in (decay_rate, frequency))
     raw = (decay, frequency, log_step, input_map, readout_map)
     wide = state.reshape(LAYERS, groups, LANES)
+    (primer,) = vmem_call(primer_kernel, [((SUBLANES, LANES), f32)], cost=COST)
+    own = tokens.reshape(steps, features)
+    pieces = swaps(own, "tp", size)
     own, gain, chosen, spread, marks = bring_small(
-        size, steps, count, lengths, tokens.reshape(steps, features), norm_gain
-    )
-    pieces = [own] + swaps(own, "tp", size)
-    (narrow,) = vmem_call(narrow_kernel, [(wide.shape, bf16)], wide, cost=COST)
+        size, steps, count, primer, lengths, own, norm_gain
+    )
+    pieces = [own] + pieces
+    (narrow,) = vmem_call(narrow_kernel, [(wide.shape, bf16)], wide, cost=SMALL_COST)
     carried = {0: wide}
     carried.update(far_swaps(narrow, "dp", size))
     weights = (gain, input_weight, gate_weight)
@@ -624,9 +624,8 @@
         )
         arrived = [message] + swaps(message, "dp", size)
         if layer == 0:
-            near = [0] + [k for k in range(2, size, 2)]
-            for k in near:
-                carried[k + 1] = swap(carried[k] if k else narrow, "dp", 1, size)
+            for k in [0] + [k for k in range(3, size, 2)]:
+                carried[k ^ 1] = swap(carried[k] if k else narrow, "dp", 1, size)
         fixed = prepare(layer, count, *raw, marks, [carried[k] for k in range(size)])
         operands = [*arrived, marks, *fixed, skip_weight]
         last = layer == LAYERS - 1

time: 51.7 us -> 47 us (0.909)
  waiting for transfers between devices: 19.8 us -> 15 us
  local copies, waits for them, and re-layouts: 0.97 us -> 2.1 us
  starting transfers between devices: 20.4 us -> 19.3 us
    ppermute x18, waiting for transfers between devices: 19.8 us -> 15 us  [swap(): return lax.ppermute(value, axis, [(i, i ^ distance) for i in range(size)])]
    unnamed x28 -> x26, local copies, waits for them, and re-layouts: 0.97 us -> 2.1 us
    ppermute x18, starting transfers between devices: 20.4 us -> 19.3 us  [swap(): return lax.ppermute(value, axis, [(i, i ^ distance) for i in range(size)])]
    pallas_call x9 -> x10, Pallas kernels: 8.83 us -> 8.9 us  [vmem_call(): pl.pallas_call(kernel, out_shape=outs, in_specs=in_specs, out_specs=[VMEM...]
  transfers between devices with their start and end apart: 18 -> 18, of which waited for: 11 -> 10; matrix products, arithmetic and copies ran while one was open for 1% -> 1% of each run, Pallas kernels for 8% -> 9%
where the time goes in v6:
time: 47 us; the launch traced here: 46.8 us
  starting transfers between devices  19.3 us (41%)
  waiting for transfers between devices  15 us (32%)
  Pallas kernels  8.9 us (19%)
  local copies, waits for them, and re-layouts  2.1 us (4%)
  between operations  0.82 us (2%)
  other arithmetic  0.66 us (1%)
    ppermute x18, starting transfers between devices, swap(): return lax.ppermute(value, axis, [(i, i ^ distance) for i in range(size)])  19.3 us
    ppermute x18, waiting for transfers between devices, swap(): return lax.ppermute(value, axis, [(i, i ^ distance) for i in range(size)])  15 us
    pallas_call x10, Pallas kernels, vmem_call(): pl.pallas_call(kernel, out_shape=outs, in_specs=in_specs, out_specs=[VMEM...  8.9 us
    unnamed x26, local copies, waits for them, and re-layouts  2.1 us
  transfers between devices with their start and end apart: 18, of which 10 were waited for; matrix products, arithmetic and copies ran while one was open for 1% of the time, Pallas kernels for 9%

profile of v6, /device:TPU:0, one launch (start us, length us, event | category | flops | bytes accessed | tf_op | source)
XLA Modules:
  0.0 46.8 jit_solution(565315208841041877)
XLA Ops:
  0.6 3.1 %collective-permute-start = (bf16[4,1024]{1,0:T(4,128)(2,1)}, bf16[4,1024]{1,0:T(4,128)(2,1)S(1)}, u32[]{:S(2)}, u32[]{:S(2)}) collective-permute-start(bf16[4,1024]{1,0:T(4,128)(2,1)} %bitcast.23), channel_id=1, source_target_pairs={{0,4},{4,0},{8,12},{12,8},{1,5},{5,1},{9,13},{13,9},{2,6},{6,2},{1... | collective-permute-start | bytes 24584 | tf_op jit(solution)/shard_map/ppermute | solution.py:86
  3.7 2.6 %collective-permute-start.1 = (bf16[4,1024]{1,0:T(4,128)(2,1)}, bf16[4,1024]{1,0:T(4,128)(2,1)S(1)}, u32[]{:S(2)}, u32[]{:S(2)}) collective-permute-start(bf16[4,1024]{1,0:T(4,128)(2,1)} %bitcast.24), channel_id=1, source_target_pairs={{0,8},{4,12},{8,0},{12,4},{1,9},{5,13},{9,1},{13,5},{2,10},{6,14},... | collective-permute-start | bytes 24584 | tf_op jit(solution)/shard_map/ppermute | solution.py:86
  6.3 0.0 collective-permute-start.2
  6.3 0.9 %copy-done.3 = f32[2,1,128,128]{3,2,1,0:T(8,128)S(1)} copy-done((f32[2,1,128,128]{3,2,1,0:T(8,128)S(1)}, f32[2,1,128,128]{3,2,1,0:T(8,128)}, u32[]{:S(2)}) %copy-start.3) | copy-done | bytes 131096
  7.3 0.0 slice-start.1
  7.3 0.0 slice-start.3
  7.3 0.5 collective-permute-start.7
  7.8 1.0 %shard_map.141 = (bf16[4,1024]{1,0:T(4,128)(2,1)S(1)}, f32[2,1024]{1,0:T(2,128)S(1)}, bf16[8,128]{1,0:T(8,128)(2,1)S(1)}, bf16[16,128]{1,0:T(8,128)(2,1)S(1)}, f32[48,128]{1,0:T(8,128)S(1)}) custom-call(f32[8,128]{1,0:T(8,128)S(1)} %shard_map.140.primer_ref, s32[4]{0:T(128)} %lengths_hbm.1, bf16[4,1024]{1,0:T(4,128)(2,1)} %bitcast.26, f32[2,1024]{1,0:T(2,128)} %refs_1_.1), custom_call_target="tpu_custom_call" | custom-call | flops 4000000 | tf_op jit(solution)/shard_map/pallas_call | solution.py:241
  8.7 0.0 collective-permute-done.refs_1_
  8.8 0.0 collective-permute-done.1.refs_2_
  8.8 3.2 %collective-permute-done.2.refs_3_ = bf16[4,1024]{1,0:T(4,128)(2,1)S(1)} collective-permute-done((bf16[4,1024]{1,0:T(4,128)(2,1)}, bf16[4,1024]{1,0:T(4,128)(2,1)S(1)}, u32[]{:S(2)}, u32[]{:S(2)}) %collective-permute-start.2) | collective-permute-done | bytes 8224 | tf_op jit(solution)/shard_map/ppermute | solution.py:86
  12.0 1.1 %slice-done.3 = s8[4194304]{0:T(1024)(128)(4,1)S(1)} async-done(((s8[8388608]{0:T(1024)(128)(4,1)}), s8[4194304]{0:T(1024)(128)(4,1)S(1)}, s32[]{:S(2)}) %slice-start.3) | async-done | bytes 4194328
  13.1 0.0 copy-start.5
  13.2 0.0 copy-start.6
  13.2 0.0 copy-start.8
  13.2 0.0 copy-start
  13.2 0.0 copy-start.7
  13.2 1.3 %shard_map.142 = (bf16[8,4224]{1,0:T(8,128)(2,1)S(1)}, f32[8,1024]{1,0:T(8,128)S(1)}) custom-call(bf16[8,128]{1,0:T(8,128)(2,1)S(1)} %get-tuple-element.28.pick_ref, bf16[4,1024]{1,0:T(4,128)(2,1)S(1)} %get-tuple-element.29.refs_0_.refs_13_, bf16[4,1024]{1,0:T(4,128)(2,1)S(1)} %collective-permute-done.refs_1_, ...), custom_call_target="tpu_custom_call" | custom-call | tf_op jit(solution)/shard_map/pallas_call | solution.py:241
  14.5 1.8 %collective-permute-start.4 = (bf16[8,4224]{1,0:T(8,128)(2,1)S(1)}, bf16[8,4224]{1,0:T(8,128)(2,1)S(1)}, u32[]{:S(2)}, u32[]{:S(2)}) collective-permute-start(bf16[8,4224]{1,0:T(8,128)(2,1)S(1)} %get-tuple-element.32.refs_0_), channel_id=1, source_target_pairs={{0,2},{1,3},{2,0},{3,1},{4,6},{5,7},{6,4},{7,5},{8,10},{9,11},{10,... | collective-permute-start | bytes 202760 | tf_op jit(solution)/shard_map/ppermute | solution.py:86
  16.3 0.1 collective-permute-start.5
  16.4 0.3 collective-permute-start.6
  16.7 0.2 collective-permute-start.8
  16.9 0.7 %collective-permute-done.6.refs_1_ = bf16[2,128,128]{2,1,0:T(8,128)(2,1)S(1)} collective-permute-done((bf16[2,128,128]{2,1,0:T(8,128)(2,1)S(1)}, bf16[2,128,128]{2,1,0:T(8,128)(2,1)S(1)}, u32[]{:S(2)}, u32[]{:S(2)}) %collective-permute-start.6) | collective-permute-done | bytes 65568 | tf_op jit(solution)/shard_map/ppermute | solution.py:86
  17.6 0.3 collective-permute-done.8.refs_2_
  18.0 1.0 %shard_map.144 = (f32[128,128]{1,0:T(8,128)S(1)}, f32[128,128]{1,0:T(8,128)S(1)}, bf16[16,256,128]{2,1,0:T(8,128)(2,1)S(1)}, bf16[16,128,128]{2,1,0:T(8,128)(2,1)S(1)}, f32[8,128,128]{2,1,0:T(8,128)S(1)}) custom-call(f32[2,64,128]{2,1,0:T(8,128)S(1)} %bitcast.17, f32[2,64,128]{2,1,0:T(8,128)S(1)} %bitcast.19, f32[2,128]{1,0:T(2,128)S(1)} %copy-done.8, ...), custom_call_target="tpu_custom_call" | custom-call | flops 4000000 | tf_op jit(solution)/shard_map/pallas_call | solution.py:241
  19.0 0.1 collective-permute-done.4.refs_2_
  19.1 1.3 %collective-permute-done.5.refs_3_ = bf16[8,4224]{1,0:T(8,128)(2,1)S(1)} collective-permute-done((bf16[8,4224]{1,0:T(8,128)(2,1)S(1)}, bf16[8,4224]{1,0:T(8,128)(2,1)S(1)}, u32[]{:S(2)}, u32[]{:S(2)}) %collective-permute-start.5) | collective-permute-done | bytes 67616 | tf_op jit(solution)/shard_map/ppermute | solution.py:86
  20.3 1.4 %shard_map.145 = (bf16[8,1024]{1,0:T(8,128)(2,1)S(1)}, f32[128,128]{1,0:T(8,128)S(1)}) custom-call(bf16[8,4224]{1,0:T(8,128)(2,1)S(1)} %get-tuple-element.32.refs_0_, bf16[8,4224]{1,0:T(8,128)(2,1)S(1)} %collective-permute-done.3.refs_1_, bf16[8,4224]{1,0:T(8,128)(2,1)S(1)} %collective-permute-done.4.refs_2_, ...), custom_call_target="tpu_custom_call" | custom-call | tf_op jit(solution)/shard_map/pallas_call | solution.py:241
  21.7 0.7 %collective-permute-start.9 = (bf16[8,1024]{1,0:T(8,128)(2,1)S(1)}, bf16[8,1024]{1,0:T(8,128)(2,1)S(1)}, u32[]{:S(2)}, u32[]{:S(2)}) collective-permute-start(bf16[8,1024]{1,0:T(8,128)(2,1)S(1)} %get-tuple-element.39.refs_0_), channel_id=1, source_target_pairs={{0,4},{4,0},{8,12},{12,8},{1,5},{5,1},{9,13},{13,9},{2,6},{6,2},{1... | collective-permute-start | bytes 49160 | tf_op jit(solution)/shard_map/ppermute | solution.py:86
  22.4 3.5 %collective-permute-start.10 = (bf16[8,1024]{1,0:T(8,128)(2,1)S(1)}, bf16[8,1024]{1,0:T(8,128)(2,1)S(1)}, u32[]{:S(2)}, u32[]{:S(2)}) collective-permute-start(bf16[8,1024]{1,0:T(8,128)(2,1)S(1)} %get-tuple-element.39.refs_0_), channel_id=1, source_target_pairs={{0,8},{4,12},{8,0},{12,4},{1,9},{5,13},{9,1},{13,5},{2,10},{6,14},... | collective-permute-start | bytes 49160 | tf_op jit(solution)/shard_map/ppermute | solution.py:86
  25.9 0.2 collective-permute-start.11
  26.1 0.0 collective-permute-done.9.refs_1_
  26.1 1.5 %collective-permute-done.10.refs_2_ = bf16[8,1024]{1,0:T(8,128)(2,1)S(1)} collective-permute-done((bf16[8,1024]{1,0:T(8,128)(2,1)S(1)}, bf16[8,1024]{1,0:T(8,128)(2,1)S(1)}, u32[]{:S(2)}, u32[]{:S(2)}) %collective-permute-start.10) | collective-permute-done | bytes 16416 | tf_op jit(solution)/shard_map/ppermute | solution.py:86
  27.6 3.8 %collective-permute-done.11.refs_3_ = bf16[8,1024]{1,0:T(8,128)(2,1)S(1)} collective-permute-done((bf16[8,1024]{1,0:T(8,128)(2,1)S(1)}, bf16[8,1024]{1,0:T(8,128)(2,1)S(1)}, u32[]{:S(2)}, u32[]{:S(2)}) %collective-permute-start.11) | collective-permute-done | bytes 16416 | tf_op jit(solution)/shard_map/ppermute | solution.py:86
  31.4 1.2 %shard_map.146 = (bf16[8,4224]{1,0:T(8,128)(2,1)S(1)}, f32[8,1024]{1,0:T(8,128)S(1)}) custom-call(f32[8,1024]{1,0:T(8,128)S(1)} %get-tuple-element.31.base_ref, bf16[8,1024]{1,0:T(8,128)(2,1)S(1)} %get-tuple-element.39.refs_0_, bf16[8,1024]{1,0:T(8,128)(2,1)S(1)} %collective-permute-done.9.refs_1_, bf16[8,1024]{1,0:T(8,128)(2,1)S(1)} %collective-permute-done.10.refs_2_, ...), custom_call_target="tpu_custom_call" | custom-call | tf_op jit(solution)/shard_map/pallas_call | solution.py:241
  32.6 0.0 collective-permute-start.12
  32.6 1.4 %collective-permute-start.13 = (bf16[8,4224]{1,0:T(8,128)(2,1)S(1)}, bf16[8,4224]{1,0:T(8,128)(2,1)S(1)}, u32[]{:S(2)}, u32[]{:S(2)}) collective-permute-start(bf16[8,4224]{1,0:T(8,128)(2,1)S(1)} %get-tuple-element.40.refs_0_), channel_id=1, source_target_pairs={{0,2},{1,3},{2,0},{3,1},{4,6},{5,7},{6,4},{7,5},{8,10},{9,11},{10,... | collective-permute-start | bytes 202760 | tf_op jit(solution)/shard_map/ppermute | solution.py:86
  34.1 0.4 collective-permute-start.14
  34.5 1.0 %shard_map.147 = (f32[128,128]{1,0:T(8,128)S(1)}, f32[128,128]{1,0:T(8,128)S(1)}, bf16[16,256,128]{2,1,0:T(8,128)(2,1)S(1)}, bf16[16,128,128]{2,1,0:T(8,128)(2,1)S(1)}, f32[8,128,128]{2,1,0:T(8,128)S(1)}) custom-call(f32[2,64,128]{2,1,0:T(8,128)S(1)} %bitcast.18, f32[2,64,128]{2,1,0:T(8,128)S(1)} %bitcast.20, f32[2,128]{1,0:T(2,128)S(1)} %copy-done.8, ...), custom_call_target="tpu_custom_call" | custom-call | flops 4000000 | tf_op jit(solution)/shard_map/pallas_call | solution.py:241
  35.5 1.8 %collective-permute-done.13.refs_2_ = bf16[8,4224]{1,0:T(8,128)(2,1)S(1)} collective-permute-done((bf16[8,4224]{1,0:T(8,128)(2,1)S(1)}, bf16[8,4224]{1,0:T(8,128)(2,1)S(1)}, u32[]{:S(2)}, u32[]{:S(2)}) %collective-permute-start.13) | collective-permute-done | bytes 67616 | tf_op jit(solution)/shard_map/ppermute | solution.py:86
  37.3 1.1 %collective-permute-done.14.refs_3_ = bf16[8,4224]{1,0:T(8,128)(2,1)S(1)} collective-permute-done((bf16[8,4224]{1,0:T(8,128)(2,1)S(1)}, bf16[8,4224]{1,0:T(8,128)(2,1)S(1)}, u32[]{:S(2)}, u32[]{:S(2)}) %collective-permute-start.14) | collective-permute-done | bytes 67616 | tf_op jit(solution)/shard_map/ppermute | solution.py:86
  38.4 1.5 %shard_map.148 = (f32[4,1024]{1,0:T(4,128)S(1)}, bf16[4,1024]{1,0:T(4,128)(2,1)S(1)}, bf16[4,1024]{1,0:T(4,128)(2,1)S(1)}, bf16[4,1024]{1,0:T(4,128)(2,1)S(1)}, f32[128,128]{1,0:T(8,128)S(1)}) custom-call(bf16[8,4224]{1,0:T(8,128)(2,1)S(1)} %get-tuple-element.40.refs_0_, bf16[8,4224]{1,0:T(8,128)(2,1)S(1)} %collective-permute-done.12.refs_1_, ...), custom_call_target="tpu_custom_call" | custom-call | tf_op jit(solution)/shard_map/pallas_call | solution.py:241
  39.9 0.1 collective-permute-start.15
  40.0 0.7 %collective-permute-start.16 = (bf16[4,1024]{1,0:T(4,128)(2,1)S(1)}, bf16[4,1024]{1,0:T(4,128)(2,1)S(1)}, u32[]{:S(2)}, u32[]{:S(2)}) collective-permute-start(bf16[4,1024]{1,0:T(4,128)(2,1)S(1)} %get-tuple-element.50), channel_id=1, source_target_pairs={{0,8},{4,12},{8,0},{12,4},{1,9},{5,13},{9,1},{13,5},{2,10},{6,14},... | collective-permute-start | bytes 24584 | tf_op jit(solution)/shard_map/ppermute | solution.py:86
  40.7 3.6 %collective-permute-start.17 = (bf16[4,1024]{1,0:T(4,128)(2,1)S(1)}, bf16[4,1024]{1,0:T(4,128)(2,1)S(1)}, u32[]{:S(2)}, u32[]{:S(2)}) collective-permute-start(bf16[4,1024]{1,0:T(4,128)(2,1)S(1)} %get-tuple-element.51), channel_id=1, source_target_pairs={{0,12},{4,8},{8,4},{12,0},{1,13},{5,9},{9,5},{13,1},{2,14},{6,10},... | collective-permute-start | bytes 24584 | tf_op jit(solution)/shard_map/ppermute | solution.py:86
  44.4 0.7 %maximum_bitcast_fusion = f32[2,1,128,128]{3,2,1,0:T(8,128)} fusion(f32[1,128,128]{2,1,0:T(8,128)S(1)} %bitcast.22, f32[1,128,128]{2,1,0:T(8,128)S(1)} %bitcast.21), kind=kLoop, calls=%fused_computation | loop fusion | flops 32768 | bytes 262144
  45.0 1.1 %collective-permute-done.17.refs_2_ = bf16[4,1024]{1,0:T(4,128)(2,1)S(1)} collective-permute-done((bf16[4,1024]{1,0:T(4,128)(2,1)S(1)}, bf16[4,1024]{1,0:T(4,128)(2,1)S(1)}, u32[]{:S(2)}, u32[]{:S(2)}) %collective-permute-start.17) | collective-permute-done | bytes 8224 | tf_op jit(solution)/shard_map/ppermute | solution.py:86
  46.2 0.6 %shard_map.149 = bf16[1,4,1024]{2,1,0:T(4,128)(2,1)} custom-call(f32[4,1024]{1,0:T(4,128)S(1)} %get-tuple-element.48.own_ref, bf16[4,1024]{1,0:T(4,128)(2,1)S(1)} %collective-permute-done.15.refs_0_, bf16[4,1024]{1,0:T(4,128)(2,1)S(1)} %collective-permute-done.16.refs_1_, bf16[4,1024]{1,0:T(4,128)(2,1)S(1)} %collective-permute-done.17.refs_2_), custom_call_target="tpu_custom_call" | custom-call | tf_op jit(solution)/shard_map/pallas_call | solution.py:241
  (27 shorter events, 0.1 us)
Async XLA Ops:
  0.6 8.1 %collective-permute-start = (bf16[4,1024]{1,0:T(4,128)(2,1)}, bf16[4,1024]{1,0:T(4,128)(2,1)S(1)}, u32[]{:S(2)}, u32[]{:S(2)}) collective-permute-start(bf16[4,1024]{1,0:T(4,128)(2,1)} %bitcast.23), channel_id=1, source_target_pairs={{0,4},{4,0},{8,12},{12,8},{1,5},{5,1},{9,13},{13,9},{2,6},{6,2},{1... | collective-permute-start | bytes 24584 | tf_op jit(solution)/shard_map/ppermute | solution.py:86
  3.7 5.0 %collective-permute-start.1 = (bf16[4,1024]{1,0:T(4,128)(2,1)}, bf16[4,1024]{1,0:T(4,128)(2,1)S(1)}, u32[]{:S(2)}, u32[]{:S(2)}) collective-permute-start(bf16[4,1024]{1,0:T(4,128)(2,1)} %bitcast.24), channel_id=1, source_target_pairs={{0,8},{4,12},{8,0},{12,4},{1,9},{5,13},{9,1},{13,5},{2,10},{6,14},... | collective-permute-start | bytes 24584 | tf_op jit(solution)/shard_map/ppermute | solution.py:86
  6.3 5.7 %collective-permute-start.2 = (bf16[4,1024]{1,0:T(4,128)(2,1)}, bf16[4,1024]{1,0:T(4,128)(2,1)S(1)}, u32[]{:S(2)}, u32[]{:S(2)}) collective-permute-start(bf16[4,1024]{1,0:T(4,128)(2,1)} %bitcast.25), channel_id=1, source_target_pairs={{0,12},{4,8},{8,4},{12,0},{1,13},{5,9},{9,5},{13,1},{2,14},{6,10},... | collective-permute-start | bytes 24584 | tf_op jit(solution)/shard_map/ppermute | solution.py:86
  6.3 0.9 %copy-start.3 = (f32[2,1,128,128]{3,2,1,0:T(8,128)S(1)}, f32[2,1,128,128]{3,2,1,0:T(8,128)}, u32[]{:S(2)}) copy-start(f32[2,1,128,128]{3,2,1,0:T(8,128)} %param.25) | copy-start | bytes 393220
  7.2 4.8 %slice-start = ((s8[8388608]{0:T(1024)(128)(4,1)}), s8[4194304]{0:T(1024)(128)(4,1)S(1)}, s32[]{:S(2)}) async-start(s8[8388608]{0:T(1024)(128)(4,1)} %bitcast.10), calls=%async_computation | async-start | bytes 8388608
  7.2 4.8 %slice-start.2 = ((s8[8388608]{0:T(1024)(128)(4,1)}), s8[4194304]{0:T(1024)(128)(4,1)S(1)}, s32[]{:S(2)}) async-start(s8[8388608]{0:T(1024)(128)(4,1)} %bitcast.12), calls=%async_computation.2 | async-start | bytes 8388608
  7.3 4.7 %slice-start.1 = ((s8[8388608]{0:T(1024)(128)(4,1)}), s8[4194304]{0:T(1024)(128)(4,1)S(1)}, s32[]{:S(2)}) async-start(s8[8388608]{0:T(1024)(128)(4,1)} %bitcast.10), calls=%async_computation.1 | async-start | bytes 8388608
  7.3 5.9 %slice-start.3 = ((s8[8388608]{0:T(1024)(128)(4,1)}), s8[4194304]{0:T(1024)(128)(4,1)S(1)}, s32[]{:S(2)}) async-start(s8[8388608]{0:T(1024)(128)(4,1)} %bitcast.12), calls=%async_computation.3 | async-start | bytes 8388608
  7.3 9.4 %collective-permute-start.7 = (bf16[2,128,128]{2,1,0:T(8,128)(2,1)S(1)}, bf16[2,128,128]{2,1,0:T(8,128)(2,1)S(1)}, u32[]{:S(2)}, u32[]{:S(2)}) collective-permute-start(bf16[2,128,128]{2,1,0:T(8,128)(2,1)S(1)} %shard_map.143), channel_id=1, source_target_pairs={{0,3},{1,2},{2,1},{3,0},{4,7},{5,6},{6,5},{7,4},{8,11},{9,10},{10,... | collective-permute-start | bytes 196616 | tf_op jit(solution)/shard_map/ppermute | solution.py:86
  13.1 4.8 %copy-start.1 = (bf16[2,128,16,128]{3,2,1,0:T(8,128)(2,1)S(1)}, bf16[2,128,16,128]{3,2,1,0:T(8,128)(2,1)}, u32[]{:S(2)}) copy-start(bf16[2,128,16,128]{3,2,1,0:T(8,128)(2,1)} %map_ref.3) | copy-start | bytes 3145732
  13.1 4.8 %copy-start.2 = (bf16[2,128,16,128]{3,2,1,0:T(8,128)(2,1)S(1)}, bf16[2,128,16,128]{3,2,1,0:T(8,128)(2,1)}, u32[]{:S(2)}) copy-start(bf16[2,128,16,128]{3,2,1,0:T(8,128)(2,1)} %readout_ref.3) | copy-start | bytes 3145732
  13.1 4.8 %copy-start.4 = (f32[2,1,128,128]{3,2,1,0:T(8,128)S(1)}, f32[2,1,128,128]{3,2,1,0:T(8,128)}, u32[]{:S(2)}) copy-start(f32[2,1,128,128]{3,2,1,0:T(8,128)} %param.25) | copy-start | bytes 393220
  13.1 4.8 %copy-start.5 = (f32[2,128,64]{1,2,0:T(8,128)S(1)}, f32[2,128,64]{1,2,0:T(8,128)}, u32[]{:S(2)}) copy-start(f32[2,128,64]{1,2,0:T(8,128)} %param.18) | copy-start | bytes 196612
  13.2 4.8 %copy-start.6 = (f32[2,128,64]{1,2,0:T(8,128)S(1)}, f32[2,128,64]{1,2,0:T(8,128)}, u32[]{:S(2)}) copy-start(f32[2,128,64]{1,2,0:T(8,128)} %param.19) | copy-start | bytes 196612
  13.2 4.8 %copy-start.8 = (f32[2,128]{1,0:T(2,128)S(1)}, f32[2,128]{1,0:T(2,128)}, u32[]{:S(2)}) copy-start(f32[2,128]{1,0:T(2,128)} %log_step_ref.3) | copy-start | bytes 3076
  13.2 7.2 %copy-start = (bf16[2,2048,1024]{2,1,0:T(8,128)(2,1)S(1)}, bf16[2,2048,1024]{2,1,0:T(8,128)(2,1)}, u32[]{:S(2)}) copy-start(bf16[2,2048,1024]{2,1,0:T(8,128)(2,1)} %refs_14_.1) | copy-start | bytes 25165828
  13.2 7.1 %copy-start.7 = (bf16[2,2048]{1,0:T(2,128)(2,1)S(1)}, bf16[2,2048]{1,0:T(2,128)(2,1)}, u32[]{:S(2)}) copy-start(bf16[2,2048]{1,0:T(2,128)(2,1)} %refs_10_.3) | copy-start | bytes 24580
  14.5 4.5 %collective-permute-start.3 = (bf16[8,4224]{1,0:T(8,128)(2,1)S(1)}, bf16[8,4224]{1,0:T(8,128)(2,1)S(1)}, u32[]{:S(2)}, u32[]{:S(2)}) collective-permute-start(bf16[8,4224]{1,0:T(8,128)(2,1)S(1)} %get-tuple-element.32.refs_0_), channel_id=1, source_target_pairs={{0,1},{1,0},{2,3},{3,2},{4,5},{5,4},{6,7},{7,6},{8,9},{9,8},{10,11... | collective-permute-start | bytes 202760 | tf_op jit(solution)/shard_map/ppermute | solution.py:86
  14.5 4.6 %collective-permute-start.4 = (bf16[8,4224]{1,0:T(8,128)(2,1)S(1)}, bf16[8,4224]{1,0:T(8,128)(2,1)S(1)}, u32[]{:S(2)}, u32[]{:S(2)}) collective-permute-start(bf16[8,4224]{1,0:T(8,128)(2,1)S(1)} %get-tuple-element.32.refs_0_), channel_id=1, source_target_pairs={{0,2},{1,3},{2,0},{3,1},{4,6},{5,7},{6,4},{7,5},{8,10},{9,11},{10,... | collective-permute-start | bytes 202760 | tf_op jit(solution)/shard_map/ppermute | solution.py:86
  16.3 4.1 %collective-permute-start.5 = (bf16[8,4224]{1,0:T(8,128)(2,1)S(1)}, bf16[8,4224]{1,0:T(8,128)(2,1)S(1)}, u32[]{:S(2)}, u32[]{:S(2)}) collective-permute-start(bf16[8,4224]{1,0:T(8,128)(2,1)S(1)} %get-tuple-element.32.refs_0_), channel_id=1, source_target_pairs={{0,3},{1,2},{2,1},{3,0},{4,7},{5,6},{6,5},{7,4},{8,11},{9,10},{10,... | collective-permute-start | bytes 202760 | tf_op jit(solution)/shard_map/ppermute | solution.py:86
  16.4 1.3 %collective-permute-start.6 = (bf16[2,128,128]{2,1,0:T(8,128)(2,1)S(1)}, bf16[2,128,128]{2,1,0:T(8,128)(2,1)S(1)}, u32[]{:S(2)}, u32[]{:S(2)}) collective-permute-start(bf16[2,128,128]{2,1,0:T(8,128)(2,1)S(1)} %shard_map.143), channel_id=1, source_target_pairs={{0,1},{1,0},{2,3},{3,2},{4,5},{5,4},{6,7},{7,6},{8,9},{9,8},{10,11... | collective-permute-start | bytes 196616 | tf_op jit(solution)/shard_map/ppermute | solution.py:86
  16.7 1.3 %collective-permute-start.8 = (bf16[2,128,128]{2,1,0:T(8,128)(2,1)S(1)}, bf16[2,128,128]{2,1,0:T(8,128)(2,1)S(1)}, u32[]{:S(2)}, u32[]{:S(2)}) collective-permute-start(bf16[2,128,128]{2,1,0:T(8,128)(2,1)S(1)} %collective-permute-done.7.refs_3_), channel_id=1, source_target_pairs={{0,1},{1,0},{2,3},{3,2},{4,5},{5,4},{6,7},{7,6},{8,9},{9,8},{10,11... | collective-permute-start | bytes 196616 | tf_op jit(solution)/shard_map/ppermute | solution.py:86
  21.7 4.4 %collective-permute-start.9 = (bf16[8,1024]{1,0:T(8,128)(2,1)S(1)}, bf16[8,1024]{1,0:T(8,128)(2,1)S(1)}, u32[]{:S(2)}, u32[]{:S(2)}) collective-permute-start(bf16[8,1024]{1,0:T(8,128)(2,1)S(1)} %get-tuple-element.39.refs_0_), channel_id=1, source_target_pairs={{0,4},{4,0},{8,12},{12,8},{1,5},{5,1},{9,13},{13,9},{2,6},{6,2},{1... | collective-permute-start | bytes 49160 | tf_op jit(solution)/shard_map/ppermute | solution.py:86
  22.4 5.2 %collective-permute-start.10 = (bf16[8,1024]{1,0:T(8,128)(2,1)S(1)}, bf16[8,1024]{1,0:T(8,128)(2,1)S(1)}, u32[]{:S(2)}, u32[]{:S(2)}) collective-permute-start(bf16[8,1024]{1,0:T(8,128)(2,1)S(1)} %get-tuple-element.39.refs_0_), channel_id=1, source_target_pairs={{0,8},{4,12},{8,0},{12,4},{1,9},{5,13},{9,1},{13,5},{2,10},{6,14},... | collective-permute-start | bytes 49160 | tf_op jit(solution)/shard_map/ppermute | solution.py:86
  25.9 5.5 %collective-permute-start.11 = (bf16[8,1024]{1,0:T(8,128)(2,1)S(1)}, bf16[8,1024]{1,0:T(8,128)(2,1)S(1)}, u32[]{:S(2)}, u32[]{:S(2)}) collective-permute-start(bf16[8,1024]{1,0:T(8,128)(2,1)S(1)} %get-tuple-element.39.refs_0_), channel_id=1, source_target_pairs={{0,12},{4,8},{8,4},{12,0},{1,13},{5,9},{9,5},{13,1},{2,14},{6,10},... | collective-permute-start | bytes 49160 | tf_op jit(solution)/shard_map/ppermute | solution.py:86
  32.6 2.9 %collective-permute-start.12 = (bf16[8,4224]{1,0:T(8,128)(2,1)S(1)}, bf16[8,4224]{1,0:T(8,128)(2,1)S(1)}, u32[]{:S(2)}, u32[]{:S(2)}) collective-permute-start(bf16[8,4224]{1,0:T(8,128)(2,1)S(1)} %get-tuple-element.40.refs_0_), channel_id=1, source_target_pairs={{0,1},{1,0},{2,3},{3,2},{4,5},{5,4},{6,7},{7,6},{8,9},{9,8},{10,11... | collective-permute-start | bytes 202760 | tf_op jit(solution)/shard_map/ppermute | solution.py:86
  32.6 4.7 %collective-permute-start.13 = (bf16[8,4224]{1,0:T(8,128)(2,1)S(1)}, bf16[8,4224]{1,0:T(8,128)(2,1)S(1)}, u32[]{:S(2)}, u32[]{:S(2)}) collective-permute-start(bf16[8,4224]{1,0:T(8,128)(2,1)S(1)} %get-tuple-element.40.refs_0_), channel_id=1, source_target_pairs={{0,2},{1,3},{2,0},{3,1},{4,6},{5,7},{6,4},{7,5},{8,10},{9,11},{10,... | collective-permute-start | bytes 202760 | tf_op jit(solution)/shard_map/ppermute | solution.py:86
  34.1 4.3 %collective-permute-start.14 = (bf16[8,4224]{1,0:T(8,128)(2,1)S(1)}, bf16[8,4224]{1,0:T(8,128)(2,1)S(1)}, u32[]{:S(2)}, u32[]{:S(2)}) collective-permute-start(bf16[8,4224]{1,0:T(8,128)(2,1)S(1)} %get-tuple-element.40.refs_0_), channel_id=1, source_target_pairs={{0,3},{1,2},{2,1},{3,0},{4,7},{5,6},{6,5},{7,4},{8,11},{9,10},{10,... | collective-permute-start | bytes 202760 | tf_op jit(solution)/shard_map/ppermute | solution.py:86
  39.9 5.1 %collective-permute-start.15 = (bf16[4,1024]{1,0:T(4,128)(2,1)S(1)}, bf16[4,1024]{1,0:T(4,128)(2,1)S(1)}, u32[]{:S(2)}, u32[]{:S(2)}) collective-permute-start(bf16[4,1024]{1,0:T(4,128)(2,1)S(1)} %get-tuple-element.49), channel_id=1, source_target_pairs={{0,4},{4,0},{8,12},{12,8},{1,5},{5,1},{9,13},{13,9},{2,6},{6,2},{1... | collective-permute-start | bytes 24584 | tf_op jit(solution)/shard_map/ppermute | solution.py:86
  40.0 5.0 %collective-permute-start.16 = (bf16[4,1024]{1,0:T(4,128)(2,1)S(1)}, bf16[4,1024]{1,0:T(4,128)(2,1)S(1)}, u32[]{:S(2)}, u32[]{:S(2)}) collective-permute-start(bf16[4,1024]{1,0:T(4,128)(2,1)S(1)} %get-tuple-element.50), channel_id=1, source_target_pairs={{0,8},{4,12},{8,0},{12,4},{1,9},{5,13},{9,1},{13,5},{2,10},{6,14},... | collective-permute-start | bytes 24584 | tf_op jit(solution)/shard_map/ppermute | solution.py:86
  40.7 5.4 %collective-permute-start.17 = (bf16[4,1024]{1,0:T(4,128)(2,1)S(1)}, bf16[4,1024]{1,0:T(4,128)(2,1)S(1)}, u32[]{:S(2)}, u32[]{:S(2)}) collective-permute-start(bf16[4,1024]{1,0:T(4,128)(2,1)S(1)} %get-tuple-element.51), channel_id=1, source_target_pairs={{0,12},{4,8},{8,4},{12,0},{1,13},{5,9},{9,5},{13,1},{2,14},{6,10},... | collective-permute-start | bytes 24584 | tf_op jit(solution)/shard_map/ppermute | solution.py:86

commit v7 on v6

--- a/solution.py
+++ b/solution.py
@@ -540,24 +540,29 @@
     ).astype(jnp.bfloat16)
 
 
+def place(spread_ref, rows):
+    chosen = spread_ref[:, : 2 * rows.shape[0]]
+    rows = jnp.concatenate([rows, jnp.zeros_like(rows)], axis=0).astype(jnp.bfloat16)
+    return jnp.dot(chosen, rows, preferred_element_type=jnp.float32)
+
+
+def base_kernel(spread_ref, rows_ref, own_ref, base_ref):
+    steps, count = own_ref.shape[0], rows_ref.shape[0]
+    base = place(spread_ref, rows_ref[...])[:steps]
+    chosen = spread_ref[:steps, : 2 * count].astype(jnp.float32)
+    live = jnp.sum(chosen, axis=1, keepdims=True)
+    base_ref[...] = base + jnp.where(live > 0.5, 0.0, own_ref[...].astype(jnp.float32))
+
+
 def last_state_kernel(size, layer, features, *refs):
     ahead = len(refs) - (size + 2)
-    spread_ref, base_ref, own_ref, weight_ref = refs[ahead - 4 : ahead]
+    spread_ref, base_ref, weight_ref = refs[ahead - 3 : ahead]
     out_refs, (next_ref, branch_ref) = refs[ahead:-2], refs[-2:]
-    advance(size, layer, features, refs[: ahead - 4], next_ref, branch_ref)
+    advance(size, layer, features, refs[: ahead - 3], next_ref, branch_ref)
     part = jnp.dot(branch_ref[...], weight_ref[layer], preferred_element_type=jnp.float32)
-    steps = own_ref.shape[0]
-    spread = spread_ref[:, : 2 * part.shape[0]]
-
-    def place(chosen, rows):
-        rows = jnp.concatenate([rows, jnp.zeros_like(rows)], axis=0).astype(jnp.bfloat16)
-        return jnp.dot(chosen, rows, preferred_element_type=jnp.float32)
-
-    placed = place(spread, part)
-    base = place(spread, base_ref[...])[:steps]
-    live = jnp.sum(spread[:steps].astype(jnp.float32), axis=1, keepdims=True)
-    base = base + jnp.where(live > 0.5, 0.0, own_ref[...].astype(jnp.float32))
-    out_refs[0][...] = base + placed[:steps]
+    steps = base_ref.shape[0]
+    placed = place(spread_ref, part)
+    out_refs[0][...] = base_ref[...] + placed[:steps]
     for k in range(1, size):
         out_refs[k][...] = placed[k * steps : (k + 1) * steps].astype(jnp.bfloat16)
 
@@ -629,6 +634,10 @@
         fixed = prepare(layer, count, *raw, marks, [carried[k] for k in range(size)])
         operands = [*arrived, marks, *fixed, skip_weight]
         last = layer == LAYERS - 1
+        if last:
+            (base,) = vmem_call(
+                base_kernel, [((steps, features), f32)], spread, rows, own, cost=SMALL_COST
+            )
         outs = [((groups, LANES), f32)]
         scratch = [pltpu.VMEM((count, inner), bf16)]
         if not last:
@@ -643,7 +652,7 @@
         *parts, next_state = vmem_call(
             functools.partial(last_state_kernel, size, layer, D),
             [((steps, features), f32)] + [((steps, features), bf16)] * (size - 1) + outs,
-            *operands, spread, rows, own, out_weight, scratch=scratch,
+            *operands, spread, base, out_weight, scratch=scratch,
         )
         states.append(next_state)
         arrived = swaps(parts, "tp", size)

time: 47 us -> 46.9 us (level)
    pallas_call x10 -> x11, Pallas kernels: 8.9 us -> 9 us  [vmem_call(): pl.pallas_call(kernel, out_shape=outs, in_specs=in_specs, out_specs=[VMEM...]
where the time goes in v7:
time: 46.9 us; the launch traced here: 46.7 us
  starting transfers between devices  19.2 us (41%)
  waiting for transfers between devices  14.9 us (32%)
  Pallas kernels  9 us (19%)
  local copies, waits for them, and re-layouts  2.1 us (4%)
  between operations  0.8 us (2%)
  other arithmetic  0.66 us (1%)
    ppermute x18, starting transfers between devices, swap(): return lax.ppermute(value, axis, [(i, i ^ distance) for i in range(size)])  19.2 us
    ppermute x18, waiting for transfers between devices, swap(): return lax.ppermute(value, axis, [(i, i ^ distance) for i in range(size)])  14.9 us
    pallas_call x11, Pallas kernels, vmem_call(): pl.pallas_call(kernel, out_shape=outs, in_specs=in_specs, out_specs=[VMEM...  9 us
    unnamed x26, local copies, waits for them, and re-layouts  2.1 us
  transfers between devices with their start and end apart: 18, of which 10 were waited for; matrix products, arithmetic and copies ran while one was open for 1% of the time, Pallas kernels for 9%

profile of v7, /device:TPU:0, one launch (start us, length us, event | category | flops | bytes accessed | tf_op | source)
XLA Modules:
  0.0 46.7 jit_solution(7329120061337093822)
XLA Ops:
  0.6 3.1 %collective-permute-start = (bf16[4,1024]{1,0:T(4,128)(2,1)}, bf16[4,1024]{1,0:T(4,128)(2,1)S(1)}, u32[]{:S(2)}, u32[]{:S(2)}) collective-permute-start(bf16[4,1024]{1,0:T(4,128)(2,1)} %bitcast.23), channel_id=1, source_target_pairs={{0,4},{4,0},{8,12},{12,8},{1,5},{5,1},{9,13},{13,9},{2,6},{6,2},{1... | collective-permute-start | bytes 24584 | tf_op jit(solution)/shard_map/ppermute | solution.py:86
  3.7 2.6 %collective-permute-start.1 = (bf16[4,1024]{1,0:T(4,128)(2,1)}, bf16[4,1024]{1,0:T(4,128)(2,1)S(1)}, u32[]{:S(2)}, u32[]{:S(2)}) collective-permute-start(bf16[4,1024]{1,0:T(4,128)(2,1)} %bitcast.24), channel_id=1, source_target_pairs={{0,8},{4,12},{8,0},{12,4},{1,9},{5,13},{9,1},{13,5},{2,10},{6,14},... | collective-permute-start | bytes 24584 | tf_op jit(solution)/shard_map/ppermute | solution.py:86
  6.3 0.9 %copy-done.3 = f32[2,1,128,128]{3,2,1,0:T(8,128)S(1)} copy-done((f32[2,1,128,128]{3,2,1,0:T(8,128)S(1)}, f32[2,1,128,128]{3,2,1,0:T(8,128)}, u32[]{:S(2)}) %copy-start.3) | copy-done | bytes 131096
  7.3 0.0 slice-start.1
  7.3 0.0 slice-start.3
  7.3 0.5 collective-permute-start.7
  7.8 1.0 %shard_map.141 = (bf16[4,1024]{1,0:T(4,128)(2,1)S(1)}, f32[2,1024]{1,0:T(2,128)S(1)}, bf16[8,128]{1,0:T(8,128)(2,1)S(1)}, bf16[16,128]{1,0:T(8,128)(2,1)S(1)}, f32[48,128]{1,0:T(8,128)S(1)}) custom-call(f32[8,128]{1,0:T(8,128)S(1)} %shard_map.140.primer_ref, s32[4]{0:T(128)} %lengths_hbm.1, bf16[4,1024]{1,0:T(4,128)(2,1)} %bitcast.26, f32[2,1024]{1,0:T(2,128)} %refs_1_.1), custom_call_target="tpu_custom_call" | custom-call | flops 4000000 | tf_op jit(solution)/shard_map/pallas_call | solution.py:241
  8.7 0.0 collective-permute-done.refs_1_
  8.8 3.2 %collective-permute-done.2.refs_3_ = bf16[4,1024]{1,0:T(4,128)(2,1)S(1)} collective-permute-done((bf16[4,1024]{1,0:T(4,128)(2,1)}, bf16[4,1024]{1,0:T(4,128)(2,1)S(1)}, u32[]{:S(2)}, u32[]{:S(2)}) %collective-permute-start.2) | collective-permute-done | bytes 8224 | tf_op jit(solution)/shard_map/ppermute | solution.py:86
  12.0 1.1 %slice-done.3 = s8[4194304]{0:T(1024)(128)(4,1)S(1)} async-done(((s8[8388608]{0:T(1024)(128)(4,1)}), s8[4194304]{0:T(1024)(128)(4,1)S(1)}, s32[]{:S(2)}) %slice-start.3) | async-done | bytes 4194328
  13.1 0.0 copy-start.5
  13.2 0.0 copy-start.6
  13.2 0.0 copy-start.8
  13.2 0.0 copy-start
  13.2 0.0 copy-start.7
  13.2 1.3 %shard_map.142 = (bf16[8,4224]{1,0:T(8,128)(2,1)S(1)}, f32[8,1024]{1,0:T(8,128)S(1)}) custom-call(bf16[8,128]{1,0:T(8,128)(2,1)S(1)} %get-tuple-element.28.pick_ref, bf16[4,1024]{1,0:T(4,128)(2,1)S(1)} %get-tuple-element.29.refs_0_.own_ref, bf16[4,1024]{1,0:T(4,128)(2,1)S(1)} %collective-permute-done.refs_1_, ...), custom_call_target="tpu_custom_call" | custom-call | tf_op jit(solution)/shard_map/pallas_call | solution.py:241
  14.5 0.0 collective-permute-start.3
  14.5 1.8 %collective-permute-start.4 = (bf16[8,4224]{1,0:T(8,128)(2,1)S(1)}, bf16[8,4224]{1,0:T(8,128)(2,1)S(1)}, u32[]{:S(2)}, u32[]{:S(2)}) collective-permute-start(bf16[8,4224]{1,0:T(8,128)(2,1)S(1)} %get-tuple-element.32.refs_0_), channel_id=1, source_target_pairs={{0,2},{1,3},{2,0},{3,1},{4,6},{5,7},{6,4},{7,5},{8,10},{9,11},{10,... | collective-permute-start | bytes 202760 | tf_op jit(solution)/shard_map/ppermute | solution.py:86
  16.3 0.1 collective-permute-start.5
  16.4 0.3 collective-permute-start.6
  16.7 0.0 collective-permute-done.7.refs_3_
  16.7 0.2 collective-permute-start.8
  16.9 0.7 %collective-permute-done.6.refs_1_ = bf16[2,128,128]{2,1,0:T(8,128)(2,1)S(1)} collective-permute-done((bf16[2,128,128]{2,1,0:T(8,128)(2,1)S(1)}, bf16[2,128,128]{2,1,0:T(8,128)(2,1)S(1)}, u32[]{:S(2)}, u32[]{:S(2)}) %collective-permute-start.6) | collective-permute-done | bytes 65568 | tf_op jit(solution)/shard_map/ppermute | solution.py:86
  17.6 0.3 collective-permute-done.8.refs_2_
  18.0 1.0 %shard_map.144 = (f32[128,128]{1,0:T(8,128)S(1)}, f32[128,128]{1,0:T(8,128)S(1)}, bf16[16,256,128]{2,1,0:T(8,128)(2,1)S(1)}, bf16[16,128,128]{2,1,0:T(8,128)(2,1)S(1)}, f32[8,128,128]{2,1,0:T(8,128)S(1)}) custom-call(f32[2,64,128]{2,1,0:T(8,128)S(1)} %bitcast.17, f32[2,64,128]{2,1,0:T(8,128)S(1)} %bitcast.19, f32[2,128]{1,0:T(2,128)S(1)} %copy-done.8, ...), custom_call_target="tpu_custom_call" | custom-call | flops 4000000 | tf_op jit(solution)/shard_map/pallas_call | solution.py:241
  19.0 0.0 collective-permute-done.3.refs_1_
  19.0 0.1 collective-permute-done.4.refs_2_
  19.1 1.3 %collective-permute-done.5.refs_3_ = bf16[8,4224]{1,0:T(8,128)(2,1)S(1)} collective-permute-done((bf16[8,4224]{1,0:T(8,128)(2,1)S(1)}, bf16[8,4224]{1,0:T(8,128)(2,1)S(1)}, u32[]{:S(2)}, u32[]{:S(2)}) %collective-permute-start.5) | collective-permute-done | bytes 67616 | tf_op jit(solution)/shard_map/ppermute | solution.py:86
  20.3 1.4 %shard_map.145 = (bf16[8,1024]{1,0:T(8,128)(2,1)S(1)}, f32[128,128]{1,0:T(8,128)S(1)}) custom-call(bf16[8,4224]{1,0:T(8,128)(2,1)S(1)} %get-tuple-element.32.refs_0_, bf16[8,4224]{1,0:T(8,128)(2,1)S(1)} %collective-permute-done.3.refs_1_, bf16[8,4224]{1,0:T(8,128)(2,1)S(1)} %collective-permute-done.4.refs_2_, ...), custom_call_target="tpu_custom_call" | custom-call | tf_op jit(solution)/shard_map/pallas_call | solution.py:241
  21.7 0.7 %collective-permute-start.9 = (bf16[8,1024]{1,0:T(8,128)(2,1)S(1)}, bf16[8,1024]{1,0:T(8,128)(2,1)S(1)}, u32[]{:S(2)}, u32[]{:S(2)}) collective-permute-start(bf16[8,1024]{1,0:T(8,128)(2,1)S(1)} %get-tuple-element.39.refs_0_), channel_id=1, source_target_pairs={{0,4},{4,0},{8,12},{12,8},{1,5},{5,1},{9,13},{13,9},{2,6},{6,2},{1... | collective-permute-start | bytes 49160 | tf_op jit(solution)/shard_map/ppermute | solution.py:86
  22.4 3.5 %collective-permute-start.10 = (bf16[8,1024]{1,0:T(8,128)(2,1)S(1)}, bf16[8,1024]{1,0:T(8,128)(2,1)S(1)}, u32[]{:S(2)}, u32[]{:S(2)}) collective-permute-start(bf16[8,1024]{1,0:T(8,128)(2,1)S(1)} %get-tuple-element.39.refs_0_), channel_id=1, source_target_pairs={{0,8},{4,12},{8,0},{12,4},{1,9},{5,13},{9,1},{13,5},{2,10},{6,14},... | collective-permute-start | bytes 49160 | tf_op jit(solution)/shard_map/ppermute | solution.py:86
  25.9 0.2 collective-permute-start.11
  26.1 0.0 collective-permute-done.9.refs_1_
  26.1 1.5 %collective-permute-done.10.refs_2_ = bf16[8,1024]{1,0:T(8,128)(2,1)S(1)} collective-permute-done((bf16[8,1024]{1,0:T(8,128)(2,1)S(1)}, bf16[8,1024]{1,0:T(8,128)(2,1)S(1)}, u32[]{:S(2)}, u32[]{:S(2)}) %collective-permute-start.10) | collective-permute-done | bytes 16416 | tf_op jit(solution)/shard_map/ppermute | solution.py:86
  27.6 3.8 %collective-permute-done.11.refs_3_ = bf16[8,1024]{1,0:T(8,128)(2,1)S(1)} collective-permute-done((bf16[8,1024]{1,0:T(8,128)(2,1)S(1)}, bf16[8,1024]{1,0:T(8,128)(2,1)S(1)}, u32[]{:S(2)}, u32[]{:S(2)}) %collective-permute-start.11) | collective-permute-done | bytes 16416 | tf_op jit(solution)/shard_map/ppermute | solution.py:86
  31.4 1.2 %shard_map.146 = (bf16[8,4224]{1,0:T(8,128)(2,1)S(1)}, f32[8,1024]{1,0:T(8,128)S(1)}) custom-call(f32[8,1024]{1,0:T(8,128)S(1)} %get-tuple-element.31.base_ref, bf16[8,1024]{1,0:T(8,128)(2,1)S(1)} %get-tuple-element.39.refs_0_, bf16[8,1024]{1,0:T(8,128)(2,1)S(1)} %collective-permute-done.9.refs_1_, bf16[8,1024]{1,0:T(8,128)(2,1)S(1)} %collective-permute-done.10.refs_2_, ...), custom_call_target="tpu_custom_call" | custom-call | tf_op jit(solution)/shard_map/pallas_call | solution.py:241
  32.6 1.4 %collective-permute-start.13 = (bf16[8,4224]{1,0:T(8,128)(2,1)S(1)}, bf16[8,4224]{1,0:T(8,128)(2,1)S(1)}, u32[]{:S(2)}, u32[]{:S(2)}) collective-permute-start(bf16[8,4224]{1,0:T(8,128)(2,1)S(1)} %get-tuple-element.40.refs_0_), channel_id=1, source_target_pairs={{0,2},{1,3},{2,0},{3,1},{4,6},{5,7},{6,4},{7,5},{8,10},{9,11},{10,... | collective-permute-start | bytes 202760 | tf_op jit(solution)/shard_map/ppermute | solution.py:86
  34.1 0.4 collective-permute-start.14
  34.5 1.0 %shard_map.147 = (f32[128,128]{1,0:T(8,128)S(1)}, f32[128,128]{1,0:T(8,128)S(1)}, bf16[16,256,128]{2,1,0:T(8,128)(2,1)S(1)}, bf16[16,128,128]{2,1,0:T(8,128)(2,1)S(1)}, f32[8,128,128]{2,1,0:T(8,128)S(1)}) custom-call(f32[2,64,128]{2,1,0:T(8,128)S(1)} %bitcast.18, f32[2,64,128]{2,1,0:T(8,128)S(1)} %bitcast.20, f32[2,128]{1,0:T(2,128)S(1)} %copy-done.8, ...), custom_call_target="tpu_custom_call" | custom-call | flops 4000000 | tf_op jit(solution)/shard_map/pallas_call | solution.py:241
  35.5 0.1 shard_map.148.refs_12_
  35.6 1.7 %collective-permute-done.13.refs_2_ = bf16[8,4224]{1,0:T(8,128)(2,1)S(1)} collective-permute-done((bf16[8,4224]{1,0:T(8,128)(2,1)S(1)}, bf16[8,4224]{1,0:T(8,128)(2,1)S(1)}, u32[]{:S(2)}, u32[]{:S(2)}) %collective-permute-start.13) | collective-permute-done | bytes 67616 | tf_op jit(solution)/shard_map/ppermute | solution.py:86
  37.3 1.1 %collective-permute-done.14.refs_3_ = bf16[8,4224]{1,0:T(8,128)(2,1)S(1)} collective-permute-done((bf16[8,4224]{1,0:T(8,128)(2,1)S(1)}, bf16[8,4224]{1,0:T(8,128)(2,1)S(1)}, u32[]{:S(2)}, u32[]{:S(2)}) %collective-permute-start.14) | collective-permute-done | bytes 67616 | tf_op jit(solution)/shard_map/ppermute | solution.py:86
  38.4 1.5 %shard_map.149 = (f32[4,1024]{1,0:T(4,128)S(1)}, bf16[4,1024]{1,0:T(4,128)(2,1)S(1)}, bf16[4,1024]{1,0:T(4,128)(2,1)S(1)}, bf16[4,1024]{1,0:T(4,128)(2,1)S(1)}, f32[128,128]{1,0:T(8,128)S(1)}) custom-call(bf16[8,4224]{1,0:T(8,128)(2,1)S(1)} %get-tuple-element.40.refs_0_, bf16[8,4224]{1,0:T(8,128)(2,1)S(1)} %collective-permute-done.12.refs_1_, ...), custom_call_target="tpu_custom_call" | custom-call | tf_op jit(solution)/shard_map/pallas_call | solution.py:241
  39.9 0.8 %collective-permute-start.16 = (bf16[4,1024]{1,0:T(4,128)(2,1)S(1)}, bf16[4,1024]{1,0:T(4,128)(2,1)S(1)}, u32[]{:S(2)}, u32[]{:S(2)}) collective-permute-start(bf16[4,1024]{1,0:T(4,128)(2,1)S(1)} %get-tuple-element.50), channel_id=1, source_target_pairs={{0,8},{4,12},{8,0},{12,4},{1,9},{5,13},{9,1},{13,5},{2,10},{6,14},... | collective-permute-start | bytes 24584 | tf_op jit(solution)/shard_map/ppermute | solution.py:86
  40.6 3.6 %collective-permute-start.17 = (bf16[4,1024]{1,0:T(4,128)(2,1)S(1)}, bf16[4,1024]{1,0:T(4,128)(2,1)S(1)}, u32[]{:S(2)}, u32[]{:S(2)}) collective-permute-start(bf16[4,1024]{1,0:T(4,128)(2,1)S(1)} %get-tuple-element.51), channel_id=1, source_target_pairs={{0,12},{4,8},{8,4},{12,0},{1,13},{5,9},{9,5},{13,1},{2,14},{6,10},... | collective-permute-start | bytes 24584 | tf_op jit(solution)/shard_map/ppermute | solution.py:86
  44.3 0.7 %maximum_bitcast_fusion = f32[2,1,128,128]{3,2,1,0:T(8,128)} fusion(f32[1,128,128]{2,1,0:T(8,128)S(1)} %bitcast.22, f32[1,128,128]{2,1,0:T(8,128)S(1)} %bitcast.21), kind=kLoop, calls=%fused_computation | loop fusion | flops 32768 | bytes 262144
  45.0 1.1 %collective-permute-done.17.refs_2_ = bf16[4,1024]{1,0:T(4,128)(2,1)S(1)} collective-permute-done((bf16[4,1024]{1,0:T(4,128)(2,1)S(1)}, bf16[4,1024]{1,0:T(4,128)(2,1)S(1)}, u32[]{:S(2)}, u32[]{:S(2)}) %collective-permute-start.17) | collective-permute-done | bytes 8224 | tf_op jit(solution)/shard_map/ppermute | solution.py:86
  46.1 0.6 %shard_map.150 = bf16[1,4,1024]{2,1,0:T(4,128)(2,1)} custom-call(f32[4,1024]{1,0:T(4,128)S(1)} %get-tuple-element.48.own_ref, bf16[4,1024]{1,0:T(4,128)(2,1)S(1)} %collective-permute-done.15.refs_0_, bf16[4,1024]{1,0:T(4,128)(2,1)S(1)} %collective-permute-done.16.refs_1_, bf16[4,1024]{1,0:T(4,128)(2,1)S(1)} %collective-permute-done.17.refs_2_), custom_call_target="tpu_custom_call" | custom-call | tf_op jit(solution)/shard_map/pallas_call | solution.py:241
  (28 shorter events, 0.1 us)
Async XLA Ops:
  0.6 8.1 %collective-permute-start = (bf16[4,1024]{1,0:T(4,128)(2,1)}, bf16[4,1024]{1,0:T(4,128)(2,1)S(1)}, u32[]{:S(2)}, u32[]{:S(2)}) collective-permute-start(bf16[4,1024]{1,0:T(4,128)(2,1)} %bitcast.23), channel_id=1, source_target_pairs={{0,4},{4,0},{8,12},{12,8},{1,5},{5,1},{9,13},{13,9},{2,6},{6,2},{1... | collective-permute-start | bytes 24584 | tf_op jit(solution)/shard_map/ppermute | solution.py:86
  3.7 5.0 %collective-permute-start.1 = (bf16[4,1024]{1,0:T(4,128)(2,1)}, bf16[4,1024]{1,0:T(4,128)(2,1)S(1)}, u32[]{:S(2)}, u32[]{:S(2)}) collective-permute-start(bf16[4,1024]{1,0:T(4,128)(2,1)} %bitcast.24), channel_id=1, source_target_pairs={{0,8},{4,12},{8,0},{12,4},{1,9},{5,13},{9,1},{13,5},{2,10},{6,14},... | collective-permute-start | bytes 24584 | tf_op jit(solution)/shard_map/ppermute | solution.py:86
  6.3 5.7 %collective-permute-start.2 = (bf16[4,1024]{1,0:T(4,128)(2,1)}, bf16[4,1024]{1,0:T(4,128)(2,1)S(1)}, u32[]{:S(2)}, u32[]{:S(2)}) collective-permute-start(bf16[4,1024]{1,0:T(4,128)(2,1)} %bitcast.25), channel_id=1, source_target_pairs={{0,12},{4,8},{8,4},{12,0},{1,13},{5,9},{9,5},{13,1},{2,14},{6,10},... | collective-permute-start | bytes 24584 | tf_op jit(solution)/shard_map/ppermute | solution.py:86
  6.3 0.9 %copy-start.3 = (f32[2,1,128,128]{3,2,1,0:T(8,128)S(1)}, f32[2,1,128,128]{3,2,1,0:T(8,128)}, u32[]{:S(2)}) copy-start(f32[2,1,128,128]{3,2,1,0:T(8,128)} %param.25) | copy-start | bytes 393220
  7.2 4.8 %slice-start = ((s8[8388608]{0:T(1024)(128)(4,1)}), s8[4194304]{0:T(1024)(128)(4,1)S(1)}, s32[]{:S(2)}) async-start(s8[8388608]{0:T(1024)(128)(4,1)} %bitcast.10), calls=%async_computation | async-start | bytes 8388608
  7.2 4.8 %slice-start.2 = ((s8[8388608]{0:T(1024)(128)(4,1)}), s8[4194304]{0:T(1024)(128)(4,1)S(1)}, s32[]{:S(2)}) async-start(s8[8388608]{0:T(1024)(128)(4,1)} %bitcast.12), calls=%async_computation.2 | async-start | bytes 8388608
  7.3 4.7 %slice-start.1 = ((s8[8388608]{0:T(1024)(128)(4,1)}), s8[4194304]{0:T(1024)(128)(4,1)S(1)}, s32[]{:S(2)}) async-start(s8[8388608]{0:T(1024)(128)(4,1)} %bitcast.10), calls=%async_computation.1 | async-start | bytes 8388608
  7.3 5.9 %slice-start.3 = ((s8[8388608]{0:T(1024)(128)(4,1)}), s8[4194304]{0:T(1024)(128)(4,1)S(1)}, s32[]{:S(2)}) async-start(s8[8388608]{0:T(1024)(128)(4,1)} %bitcast.12), calls=%async_computation.3 | async-start | bytes 8388608
  7.3 9.4 %collective-permute-start.7 = (bf16[2,128,128]{2,1,0:T(8,128)(2,1)S(1)}, bf16[2,128,128]{2,1,0:T(8,128)(2,1)S(1)}, u32[]{:S(2)}, u32[]{:S(2)}) collective-permute-start(bf16[2,128,128]{2,1,0:T(8,128)(2,1)S(1)} %shard_map.143), channel_id=1, source_target_pairs={{0,3},{1,2},{2,1},{3,0},{4,7},{5,6},{6,5},{7,4},{8,11},{9,10},{10,... | collective-permute-start | bytes 196616 | tf_op jit(solution)/shard_map/ppermute | solution.py:86
  13.1 4.8 %copy-start.1 = (bf16[2,128,16,128]{3,2,1,0:T(8,128)(2,1)S(1)}, bf16[2,128,16,128]{3,2,1,0:T(8,128)(2,1)}, u32[]{:S(2)}) copy-start(bf16[2,128,16,128]{3,2,1,0:T(8,128)(2,1)} %map_ref.3) | copy-start | bytes 3145732
  13.1 4.8 %copy-start.2 = (bf16[2,128,16,128]{3,2,1,0:T(8,128)(2,1)S(1)}, bf16[2,128,16,128]{3,2,1,0:T(8,128)(2,1)}, u32[]{:S(2)}) copy-start(bf16[2,128,16,128]{3,2,1,0:T(8,128)(2,1)} %readout_ref.3) | copy-start | bytes 3145732
  13.1 4.8 %copy-start.4 = (f32[2,1,128,128]{3,2,1,0:T(8,128)S(1)}, f32[2,1,128,128]{3,2,1,0:T(8,128)}, u32[]{:S(2)}) copy-start(f32[2,1,128,128]{3,2,1,0:T(8,128)} %param.25) | copy-start | bytes 393220
  13.1 4.8 %copy-start.5 = (f32[2,128,64]{1,2,0:T(8,128)S(1)}, f32[2,128,64]{1,2,0:T(8,128)}, u32[]{:S(2)}) copy-start(f32[2,128,64]{1,2,0:T(8,128)} %param.18) | copy-start | bytes 196612
  13.2 4.8 %copy-start.6 = (f32[2,128,64]{1,2,0:T(8,128)S(1)}, f32[2,128,64]{1,2,0:T(8,128)}, u32[]{:S(2)}) copy-start(f32[2,128,64]{1,2,0:T(8,128)} %param.19) | copy-start | bytes 196612
  13.2 4.8 %copy-start.8 = (f32[2,128]{1,0:T(2,128)S(1)}, f32[2,128]{1,0:T(2,128)}, u32[]{:S(2)}) copy-start(f32[2,128]{1,0:T(2,128)} %log_step_ref.3) | copy-start | bytes 3076
  13.2 7.2 %copy-start = (bf16[2,2048,1024]{2,1,0:T(8,128)(2,1)S(1)}, bf16[2,2048,1024]{2,1,0:T(8,128)(2,1)}, u32[]{:S(2)}) copy-start(bf16[2,2048,1024]{2,1,0:T(8,128)(2,1)} %refs_13_.1) | copy-start | bytes 25165828
  13.2 7.1 %copy-start.7 = (bf16[2,2048]{1,0:T(2,128)(2,1)S(1)}, bf16[2,2048]{1,0:T(2,128)(2,1)}, u32[]{:S(2)}) copy-start(bf16[2,2048]{1,0:T(2,128)(2,1)} %refs_10_.3) | copy-start | bytes 24580
  14.5 4.5 %collective-permute-start.3 = (bf16[8,4224]{1,0:T(8,128)(2,1)S(1)}, bf16[8,4224]{1,0:T(8,128)(2,1)S(1)}, u32[]{:S(2)}, u32[]{:S(2)}) collective-permute-start(bf16[8,4224]{1,0:T(8,128)(2,1)S(1)} %get-tuple-element.32.refs_0_), channel_id=1, source_target_pairs={{0,1},{1,0},{2,3},{3,2},{4,5},{5,4},{6,7},{7,6},{8,9},{9,8},{10,11... | collective-permute-start | bytes 202760 | tf_op jit(solution)/shard_map/ppermute | solution.py:86
  14.5 4.6 %collective-permute-start.4 = (bf16[8,4224]{1,0:T(8,128)(2,1)S(1)}, bf16[8,4224]{1,0:T(8,128)(2,1)S(1)}, u32[]{:S(2)}, u32[]{:S(2)}) collective-permute-start(bf16[8,4224]{1,0:T(8,128)(2,1)S(1)} %get-tuple-element.32.refs_0_), channel_id=1, source_target_pairs={{0,2},{1,3},{2,0},{3,1},{4,6},{5,7},{6,4},{7,5},{8,10},{9,11},{10,... | collective-permute-start | bytes 202760 | tf_op jit(solution)/shard_map/ppermute | solution.py:86
  16.3 4.1 %collective-permute-start.5 = (bf16[8,4224]{1,0:T(8,128)(2,1)S(1)}, bf16[8,4224]{1,0:T(8,128)(2,1)S(1)}, u32[]{:S(2)}, u32[]{:S(2)}) collective-permute-start(bf16[8,4224]{1,0:T(8,128)(2,1)S(1)} %get-tuple-element.32.refs_0_), channel_id=1, source_target_pairs={{0,3},{1,2},{2,1},{3,0},{4,7},{5,6},{6,5},{7,4},{8,11},{9,10},{10,... | collective-permute-start | bytes 202760 | tf_op jit(solution)/shard_map/ppermute | solution.py:86
  16.4 1.3 %collective-permute-start.6 = (bf16[2,128,128]{2,1,0:T(8,128)(2,1)S(1)}, bf16[2,128,128]{2,1,0:T(8,128)(2,1)S(1)}, u32[]{:S(2)}, u32[]{:S(2)}) collective-permute-start(bf16[2,128,128]{2,1,0:T(8,128)(2,1)S(1)} %shard_map.143), channel_id=1, source_target_pairs={{0,1},{1,0},{2,3},{3,2},{4,5},{5,4},{6,7},{7,6},{8,9},{9,8},{10,11... | collective-permute-start | bytes 196616 | tf_op jit(solution)/shard_map/ppermute | solution.py:86
  16.7 1.3 %collective-permute-start.8 = (bf16[2,128,128]{2,1,0:T(8,128)(2,1)S(1)}, bf16[2,128,128]{2,1,0:T(8,128)(2,1)S(1)}, u32[]{:S(2)}, u32[]{:S(2)}) collective-permute-start(bf16[2,128,128]{2,1,0:T(8,128)(2,1)S(1)} %collective-permute-done.7.refs_3_), channel_id=1, source_target_pairs={{0,1},{1,0},{2,3},{3,2},{4,5},{5,4},{6,7},{7,6},{8,9},{9,8},{10,11... | collective-permute-start | bytes 196616 | tf_op jit(solution)/shard_map/ppermute | solution.py:86
  21.7 4.4 %collective-permute-start.9 = (bf16[8,1024]{1,0:T(8,128)(2,1)S(1)}, bf16[8,1024]{1,0:T(8,128)(2,1)S(1)}, u32[]{:S(2)}, u32[]{:S(2)}) collective-permute-start(bf16[8,1024]{1,0:T(8,128)(2,1)S(1)} %get-tuple-element.39.refs_0_), channel_id=1, source_target_pairs={{0,4},{4,0},{8,12},{12,8},{1,5},{5,1},{9,13},{13,9},{2,6},{6,2},{1... | collective-permute-start | bytes 49160 | tf_op jit(solution)/shard_map/ppermute | solution.py:86
  22.4 5.2 %collective-permute-start.10 = (bf16[8,1024]{1,0:T(8,128)(2,1)S(1)}, bf16[8,1024]{1,0:T(8,128)(2,1)S(1)}, u32[]{:S(2)}, u32[]{:S(2)}) collective-permute-start(bf16[8,1024]{1,0:T(8,128)(2,1)S(1)} %get-tuple-element.39.refs_0_), channel_id=1, source_target_pairs={{0,8},{4,12},{8,0},{12,4},{1,9},{5,13},{9,1},{13,5},{2,10},{6,14},... | collective-permute-start | bytes 49160 | tf_op jit(solution)/shard_map/ppermute | solution.py:86
  25.9 5.5 %collective-permute-start.11 = (bf16[8,1024]{1,0:T(8,128)(2,1)S(1)}, bf16[8,1024]{1,0:T(8,128)(2,1)S(1)}, u32[]{:S(2)}, u32[]{:S(2)}) collective-permute-start(bf16[8,1024]{1,0:T(8,128)(2,1)S(1)} %get-tuple-element.39.refs_0_), channel_id=1, source_target_pairs={{0,12},{4,8},{8,4},{12,0},{1,13},{5,9},{9,5},{13,1},{2,14},{6,10},... | collective-permute-start | bytes 49160 | tf_op jit(solution)/shard_map/ppermute | solution.py:86
  32.6 3.0 %collective-permute-start.12 = (bf16[8,4224]{1,0:T(8,128)(2,1)S(1)}, bf16[8,4224]{1,0:T(8,128)(2,1)S(1)}, u32[]{:S(2)}, u32[]{:S(2)}) collective-permute-start(bf16[8,4224]{1,0:T(8,128)(2,1)S(1)} %get-tuple-element.40.refs_0_), channel_id=1, source_target_pairs={{0,1},{1,0},{2,3},{3,2},{4,5},{5,4},{6,7},{7,6},{8,9},{9,8},{10,11... | collective-permute-start | bytes 202760 | tf_op jit(solution)/shard_map/ppermute | solution.py:86
  32.6 4.7 %collective-permute-start.13 = (bf16[8,4224]{1,0:T(8,128)(2,1)S(1)}, bf16[8,4224]{1,0:T(8,128)(2,1)S(1)}, u32[]{:S(2)}, u32[]{:S(2)}) collective-permute-start(bf16[8,4224]{1,0:T(8,128)(2,1)S(1)} %get-tuple-element.40.refs_0_), channel_id=1, source_target_pairs={{0,2},{1,3},{2,0},{3,1},{4,6},{5,7},{6,4},{7,5},{8,10},{9,11},{10,... | collective-permute-start | bytes 202760 | tf_op jit(solution)/shard_map/ppermute | solution.py:86
  34.1 4.3 %collective-permute-start.14 = (bf16[8,4224]{1,0:T(8,128)(2,1)S(1)}, bf16[8,4224]{1,0:T(8,128)(2,1)S(1)}, u32[]{:S(2)}, u32[]{:S(2)}) collective-permute-start(bf16[8,4224]{1,0:T(8,128)(2,1)S(1)} %get-tuple-element.40.refs_0_), channel_id=1, source_target_pairs={{0,3},{1,2},{2,1},{3,0},{4,7},{5,6},{6,5},{7,4},{8,11},{9,10},{10,... | collective-permute-start | bytes 202760 | tf_op jit(solution)/shard_map/ppermute | solution.py:86
  39.9 5.1 %collective-permute-start.15 = (bf16[4,1024]{1,0:T(4,128)(2,1)S(1)}, bf16[4,1024]{1,0:T(4,128)(2,1)S(1)}, u32[]{:S(2)}, u32[]{:S(2)}) collective-permute-start(bf16[4,1024]{1,0:T(4,128)(2,1)S(1)} %get-tuple-element.49), channel_id=1, source_target_pairs={{0,4},{4,0},{8,12},{12,8},{1,5},{5,1},{9,13},{13,9},{2,6},{6,2},{1... | collective-permute-start | bytes 24584 | tf_op jit(solution)/shard_map/ppermute | solution.py:86
  39.9 5.1 %collective-permute-start.16 = (bf16[4,1024]{1,0:T(4,128)(2,1)S(1)}, bf16[4,1024]{1,0:T(4,128)(2,1)S(1)}, u32[]{:S(2)}, u32[]{:S(2)}) collective-permute-start(bf16[4,1024]{1,0:T(4,128)(2,1)S(1)} %get-tuple-element.50), channel_id=1, source_target_pairs={{0,8},{4,12},{8,0},{12,4},{1,9},{5,13},{9,1},{13,5},{2,10},{6,14},... | collective-permute-start | bytes 24584 | tf_op jit(solution)/shard_map/ppermute | solution.py:86
  40.6 5.4 %collective-permute-start.17 = (bf16[4,1024]{1,0:T(4,128)(2,1)S(1)}, bf16[4,1024]{1,0:T(4,128)(2,1)S(1)}, u32[]{:S(2)}, u32[]{:S(2)}) collective-permute-start(bf16[4,1024]{1,0:T(4,128)(2,1)S(1)} %get-tuple-element.51), channel_id=1, source_target_pairs={{0,12},{4,8},{8,4},{12,0},{1,13},{5,9},{9,5},{13,1},{2,14},{6,10},... | collective-permute-start | bytes 24584 | tf_op jit(solution)/shard_map/ppermute | solution.py:86
